TPU v7x, 256 devices: a whole 4x4x8 slice. The times are simulated.
256 devices in a mesh: ep: 16 (over y, x), tp: 16 (over z, core).
Axes of the slice: x: 4, y: 4, z: 8, core: 2. Of those that a mesh axis runs over, the one named last changes fastest.
Arguments:
- tokens: bfloat16 [1024, 4096], P('ep'), may hold values from -6 to 6
- norm_gain: float32 [4096], replicated, may hold values from 0.1 to 1.9
- ffn_gain: float32 [4096], replicated, may hold values from 0.1 to 1.9
- w_in: bfloat16 [4096, 2048], P(None, 'tp'), may hold values from -0.09375 to 0.09375
- decay_rate: float32 [8192], P('tp'), may hold values from 0.02 to 2
- frequency: float32 [8192], P('tp'), may hold values from -3.140625 to 3.140625
- log_step: float32 [128], P('tp'), may hold values from -2.3 to 0
- input_real: float32 [16, 8192], P(None, 'tp'), may hold values from -1 to 1
- input_imag: float32 [16, 8192], P(None, 'tp'), may hold values from -1 to 1
- readout_real: float32 [16, 8192], P(None, 'tp'), may hold values from -0.5 to 0.5
- readout_imag: float32 [16, 8192], P(None, 'tp'), may hold values from -0.5 to 0.5
- skip_gain: float32 [2048], P('tp'), may hold values from -4 to 4
- state_real: float32 [1024, 8192], P('ep', 'tp'), may hold values from -6 to 6
- state_imag: float32 [1024, 8192], P('ep', 'tp'), may hold values from -6 to 6
- w_out: bfloat16 [2048, 4096], P('tp'), may hold values from -0.125 to 0.125
- shared_gate: bfloat16 [4096, 1024], P(None, 'tp'), may hold values from -0.09375 to 0.09375
- shared_up: bfloat16 [4096, 1024], P(None, 'tp'), may hold values from -0.09375 to 0.09375
- shared_down: bfloat16 [1024, 4096], P('tp'), may hold values from -0.1875 to 0.1875
- expert_gate: bfloat16 [64, 4096, 1024], P('ep', 'tp'), may hold values from -0.09375 to 0.09375
- expert_up: bfloat16 [64, 4096, 1024], P('ep', 'tp'), may hold values from -0.09375 to 0.09375
- expert_down: bfloat16 [64, 1024, 4096], P('ep', None, 'tp'), may hold values from -0.1875 to 0.1875
- routing: int32 [1024, 4], P('ep'), may hold values from 0 to 63, all different within a row; in each aligned block of 64 rows (0 to 63, 64 to 127, ...) at most 8 rows name the same one
- route_weight: float32 [1024, 4], P('ep'), may hold values from 0.1 to 1
Outputs:
- mixed: bfloat16 [1024, 4096], P('ep', 'tp')
- new_state_real: float32 [1024, 8192], P('ep', 'tp')
- new_state_imag: float32 [1024, 8192], P('ep', 'tp')
Inputs may be any that keep to these rules, and one draw needn't show every extreme that they name: `routing`: each row names 4 different experts. In the rows of one index of ep (aligned blocks of 64 rows) no expert is named more than 8 times, and in every draw some expert is named exactly 8 times in some block.
All inputs are finite; a program needn't handle non-finite values.
Results may differ from a plain program's by a relative error of at most 0.02.
Values may be sent and summed in bfloat16 or wider, within the bound.
No kernel may reach another device: no remote copies, remote signals or barrier semaphores. Data moves between devices by JAX's collectives and lax.ppermute only.
A program may use at most 64 MiB of HBM per device.

v0:
```python
import functools

import jax
import jax.numpy as jnp
from jax import lax
from jax.experimental import pallas as pl
from jax.experimental.pallas import tpu as pltpu
from jax.sharding import Mesh
from jax.sharding import PartitionSpec as P


EPS = 1e-06
ROUTED_SCALE = 2.5
TP = ("z", "c")
F32, BF16 = jnp.float32, jnp.bfloat16
ROOM = pltpu.CompilerParams(vmem_limit_bytes=20 * 2**20)


def swapped(x):
    return lax.ppermute(x, "c", [(0, 1), (1, 0)])


def exchanged(x, axis, bit):
    return lax.ppermute(x, axis, [(i, i ^ bit) for i in range(lax.axis_size(axis))])


def of_pair(x, which, dim):
    width = x.shape[dim] // 2
    return lax.dynamic_slice_in_dim(x, which * width, width, dim)


def rms_scale(values_in, gains):
    values = values_in.astype(F32)
    factor = lax.rsqrt(jnp.mean(values * values, axis=-1, keepdims=True) + EPS)
    return (values * factor * gains).astype(BF16)


def dot32(a, b):
    return jnp.dot(a, b, preferred_element_type=F32)


def dot_nt(a, b):
    return lax.dot_general(a, b, (((1,), (1,)), ((), ())), preferred_element_type=F32)


def two_parts(x):
    high = x.astype(BF16)
    return high, (x - high.astype(F32)).astype(BF16)


def cost(flops, moved):
    return pl.CostEstimate(flops=flops, bytes_accessed=moved, transcendentals=0)


def fetch(source, target, arrival):
    copy = pltpu.make_async_copy(source, target, arrival)
    copy.start()
    copy.wait()


def front_kernel(
    core,
    log_step,
    tokens,
    norm_gain,
    w_in,
    decay_rate,
    frequency,
    input_real,
    input_imag,
    readout_real,
    readout_imag,
    skip_gain,
    state_real,
    state_imag,
    w_out,
    new_real,
    new_imag,
    kept,
    given,
):
    groups = log_step.shape[0]
    chan_count, entries = input_real.shape
    channels = skip_gain.shape[1]
    width = entries // groups
    normed = rms_scale(tokens[...], norm_gain[...])
    drive = dot32(normed, w_in[...]).astype(BF16)
    group_of = lax.broadcasted_iota(jnp.int32, (1, entries), 1) // width
    step_size = jnp.zeros((1, entries), F32)
    for g in range(groups):
        step_size = jnp.where(group_of == g, log_step[g], step_size)
    step_size = jnp.exp(step_size)
    decays, omegas = decay_rate[...], frequency[...]
    pole_mag = jnp.exp(-decays * step_size)
    pole_angle = omegas * step_size
    pole_re = pole_mag * jnp.cos(pole_angle)
    pole_im = pole_mag * jnp.sin(pole_angle)
    pole_norm = decays * decays + omegas * omegas
    diff_re = pole_re - 1.0
    lift_re = (-decays * diff_re + omegas * pole_im) / pole_norm
    lift_im = (-decays * pole_im - omegas * diff_re) / pole_norm
    row_group = lax.broadcasted_iota(jnp.int32, (channels, entries), 0) // chan_count
    col_group = lax.broadcasted_iota(jnp.int32, (channels, entries), 1) // width
    same = row_group == col_group

    def spread(block):
        return two_parts(jnp.where(same, jnp.concatenate([block[...]] * groups, axis=0), 0.0))

    def push_of(block):
        high, low = spread(block)
        return dot32(drive, high) + dot32(drive, low)

    push_re, push_im = push_of(input_real), push_of(input_imag)
    old_re, old_im = state_real[...], state_imag[...]
    new_re = pole_re * old_re - pole_im * old_im + lift_re * push_re - lift_im * push_im
    new_im = pole_re * old_im + pole_im * old_re + lift_re * push_im + lift_im * push_re
    new_real[...] = new_re
    new_imag[...] = new_im

    def read_of(state, block):
        (high, low), (block_high, block_low) = two_parts(state), spread(block)
        return dot_nt(high, block_high) + dot_nt(high, block_low) + dot_nt(low, block_high)

    read = read_of(new_re, readout_real) - read_of(new_im, readout_imag)
    read = read + skip_gain[...] * drive.astype(F32)
    bent = jnp.tanh(0.7978845608028654 * (read + 0.044715 * (read * read * read)))
    activated = (0.5 * read * (1.0 + bent)).astype(BF16)
    wide = kept.shape[2]
    for z in range(kept.shape[0]):
        for out, c in ((kept, core[0]), (given, 1 - core[0])):
            at = pl.multiple_of((2 * z + c) * wide, wide)
            out[z] = dot32(activated, w_out[:, pl.ds(at, wide)]).astype(out.dtype)


def front(core, log_step, *arrays):
    tokens, w_out, state = arrays[0], arrays[-1], arrays[-2]
    seqs, model_width = tokens.shape
    z_count = lax.axis_size("z")
    part = (z_count, seqs, model_width // (2 * z_count))
    smem, vmem = pl.BlockSpec(memory_space=pltpu.SMEM), pl.BlockSpec(memory_space=pltpu.VMEM)
    return pl.pallas_call(
        front_kernel,
        out_shape=(
            jax.ShapeDtypeStruct(state.shape, F32),
            jax.ShapeDtypeStruct(state.shape, F32),
            jax.ShapeDtypeStruct(part, F32),
            jax.ShapeDtypeStruct(part, BF16),
        ),
        in_specs=[smem, smem] + [vmem] * len(arrays),
        out_specs=(vmem,) * 4,
        cost_estimate=cost(4 * seqs * model_width * w_out.shape[0], 2 * w_out.size * 2),
        name="front",
    )(core, log_step, *arrays)


def gate_up_kernel(
    at, arrived, gain, gate, gate_par, up, up_par, sent, incoming, weights, parcel, ins, outs
):
    half, _, _, width, _ = weights.shape
    seq_devs, _, pair_slots, _ = incoming.shape
    z_count, _, lanes = parcel.shape
    capacity = pair_slots // half
    rows = seq_devs * capacity
    first = pltpu.make_async_copy(arrived, incoming, ins.at[0])
    first.start()
    loads = {}
    for e in range(half):
        for m, (own, par) in enumerate(((gate, gate_par), (up, up_par))):
            for part, source in enumerate((own.at[half * at[0] + e], par.at[e])):
                arrival = ins.at[1 + 4 * e + 2 * m + part]
                copy = pltpu.make_async_copy(source, weights.at[e, m, part], arrival)
                copy.start()
                loads[e, m, part] = copy
    ones = jnp.ones((8, width), BF16)
    features = [pl.ds(pl.multiple_of(at[1 + part] * width, width), width) for part in range(2)]
    first.wait()
    stores = []

    def store(depth, size):
        place = pl.ds(depth, size)
        copy = pltpu.make_async_copy(
            parcel.at[:, place, :], sent.at[:, place, :], outs.at[len(stores)]
        )
        copy.start()
        stores.append(copy)

    scaled = {}
    for e in range(half):
        squares = jnp.zeros((8, rows), F32)
        for part in range(2):
            values = incoming[:, part, e * capacity : (e + 1) * capacity, :]
            values = values.reshape(rows, width).astype(F32)
            scaled[e, part] = (values * gain[:, features[part]]).astype(BF16)
            high, low = two_parts(values * values)
            squares = squares + dot_nt(ones, high) + dot_nt(ones, low)
        high, low = two_parts(squares)
        line = lax.broadcasted_iota(jnp.int32, squares.shape, 0)
        both = jnp.where(line == 0, high.astype(F32), jnp.where(line == 1, low.astype(F32), 0.0))
        depth = 2 * half * rows + e * 8
        for z in range(z_count):
            parcel[z, depth : depth + 8, :] = both.astype(BF16)
    store(2 * half * rows, half * 8)
    for e in range(half):
        for m in range(2):
            for part in range(2):
                loads[e, m, part].wait()
            sums = dot32(scaled[e, 0], weights[e, m, 0]) + dot32(scaled[e, 1], weights[e, m, 1])
            sums = sums.astype(BF16)
            depth = (half * m + e) * rows
            for z in range(z_count):
                parcel[z, depth : depth + rows, :] = sums[:, z * lanes : (z + 1) * lanes]
            store(depth, rows)
    for copy in stores:
        copy.wait()


def gate_up(at, incoming, gain, gate, gate_par, up, up_par):
    seq_devs, _, pair_slots, width = incoming.shape
    half, _, units = gate_par.shape
    z_count = lax.axis_size("z")
    pair_rows = seq_devs * pair_slots
    parcel = (z_count, 2 * pair_rows + half * 8, units // z_count)
    smem, vmem = pl.BlockSpec(memory_space=pltpu.SMEM), pl.BlockSpec(memory_space=pltpu.VMEM)
    far, any_place = pl.BlockSpec(memory_space=pltpu.HBM), pl.BlockSpec(memory_space=pl.ANY)
    return pl.pallas_call(
        gate_up_kernel,
        in_specs=[smem, any_place, vmem, far, any_place, far, any_place],
        out_specs=far,
        out_shape=pltpu.HBM(parcel, BF16),
        scratch_shapes=[
            pltpu.VMEM(incoming.shape, BF16),
            pltpu.VMEM((half, 2, 2, width, units), BF16),
            pltpu.VMEM(parcel, BF16),
            pltpu.SemaphoreType.DMA((1 + 4 * half,)),
            pltpu.SemaphoreType.DMA((1 + 2 * half,)),
        ],
        compiler_params=pltpu.CompilerParams(vmem_limit_bytes=62 * 2**20),
        cost_estimate=cost(8 * pair_rows * width * units, 8 * half * width * units),
        name="gate_up",
    )(at, incoming, gain, gate, gate_par, up, up_par)


def dispatch_kernel(spread, own_in, par_in, outgoing, own, par, arrivals):
    copies = [
        pltpu.make_async_copy(source, target, arrivals.at[i])
        for i, (source, target) in enumerate(((own_in, own), (par_in, par)))
    ]
    for copy in copies:
        copy.start()
    for copy in copies:
        copy.wait()
    shape = outgoing.shape[:1] + outgoing.shape[2:]
    for part, rows in enumerate((own, par)):
        outgoing[:, part] = dot32(spread[...], rows[...]).astype(BF16).reshape(shape)


def dispatch(spread, own, par, ep_count):
    slots, (_, width) = spread.shape[0], own.shape
    vmem = pl.BlockSpec(memory_space=pltpu.VMEM)
    return pl.pallas_call(
        dispatch_kernel,
        out_shape=jax.ShapeDtypeStruct((ep_count, 2, slots // ep_count, width), BF16),
        in_specs=[vmem, pl.BlockSpec(memory_space=pl.ANY), pl.BlockSpec(memory_space=pl.ANY)],
        out_specs=vmem,
        scratch_shapes=[
            pltpu.VMEM(own.shape, BF16),
            pltpu.VMEM(own.shape, BF16),
            pltpu.SemaphoreType.DMA((2,)),
        ],
        compiler_params=ROOM,
        cost_estimate=cost(4 * spread.size * width, 4 * slots * width),
        name="dispatch",
    )(spread, own, par)


def combine_kernel(weights, arrived, own, given, returned, arrival):
    fetch(arrived, returned, arrival)
    high, low = two_parts(weights[...])
    rows, width = weights.shape[1], returned.shape[3]
    for part, out in enumerate((own, given)):
        values = returned[:, part].reshape(rows, width)
        out[...] = (dot32(high, values) + dot32(low, values)).astype(out.dtype)


def combined(weights, returned):
    shape = (weights.shape[0], returned.shape[3])
    vmem = pl.BlockSpec(memory_space=pltpu.VMEM)
    return pl.pallas_call(
        combine_kernel,
        out_shape=(jax.ShapeDtypeStruct(shape, F32), jax.ShapeDtypeStruct(shape, BF16)),
        in_specs=[vmem, pl.BlockSpec(memory_space=pl.ANY)],
        out_specs=(vmem, vmem),
        scratch_shapes=[pltpu.VMEM(returned.shape, BF16), pltpu.SemaphoreType.DMA],
        compiler_params=ROOM,
        cost_estimate=cost(8 * weights.size * shape[1], 2 * returned.size),
        name="combine",
    )(weights, returned)


def shared_kernel(at, pieces, gain, gate_t, up_t, down_t, kept, given):
    c, z = at[0], at[1] // 2
    seqs, width = kept.shape[1:]
    squares = jnp.zeros((seqs, 1), F32)
    gate = jnp.zeros((seqs, gate_t.shape[0]), F32)
    up = gate
    chips = grown_order(kept.shape[0])
    for part, place in ((0, c), (1, 1 - c)):
        rows = [piece[part][i] for piece in pieces for i in range(piece[part].shape[0])]
        for chip, values in zip(chips, rows, strict=True):
            values = values.astype(F32)
            squares = squares + jnp.sum(values * values, axis=-1, keepdims=True)
            first = (2 * jnp.bitwise_xor(z, chip) + place) * width
            features = pl.ds(pl.multiple_of(first, width), width)
            scaled = (values * gain[:, features]).astype(BF16)
            gate = gate + dot_nt(scaled, gate_t[:, features])
            up = up + dot_nt(scaled, up_t[:, features])
    factor = lax.rsqrt(squares / (2 * len(chips) * width) + EPS)
    gate, up = gate * factor, up * factor
    inner = (gate / (1.0 + jnp.exp(-gate)) * up).astype(BF16)
    for chip in range(len(chips)):
        for out, place in ((kept, c), (given, 1 - c)):
            first = (2 * jnp.bitwise_xor(z, chip) + place) * width
            features = pl.ds(pl.multiple_of(first, width), width)
            out[chip] = dot32(inner, down_t[:, features]).astype(out.dtype)


def growing(chips):
    far = chips // 2
    return [far] + [1 << i for i in range(far.bit_length() - 1)]


def grown_order(chips):
    order = [0]
    for bit in growing(chips):
        order = order + [owner ^ bit for owner in order]
    return order


def shared_parts(at, pieces, gain, gate_t, up_t, w_down, after):
    smem, vmem = pl.BlockSpec(memory_space=pltpu.SMEM), pl.BlockSpec(memory_space=pltpu.VMEM)
    flat = [rows for piece in pieces for rows in piece]
    (seqs, width), z_count = flat[0].shape[1:], sum(rows.shape[0] for rows in flat) // 2

    def kernel(at, *refs):
        rows, rest = refs[: len(flat)], refs[len(flat) :]
        paired = [(rows[i], rows[i + 1]) for i in range(0, len(flat), 2)]
        shared_kernel(at, paired, *rest[:4], *rest[5:])

    return pl.pallas_call(
        kernel,
        out_shape=(
            jax.ShapeDtypeStruct((z_count, seqs, width), F32),
            jax.ShapeDtypeStruct((z_count, seqs, width), BF16),
        ),
        in_specs=[smem] + [vmem] * (len(flat) + 4) + [pl.BlockSpec(memory_space=pl.ANY)],
        out_specs=(vmem, vmem),
        compiler_params=ROOM,
        cost_estimate=cost(seqs * 6 * w_down.size, 6 * w_down.size),
        name="shared",
    )(at, *flat, gain, gate_t, up_t, w_down, after)


def inner_kernel(model_width, half, arrived, inner, parcels, arrival):
    fetch(arrived, parcels, arrival)
    totals = parcels[0].astype(F32)
    z_count = parcels.shape[0]
    for z in range(1, z_count):
        totals = totals + parcels[z].astype(F32)
    lanes = totals.shape[1]
    pair_rows = inner.shape[1]
    rows = pair_rows // half
    for e in range(half):
        line = 2 * pair_rows + 8 * e
        squares = totals[line : line + 1] + totals[line + 1 : line + 2]
        factor = lax.rsqrt(squares / model_width + EPS)
        factor = jnp.broadcast_to(factor, (lanes, rows)).T
        gate = totals[e * rows : (e + 1) * rows] * factor
        up = totals[pair_rows + e * rows : pair_rows + (e + 1) * rows] * factor
        done = (gate / (1.0 + jnp.exp(-gate)) * up).astype(BF16)
        for z in range(z_count):
            inner[z, e * rows : (e + 1) * rows, :] = done


def inner_copies(parcels, model_width, half):
    z_count, depth, lanes = parcels.shape
    pair_rows = (depth - half * 8) // 2
    return pl.pallas_call(
        functools.partial(inner_kernel, model_width, half),
        out_shape=jax.ShapeDtypeStruct((z_count, pair_rows, lanes), BF16),
        in_specs=[pl.BlockSpec(memory_space=pl.ANY)],
        out_specs=pl.BlockSpec(memory_space=pltpu.VMEM),
        scratch_shapes=[pltpu.VMEM(parcels.shape, BF16), pltpu.SemaphoreType.DMA],
        compiler_params=ROOM,
        cost_estimate=cost(parcels.size * 4, parcels.size * 4),
        name="inner",
    )(parcels)


def down_kernel(at, arrived, own, par, sent, inner, weights, results, ins, outs):
    half = weights.shape[0]
    first = pltpu.make_async_copy(arrived, inner, ins.at[0])
    first.start()
    loads = []
    for e in range(half):
        for part, source in enumerate((own.at[half * at[0] + e], par.at[e])):
            arrival = ins.at[1 + 2 * e + part]
            copy = pltpu.make_async_copy(source, weights.at[e, part], arrival)
            copy.start()
            loads.append(copy)
    first.wait()
    rows = inner.shape[1] // half
    seq_devs, _, pair_slots, width = results.shape
    capacity = pair_slots // half
    stores = []
    for e in range(half):
        row = [inner[z, e * rows : (e + 1) * rows, :] for z in range(inner.shape[0])]
        row = jnp.concatenate(row, axis=1)
        place = slice(e * capacity, (e + 1) * capacity)
        for part in range(2):
            loads[2 * e + part].wait()
            out = dot32(row, weights[e, part]).astype(BF16)
            results[:, part, place, :] = out.reshape(seq_devs, capacity, width)
        place = pl.ds(e * capacity, capacity)
        copy = pltpu.make_async_copy(
            results.at[:, :, place, :], sent.at[:, :, place, :], outs.at[e]
        )
        copy.start()
        stores.append(copy)
    for copy in stores:
        copy.wait()


def down(at, inner, w_down, w_par, seq_devs, capacity):
    half, units, width = w_par.shape
    results = (seq_devs, 2, half * capacity, width)
    smem, any_place = pl.BlockSpec(memory_space=pltpu.SMEM), pl.BlockSpec(memory_space=pl.ANY)
    return pl.pallas_call(
        down_kernel,
        in_specs=[smem, any_place, any_place, any_place],
        out_specs=pl.BlockSpec(memory_space=pltpu.HBM),
        out_shape=pltpu.HBM(results, BF16),
        scratch_shapes=[
            pltpu.VMEM(inner.shape, BF16),
            pltpu.VMEM((half, 2, units, width), BF16),
            pltpu.VMEM(results, BF16),
            pltpu.SemaphoreType.DMA((1 + 2 * half,)),
            pltpu.SemaphoreType.DMA((half,)),
        ],
        compiler_params=ROOM,
        cost_estimate=cost(4 * inner.shape[1] * units * width, 4 * half * units * width),
        name="down",
    )(at, inner, w_down, w_par)


def local(
    tokens,
    norm_gain,
    ffn_gain,
    w_in,
    decay_rate,
    frequency,
    log_step,
    input_real,
    input_imag,
    readout_real,
    readout_imag,
    skip_gain,
    state_real,
    state_imag,
    w_out,
    shared_gate,
    shared_up,
    shared_down,
    expert_gate,
    expert_up,
    expert_down,
    routing,
    route_weight,
):
    seq_count, model_width = tokens.shape
    ep_count, z_count = lax.axis_size("ep"), lax.axis_size("z")
    z, c = lax.axis_index("z"), lax.axis_index("c")
    core = c.reshape(1)
    slice_width = model_width // (2 * z_count)
    offset = (2 * z + c) * slice_width

    partner = []
    for w in (expert_gate, expert_up, expert_down):
        cut = of_pair(w, 1 - c, 0)
        partner.append(swapped(cut))
    gate_par, up_par, down_par = partner

    new_real, new_imag, kept, given = front(
        core,
        log_step,
        tokens,
        norm_gain.reshape(1, -1),
        w_in,
        decay_rate.reshape(1, -1),
        frequency.reshape(1, -1),
        input_real,
        input_imag,
        readout_real,
        readout_imag,
        skip_gain.reshape(1, -1),
        state_real,
        state_imag,
        w_out,
    )
    both = (kept + swapped(given).astype(F32)).astype(BF16)
    mixer_own = lax.all_to_all(both, "z", split_axis=0, concat_axis=0, tiled=True)
    mixer_own = mixer_own.astype(F32).sum(axis=0)
    own_tokens = lax.dynamic_slice_in_dim(tokens, offset, slice_width, 1)
    resid_own = (own_tokens.astype(F32) + mixer_own).astype(BF16)
    resid_par = swapped(resid_own)

    expert_dev = expert_gate.shape[0]
    half = expert_dev // 2
    top_count = routing.shape[1]
    capacity = 2 * seq_count * top_count // (expert_dev * ep_count)
    slot_count = half * ep_count * capacity
    flat_ids = routing.reshape(-1)
    one_hot = (
        flat_ids[:, None] == jnp.arange(expert_dev * ep_count, dtype=jnp.int32)[None, :]
    ).astype(jnp.int32)
    earlier = jnp.cumsum(one_hot, axis=0) - one_hot
    slot_rank = jnp.sum(earlier * one_hot, axis=1)
    home, within = flat_ids // expert_dev, flat_ids % expert_dev
    target = (home * half + within % half) * capacity + slot_rank
    target = jnp.where(within // half == c, target, -1)
    slot_ids = jnp.arange(slot_count, dtype=jnp.int32)
    placed = (target[None, :] == slot_ids[:, None]).reshape(slot_count, seq_count, top_count)
    spread = jnp.sum(placed.astype(F32), axis=2).astype(BF16)
    outgoing = dispatch(spread, resid_own, resid_par, ep_count)
    incoming = lax.all_to_all(outgoing, "ep", split_axis=0, concat_axis=0, tiled=True)

    at = jnp.array([1, 1, -1], jnp.int32) * c + jnp.array([0, 2, 2], jnp.int32) * z
    at = at + jnp.array([0, 0, 1], jnp.int32)
    gain = ffn_gain.reshape(1, -1)
    parcel = gate_up(at, incoming, gain, expert_gate, gate_par, expert_up, up_par)
    parcels = lax.all_to_all(parcel, "z", split_axis=0, concat_axis=0, tiled=True)
    copies = inner_copies(parcels, model_width, half)
    inner_all = lax.all_to_all(copies, "z", split_axis=0, concat_axis=0, tiled=True)
    results = down(at, inner_all, expert_down, down_par, ep_count, capacity)
    returned = lax.all_to_all(results, "ep", split_axis=0, concat_axis=0, tiled=True)

    pieces = [(resid_own[None], resid_par[None])]
    for bit in growing(z_count):
        held = jnp.concatenate([piece[0] for piece in pieces])
        theirs = exchanged(held, "z", bit)
        pieces.append((theirs, swapped(theirs)))
    kept, given = shared_parts(
        at, pieces, gain, shared_gate.T, shared_up.T, shared_down, copies
    )
    got = swapped(given)
    shared_own = kept + got.astype(F32)
    count = z_count // 2
    while count > 0:
        theirs = exchanged(shared_own[count:].astype(BF16), "z", count)
        shared_own = shared_own[:count] + theirs.astype(F32)
        count //= 2
    shared_own = shared_own[0]

    weights = route_weight / jnp.sum(route_weight, axis=1, keepdims=True) * ROUTED_SCALE
    chosen = target.reshape(seq_count, top_count)[:, :, None] == slot_ids[None, None, :]
    combine = jnp.sum(jnp.where(chosen, weights[:, :, None], 0.0), axis=1)
    routed, routed_par = combined(combine, returned)
    routed = routed + swapped(routed_par).astype(F32)
    mixed = (resid_own.astype(F32) + shared_own + routed).astype(BF16)
    return (mixed, new_real, new_imag)


def solution(mesh):
    ep_count, tp_count = mesh.devices.shape
    cores = Mesh(mesh.devices.reshape(ep_count, tp_count // 2, 2), ("ep", "z", "c"))
    placed = (
        P("ep", None),
        P(),
        P(),
        P(None, TP),
        P(TP),
        P(TP),
        P(TP),
        P(None, TP),
        P(None, TP),
        P(None, TP),
        P(None, TP),
        P(TP),
        P("ep", TP),
        P("ep", TP),
        P(TP, None),
        P(None, TP),
        P(None, TP),
        P(TP, None),
        P("ep", TP, None),
        P("ep", TP, None),
        P("ep", None, TP),
        P("ep", None),
        P("ep", None),
    )

    def step(*arrays):
        return local(*arrays)

    step = jax.shard_map(
        step,
        mesh=cores,
        in_specs=placed,
        out_specs=(P("ep", TP), P("ep", TP), P("ep", TP)),
        check_vma=False,
    )
    return step
```

profile of v0, /device:TPU:1, one launch (start us, length us, event | category | flops | bytes accessed | tf_op | source)
XLA Modules:
  0.0 156.0 jit_solution(5753776636766502043)
XLA Ops:
  0.7 4.3 %front.1 = (f32[64,512]{1,0:T(8,128)}, f32[64,512]{1,0:T(8,128)}, f32[8,64,256]{2,1,0:T(8,128)}, bf16[8,64,256]{2,1,0:T(8,128)(2,1)}) custom-call(s32[1]{0:T(128)} %bitcast.core, f32[8]{0:T(128)} %log_step.1, bf16[64,4096]{1,0:T(8,128)(2,1)} %tokens.1, f32[1,4096]{1,0:T(1,128)} %bitcast.46, bf16[4096,128]{1,0:T(8,128)(2,1)} %w_in.1, f32[1,512]{1,0:T(1,128)} %bitcast.47, ...), custom_call_target="tpu_custom_call" | custom-call | flops 134217728 | bytes 2097152 | tf_op jit(solution)/shard_map/front/pallas_call | solution.py:141
  4.9 3.2 %collective-permute-start = (bf16[8,64,256]{2,1,0:T(8,128)(2,1)}, bf16[8,64,256]{2,1,0:T(8,128)(2,1)S(1)}, u32[]{:S(2)}, u32[]{:S(2)}) collective-permute-start(bf16[8,64,256]{2,1,0:T(8,128)(2,1)} %get-tuple-element.12), channel_id=1, source_target_pairs={{0,1},{1,0},{2,3},{3,2},{4,5},{5,4},{6,7},{7,6},{8,9},{9,8},{10,11... | collective-permute-start | bytes 786440 | tf_op jit(solution)/shard_map/ppermute | solution.py:20
  10.9 6.5 %all-to-all-start = ((bf16[8,64,256]{2,1,0:T(8,128)(2,1)}), bf16[8,64,256]{2,1,0:T(8,128)(2,1)S(1)}, u32[]{:S(2)}, u32[]{:S(2)}) async-start(bf16[8,64,256]{2,1,0:T(8,128)(2,1)} %add_convert_fusion), calls=%async_computation | async-start | bytes 524288 | tf_op jit(solution)/shard_map/all_to_all | solution.py:511
  18.7 9.4 %all-to-all-done = bf16[8,64,256]{2,1,0:T(8,128)(2,1)S(1)} async-done(((bf16[8,64,256]{2,1,0:T(8,128)(2,1)}), bf16[8,64,256]{2,1,0:T(8,128)(2,1)S(1)}, u32[]{:S(2)}, u32[]{:S(2)}) %all-to-all-start) | async-done | bytes 262176 | tf_op jit(solution)/shard_map/all_to_all | solution.py:511
  29.0 2.1 %collective-permute-start.1 = (bf16[64,256]{1,0:T(8,128)(2,1)S(1)}, bf16[64,256]{1,0:T(8,128)(2,1)S(1)}, u32[]{:S(2)}, u32[]{:S(2)}) collective-permute-start(bf16[64,256]{1,0:T(8,128)(2,1)S(1)} %add_convert_fusion.1.own_in), channel_id=1, source_target_pairs={{0,1},{1,0},{2,3},{3,2},{4,5},{5,4},{6,7},{7,6},{8,9},{9,8},{10,11... | collective-permute-start | bytes 98312 | tf_op jit(solution)/shard_map/ppermute | solution.py:20
  32.9 6.8 %all-to-all-start.1 = ((bf16[16,2,16,256]{3,2,1,0:T(8,128)(2,1)}), bf16[16,2,16,256]{3,2,1,0:T(8,128)(2,1)S(1)}, u32[]{:S(2)}, u32[]{:S(2)}) async-start(bf16[16,2,16,256]{3,2,1,0:T(8,128)(2,1)} %dispatch.1), calls=%async_computation.1 | async-start | bytes 524288 | tf_op jit(solution)/shard_map/all_to_all | solution.py:535
  40.3 7.5 %all-to-all-done.1.arrived = bf16[16,2,16,256]{3,2,1,0:T(8,128)(2,1)S(1)} async-done(((bf16[16,2,16,256]{3,2,1,0:T(8,128)(2,1)}), bf16[16,2,16,256]{3,2,1,0:T(8,128)(2,1)S(1)}, u32[]{:S(2)}, u32[]{:S(2)}) %all-to-all-start.1) | async-done | bytes 262176 | tf_op jit(solution)/shard_map/all_to_all | solution.py:535
  48.5 4.1 %gate_up.1 = bf16[8,528,128]{2,1,0:T(8,128)(2,1)} custom-call(s32[3]{0:T(128)} %add_add_fusion.at, bf16[16,2,16,256]{3,2,1,0:T(8,128)(2,1)} %copy-done.9, f32[1,4096]{1,0:T(1,128)} %bitcast.44, bf16[4,256,1024]{2,1,0:T(8,128)(2,1)} %gate.1, bf16[2,256,1024]{2,1,0:T(8,128)(2,1)} %collective-permute-done.8.gate_par, bf16[4,256,1024]{2,1,0:T(8,128)(2,1)} %up.1, ...), custom_call_target="tpu_custom_call" | custom-call | flops 536870912 | bytes 4194304 | tf_op jit(solution)/shard_map/gate_up/pallas_call | solution.py:225
  52.6 3.7 %all-to-all-start.2 = ((bf16[8,528,128]{2,1,0:T(8,128)(2,1)}), bf16[8,528,128]{2,1,0:T(8,128)(2,1)S(1)}, u32[]{:S(2)}, u32[]{:S(2)}) async-start(bf16[8,528,128]{2,1,0:T(8,128)(2,1)} %gate_up.1), calls=%async_computation.2 | async-start | bytes 2162688 | tf_op jit(solution)/shard_map/all_to_all | solution.py:541
  56.3 5.3 %collective-permute-start.2 = (bf16[1,64,256]{2,1,0:T(8,128)(2,1)S(1)}, bf16[1,64,256]{2,1,0:T(8,128)(2,1)S(1)}, u32[]{:S(2)}, u32[]{:S(2)}) collective-permute-start(bf16[1,64,256]{2,1,0:T(8,128)(2,1)S(1)} %bitcast.37), channel_id=1, source_target_pairs={{0,8},{2,10},{4,12},{6,14},{8,0},{10,2},{12,4},{14,6},{1,9},{3,11}... | collective-permute-start | bytes 98312 | tf_op jit(solution)/shard_map/ppermute | solution.py:24
  61.6 25.9 %collective-permute-done.2.refs_2_ = bf16[1,64,256]{2,1,0:T(8,128)(2,1)S(1)} collective-permute-done((bf16[1,64,256]{2,1,0:T(8,128)(2,1)S(1)}, bf16[1,64,256]{2,1,0:T(8,128)(2,1)S(1)}, u32[]{:S(2)}, u32[]{:S(2)}) %collective-permute-start.2) | collective-permute-done | bytes 32800 | tf_op jit(solution)/shard_map/ppermute | solution.py:24
  87.6 3.1 %collective-permute-done.4.refs_4_ = bf16[2,64,256]{2,1,0:T(8,128)(2,1)S(1)} collective-permute-done((bf16[2,64,256]{2,1,0:T(8,128)(2,1)S(1)}, bf16[2,64,256]{2,1,0:T(8,128)(2,1)S(1)}, u32[]{:S(2)}, u32[]{:S(2)}) %collective-permute-start.4) | collective-permute-done | bytes 65568 | tf_op jit(solution)/shard_map/ppermute | solution.py:24
  90.9 1.8 %collective-permute-start.5 = (bf16[2,64,256]{2,1,0:T(8,128)(2,1)S(1)}, bf16[2,64,256]{2,1,0:T(8,128)(2,1)S(1)}, u32[]{:S(2)}, u32[]{:S(2)}) collective-permute-start(bf16[2,64,256]{2,1,0:T(8,128)(2,1)S(1)} %collective-permute-done.4.refs_4_), channel_id=1, source_target_pairs={{0,1},{1,0},{2,3},{3,2},{4,5},{5,4},{6,7},{7,6},{8,9},{9,8},{10,11... | collective-permute-start | bytes 196616 | tf_op jit(solution)/shard_map/ppermute | solution.py:20
  92.7 6.0 %collective-permute-done.6.refs_6_ = bf16[4,64,256]{2,1,0:T(8,128)(2,1)S(1)} collective-permute-done((bf16[4,64,256]{2,1,0:T(8,128)(2,1)S(1)}, bf16[4,64,256]{2,1,0:T(8,128)(2,1)S(1)}, u32[]{:S(2)}, u32[]{:S(2)}) %collective-permute-start.6) | collective-permute-done | bytes 131104 | tf_op jit(solution)/shard_map/ppermute | solution.py:24
  98.7 1.5 collective-permute-start.7
  102.9 1.4 collective-permute-done.3.refs_3_
  108.1 2.4 %shared.1 = (f32[8,64,256]{2,1,0:T(8,128)S(1)}, bf16[8,64,256]{2,1,0:T(8,128)(2,1)}) custom-call(s32[3]{0:T(128)S(1)} %copy-done.5, bf16[1,64,256]{2,1,0:T(8,128)(2,1)S(1)} %bitcast.40, bf16[1,64,256]{2,1,0:T(8,128)(2,1)S(1)} %bitcast.43, bf16[1,64,256]{2,1,0:T(8,128)(2,1)S(1)} %collective-permute-done.2.refs_2_, ...), custom_call_target="tpu_custom_call" | custom-call | flops 100663296 | bytes 1572864 | tf_op jit(solution)/shard_map/shared/pallas_call | solution.py:349
  110.6 3.5 %all-to-all-start.3 = ((bf16[8,256,128]{2,1,0:T(8,128)(2,1)}), bf16[8,256,128]{2,1,0:T(8,128)(2,1)S(1)}, u32[]{:S(2)}, u32[]{:S(2)}) async-start(bf16[8,256,128]{2,1,0:T(8,128)(2,1)} %inner.1.refs_12_), calls=%async_computation.3 | async-start | bytes 1048576 | tf_op jit(solution)/shard_map/all_to_all | solution.py:543
  114.3 5.5 %collective-permute-start.11 = (bf16[4,64,256]{2,1,0:T(8,128)(2,1)S(1)}, bf16[4,64,256]{2,1,0:T(8,128)(2,1)S(1)}, u32[]{:S(2)}, u32[]{:S(2)}) collective-permute-start(bf16[4,64,256]{2,1,0:T(8,128)(2,1)S(1)} %slice.57), channel_id=1, source_target_pairs={{0,8},{2,10},{4,12},{6,14},{8,0},{10,2},{12,4},{14,6},{1,9},{3,11}... | collective-permute-start | bytes 393224 | tf_op jit(solution)/shard_map/ppermute | solution.py:24
  119.8 17.8 %collective-permute-done.11 = bf16[4,64,256]{2,1,0:T(8,128)(2,1)S(1)} collective-permute-done((bf16[4,64,256]{2,1,0:T(8,128)(2,1)S(1)}, bf16[4,64,256]{2,1,0:T(8,128)(2,1)S(1)}, u32[]{:S(2)}, u32[]{:S(2)}) %collective-permute-start.11) | collective-permute-done | bytes 131104 | tf_op jit(solution)/shard_map/ppermute | solution.py:24
  137.8 3.2 %down.1 = bf16[16,2,16,256]{3,2,1,0:T(8,128)(2,1)} custom-call(s32[3]{0:T(128)S(1)} %copy-done.6, bf16[8,256,128]{2,1,0:T(8,128)(2,1)S(1)} %all-to-all-done.3.arrived, bf16[4,1024,256]{2,1,0:T(8,128)(2,1)S(1)} %copy-done, bf16[2,1024,256]{2,1,0:T(8,128)(2,1)} %collective-permute-done.14.par), custom_call_target="tpu_custom_call" | custom-call | flops 268435456 | bytes 2097152 | tf_op jit(solution)/shard_map/down/pallas_call | solution.py:437
  141.1 3.5 %all-to-all-start.4 = ((bf16[16,2,16,256]{3,2,1,0:T(8,128)(2,1)}), bf16[16,2,16,256]{3,2,1,0:T(8,128)(2,1)S(1)}, u32[]{:S(2)}, u32[]{:S(2)}) async-start(bf16[16,2,16,256]{3,2,1,0:T(8,128)(2,1)} %down.1), calls=%async_computation.4 | async-start | bytes 524288 | tf_op jit(solution)/shard_map/all_to_all | solution.py:545
  144.9 7.5 %all-to-all-done.4.arrived = bf16[16,2,16,256]{3,2,1,0:T(8,128)(2,1)S(1)} async-done(((bf16[16,2,16,256]{3,2,1,0:T(8,128)(2,1)}), bf16[16,2,16,256]{3,2,1,0:T(8,128)(2,1)S(1)}, u32[]{:S(2)}, u32[]{:S(2)}) %all-to-all-start.4) | async-done | bytes 262176 | tf_op jit(solution)/shard_map/all_to_all | solution.py:545
  152.7 1.9 %collective-permute-start.15 = (bf16[64,256]{1,0:T(8,128)(2,1)S(1)}, bf16[64,256]{1,0:T(8,128)(2,1)S(1)}, u32[]{:S(2)}, u32[]{:S(2)}) collective-permute-start(bf16[64,256]{1,0:T(8,128)(2,1)S(1)} %get-tuple-element.16), channel_id=1, source_target_pairs={{0,1},{1,0},{2,3},{3,2},{4,5},{5,4},{6,7},{7,6},{8,9},{9,8},{10,11... | collective-permute-start | bytes 98312 | tf_op jit(solution)/shard_map/ppermute | solution.py:20
  (94 shorter events, 17.1 us)
Async XLA Ops:
  4.9 5.2 %collective-permute-start = (bf16[8,64,256]{2,1,0:T(8,128)(2,1)}, bf16[8,64,256]{2,1,0:T(8,128)(2,1)S(1)}, u32[]{:S(2)}, u32[]{:S(2)}) collective-permute-start(bf16[8,64,256]{2,1,0:T(8,128)(2,1)} %get-tuple-element.12), channel_id=1, source_target_pairs={{0,1},{1,0},{2,3},{3,2},{4,5},{5,4},{6,7},{7,6},{8,9},{9,8},{10,11... | collective-permute-start | bytes 786440 | tf_op jit(solution)/shard_map/ppermute | solution.py:20
  8.2 39.6 %collective-permute-start.8 = (bf16[2,256,1024]{2,1,0:T(8,128)(2,1)S(1)}, bf16[2,256,1024]{2,1,0:T(8,128)(2,1)}, u32[]{:S(2)}, u32[]{:S(2)}) collective-permute-start(bf16[2,256,1024]{2,1,0:T(8,128)(2,1)S(1)} %constant_dynamic-slice_fusion.2), channel_id=1, source_target_pairs={{0,1},{1,0},{2,3},{3,2},{4,5},{5,4},{6,7},{7,6},{8,9},{9,8},{10,11... | collective-permute-start | bytes 3145736 | tf_op jit(solution)/shard_map/ppermute | solution.py:20
  9.8 29.9 %copy-start.15 = (s32[3]{0:T(128)S(1)}, s32[3]{0:T(128)}, u32[]{:S(2)}) copy-start(s32[3]{0:T(128)} %constant.81.clone) | copy-start | bytes 40
  9.8 38.0 %collective-permute-start.9 = (bf16[2,256,1024]{2,1,0:T(8,128)(2,1)S(1)}, bf16[2,256,1024]{2,1,0:T(8,128)(2,1)}, u32[]{:S(2)}, u32[]{:S(2)}) collective-permute-start(bf16[2,256,1024]{2,1,0:T(8,128)(2,1)S(1)} %constant_dynamic-slice_fusion.1), channel_id=1, source_target_pairs={{0,1},{1,0},{2,3},{3,2},{4,5},{5,4},{6,7},{7,6},{8,9},{9,8},{10,11... | collective-permute-start | bytes 3145736 | tf_op jit(solution)/shard_map/ppermute | solution.py:20
  10.9 17.3 %all-to-all-start = ((bf16[8,64,256]{2,1,0:T(8,128)(2,1)}), bf16[8,64,256]{2,1,0:T(8,128)(2,1)S(1)}, u32[]{:S(2)}, u32[]{:S(2)}) async-start(bf16[8,64,256]{2,1,0:T(8,128)(2,1)} %add_convert_fusion), calls=%async_computation | async-start | bytes 524288 | tf_op jit(solution)/shard_map/all_to_all | solution.py:511
  29.0 2.9 %collective-permute-start.1 = (bf16[64,256]{1,0:T(8,128)(2,1)S(1)}, bf16[64,256]{1,0:T(8,128)(2,1)S(1)}, u32[]{:S(2)}, u32[]{:S(2)}) collective-permute-start(bf16[64,256]{1,0:T(8,128)(2,1)S(1)} %add_convert_fusion.1.own_in), channel_id=1, source_target_pairs={{0,1},{1,0},{2,3},{3,2},{4,5},{5,4},{6,7},{7,6},{8,9},{9,8},{10,11... | collective-permute-start | bytes 98312 | tf_op jit(solution)/shard_map/ppermute | solution.py:20
  32.9 14.9 %all-to-all-start.1 = ((bf16[16,2,16,256]{3,2,1,0:T(8,128)(2,1)}), bf16[16,2,16,256]{3,2,1,0:T(8,128)(2,1)S(1)}, u32[]{:S(2)}, u32[]{:S(2)}) async-start(bf16[16,2,16,256]{3,2,1,0:T(8,128)(2,1)} %dispatch.1), calls=%async_computation.1 | async-start | bytes 524288 | tf_op jit(solution)/shard_map/all_to_all | solution.py:535
  52.6 47.6 %copy-start = (bf16[4,1024,256]{2,1,0:T(8,128)(2,1)S(1)}, bf16[4,1024,256]{2,1,0:T(8,128)(2,1)}, u32[]{:S(2)}) copy-start(bf16[4,1024,256]{2,1,0:T(8,128)(2,1)} %own.1) | copy-start | bytes 6291460
  52.6 49.2 %all-to-all-start.2 = ((bf16[8,528,128]{2,1,0:T(8,128)(2,1)}), bf16[8,528,128]{2,1,0:T(8,128)(2,1)S(1)}, u32[]{:S(2)}, u32[]{:S(2)}) async-start(bf16[8,528,128]{2,1,0:T(8,128)(2,1)} %gate_up.1), calls=%async_computation.2 | async-start | bytes 2162688 | tf_op jit(solution)/shard_map/all_to_all | solution.py:541
  56.3 48.0 %copy-start.4 = (f32[4096]{0:T(1024)S(1)}, f32[4096]{0:T(1024)}, u32[]{:S(2)}) copy-start(f32[4096]{0:T(1024)} %param.28) | copy-start | bytes 49156
  56.3 31.2 %collective-permute-start.2 = (bf16[1,64,256]{2,1,0:T(8,128)(2,1)S(1)}, bf16[1,64,256]{2,1,0:T(8,128)(2,1)S(1)}, u32[]{:S(2)}, u32[]{:S(2)}) collective-permute-start(bf16[1,64,256]{2,1,0:T(8,128)(2,1)S(1)} %bitcast.37), channel_id=1, source_target_pairs={{0,8},{2,10},{4,12},{6,14},{8,0},{10,2},{12,4},{14,6},{1,9},{3,11}... | collective-permute-start | bytes 98312 | tf_op jit(solution)/shard_map/ppermute | solution.py:24
  87.5 3.2 %collective-permute-start.4 = (bf16[2,64,256]{2,1,0:T(8,128)(2,1)S(1)}, bf16[2,64,256]{2,1,0:T(8,128)(2,1)S(1)}, u32[]{:S(2)}, u32[]{:S(2)}) collective-permute-start(bf16[2,64,256]{2,1,0:T(8,128)(2,1)S(1)} %pad_maximum_fusion.1), channel_id=1, source_target_pairs={{0,2},{2,0},{4,6},{6,4},{8,10},{10,8},{12,14},{14,12},{1,3},{3,1},... | collective-permute-start | bytes 196616 | tf_op jit(solution)/shard_map/ppermute | solution.py:24
  90.8 8.0 %collective-permute-start.6 = (bf16[4,64,256]{2,1,0:T(8,128)(2,1)S(1)}, bf16[4,64,256]{2,1,0:T(8,128)(2,1)S(1)}, u32[]{:S(2)}, u32[]{:S(2)}) collective-permute-start(bf16[4,64,256]{2,1,0:T(8,128)(2,1)S(1)} %pad_maximum_fusion), channel_id=1, source_target_pairs={{0,4},{2,6},{4,0},{6,2},{8,12},{10,14},{12,8},{14,10},{1,5},{3,7},... | collective-permute-start | bytes 393224 | tf_op jit(solution)/shard_map/ppermute | solution.py:24
  90.9 13.4 %collective-permute-start.5 = (bf16[2,64,256]{2,1,0:T(8,128)(2,1)S(1)}, bf16[2,64,256]{2,1,0:T(8,128)(2,1)S(1)}, u32[]{:S(2)}, u32[]{:S(2)}) collective-permute-start(bf16[2,64,256]{2,1,0:T(8,128)(2,1)S(1)} %collective-permute-done.4.refs_4_), channel_id=1, source_target_pairs={{0,1},{1,0},{2,3},{3,2},{4,5},{5,4},{6,7},{7,6},{8,9},{9,8},{10,11... | collective-permute-start | bytes 196616 | tf_op jit(solution)/shard_map/ppermute | solution.py:20
  98.7 5.6 %collective-permute-start.7 = (bf16[4,64,256]{2,1,0:T(8,128)(2,1)S(1)}, bf16[4,64,256]{2,1,0:T(8,128)(2,1)}, u32[]{:S(2)}, u32[]{:S(2)}) collective-permute-start(bf16[4,64,256]{2,1,0:T(8,128)(2,1)S(1)} %collective-permute-done.6.refs_6_), channel_id=1, source_target_pairs={{0,1},{1,0},{2,3},{3,2},{4,5},{5,4},{6,7},{7,6},{8,9},{9,8},{10,11... | collective-permute-start | bytes 393224 | tf_op jit(solution)/shard_map/ppermute | solution.py:20
  101.3 36.5 %collective-permute-start.14 = (bf16[2,1024,256]{2,1,0:T(8,128)(2,1)}, bf16[2,1024,256]{2,1,0:T(8,128)(2,1)}, u32[]{:S(2)}, u32[]{:S(2)}) collective-permute-start(bf16[2,1024,256]{2,1,0:T(8,128)(2,1)} %constant_dynamic-slice_fusion), channel_id=1, source_target_pairs={{0,1},{1,0},{2,3},{3,2},{4,5},{5,4},{6,7},{7,6},{8,9},{9,8},{10,11... | collective-permute-start | bytes 3145736 | tf_op jit(solution)/shard_map/ppermute | solution.py:20
  101.3 3.0 %collective-permute-start.3 = (bf16[1,64,256]{2,1,0:T(8,128)(2,1)S(1)}, bf16[1,64,256]{2,1,0:T(8,128)(2,1)}, u32[]{:S(2)}, u32[]{:S(2)}) collective-permute-start(bf16[1,64,256]{2,1,0:T(8,128)(2,1)S(1)} %collective-permute-done.2.refs_2_), channel_id=1, source_target_pairs={{0,1},{1,0},{2,3},{3,2},{4,5},{5,4},{6,7},{7,6},{8,9},{9,8},{10,11... | collective-permute-start | bytes 98312 | tf_op jit(solution)/shard_map/ppermute | solution.py:20
  110.5 3.7 %collective-permute-start.10 = (bf16[8,64,256]{2,1,0:T(8,128)(2,1)}, bf16[8,64,256]{2,1,0:T(8,128)(2,1)S(1)}, u32[]{:S(2)}, u32[]{:S(2)}) collective-permute-start(bf16[8,64,256]{2,1,0:T(8,128)(2,1)} %get-tuple-element.14), channel_id=1, source_target_pairs={{0,1},{1,0},{2,3},{3,2},{4,5},{5,4},{6,7},{7,6},{8,9},{9,8},{10,11... | collective-permute-start | bytes 786440 | tf_op jit(solution)/shard_map/ppermute | solution.py:20
  110.6 27.2 %all-to-all-start.3 = ((bf16[8,256,128]{2,1,0:T(8,128)(2,1)}), bf16[8,256,128]{2,1,0:T(8,128)(2,1)S(1)}, u32[]{:S(2)}, u32[]{:S(2)}) async-start(bf16[8,256,128]{2,1,0:T(8,128)(2,1)} %inner.1.refs_12_), calls=%async_computation.3 | async-start | bytes 1048576 | tf_op jit(solution)/shard_map/all_to_all | solution.py:543
  114.3 23.4 %collective-permute-start.11 = (bf16[4,64,256]{2,1,0:T(8,128)(2,1)S(1)}, bf16[4,64,256]{2,1,0:T(8,128)(2,1)S(1)}, u32[]{:S(2)}, u32[]{:S(2)}) collective-permute-start(bf16[4,64,256]{2,1,0:T(8,128)(2,1)S(1)} %slice.57), channel_id=1, source_target_pairs={{0,8},{2,10},{4,12},{6,14},{8,0},{10,2},{12,4},{14,6},{1,9},{3,11}... | collective-permute-start | bytes 393224 | tf_op jit(solution)/shard_map/ppermute | solution.py:24
  137.7 7.1 %collective-permute-start.12 = (bf16[2,64,256]{2,1,0:T(8,128)(2,1)S(1)}, bf16[2,64,256]{2,1,0:T(8,128)(2,1)S(1)}, u32[]{:S(2)}, u32[]{:S(2)}) collective-permute-start(bf16[2,64,256]{2,1,0:T(8,128)(2,1)S(1)} %slice.58), channel_id=1, source_target_pairs={{0,4},{2,6},{4,0},{6,2},{8,12},{10,14},{12,8},{14,10},{1,5},{3,7},... | collective-permute-start | bytes 196616 | tf_op jit(solution)/shard_map/ppermute | solution.py:24
  141.1 11.3 %all-to-all-start.4 = ((bf16[16,2,16,256]{3,2,1,0:T(8,128)(2,1)}), bf16[16,2,16,256]{3,2,1,0:T(8,128)(2,1)S(1)}, u32[]{:S(2)}, u32[]{:S(2)}) async-start(bf16[16,2,16,256]{3,2,1,0:T(8,128)(2,1)} %down.1), calls=%async_computation.4 | async-start | bytes 524288 | tf_op jit(solution)/shard_map/all_to_all | solution.py:545
  144.8 9.7 %collective-permute-start.13 = (bf16[1,64,256]{2,1,0:T(8,128)(2,1)S(1)}, bf16[1,64,256]{2,1,0:T(8,128)(2,1)S(1)}, u32[]{:S(2)}, u32[]{:S(2)}) collective-permute-start(bf16[1,64,256]{2,1,0:T(8,128)(2,1)S(1)} %slice.59), channel_id=1, source_target_pairs={{0,2},{2,0},{4,6},{6,4},{8,10},{10,8},{12,14},{14,12},{1,3},{3,1},... | collective-permute-start | bytes 98312 | tf_op jit(solution)/shard_map/ppermute | solution.py:24
  152.7 2.7 %collective-permute-start.15 = (bf16[64,256]{1,0:T(8,128)(2,1)S(1)}, bf16[64,256]{1,0:T(8,128)(2,1)S(1)}, u32[]{:S(2)}, u32[]{:S(2)}) collective-permute-start(bf16[64,256]{1,0:T(8,128)(2,1)S(1)} %get-tuple-element.16), channel_id=1, source_target_pairs={{0,1},{1,0},{2,3},{3,2},{4,5},{5,4},{6,7},{7,6},{8,9},{9,8},{10,11... | collective-permute-start | bytes 98312 | tf_op jit(solution)/shard_map/ppermute | solution.py:20
  (15 other events, 134.9 us)
where the time goes:
time: 157 us; the launch traced here: 156 us
  waiting for transfers between devices  80.2 us (51%)
  starting transfers between devices  46.5 us (30%)
  Pallas kernels  16.3 us (10%)
  local copies, waits for them, and re-layouts  7.93 us (5%)
  other arithmetic  4.02 us (3%)
    ppermute x6, waiting for transfers between devices, exchanged(): lax.ppermute(x, axis, [(i, i ^ bit) for i in range(lax.axis_size(axis))])  52.9 us
    ppermute x10, starting transfers between devices, swapped(): return lax.ppermute(x, 'c', [(0, 1), (1, 0)])  11.3 us
    ppermute x6, starting transfers between devices, exchanged(): lax.ppermute(x, axis, [(i, i ^ bit) for i in range(lax.axis_size(axis))])  11.2 us
    all_to_all x1, waiting for transfers between devices, local(): lax.all_to_all(both, 'z', split_axis=0, concat_axis=0, tiled=True)  9.44 us
    all_to_all x1, waiting for transfers between devices, local(): lax.all_to_all(outgoing, 'ep', split_axis=0, concat_axis=0, tiled=True)  7.51 us
    all_to_all x1, waiting for transfers between devices, local(): lax.all_to_all(results, 'ep', split_axis=0, concat_axis=0, tiled=True)  7.5 us
    all_to_all x1, starting transfers between devices, local(): lax.all_to_all(outgoing, 'ep', split_axis=0, concat_axis=0, tiled=True)  6.76 us
    all_to_all x1, starting transfers between devices, local(): lax.all_to_all(both, 'z', split_axis=0, concat_axis=0, tiled=True)  6.49 us
  transfers between devices with their start and end apart: 21, of which 10 were waited for; matrix products, arithmetic and copies ran while one was open for 3% of the time, Pallas kernels for 5%

commit v1 on v0

--- a/solution.py
+++ b/solution.py
@@ -18,6 +18,11 @@
 
 def swapped(x):
     return lax.ppermute(x, "c", [(0, 1), (1, 0)])
+
+
+def moved(x, axis, steps):
+    count = lax.axis_size(axis)
+    return lax.ppermute(x, axis, [(i, (i + steps) % count) for i in range(count)])
 
 
 def exchanged(x, axis, bit):
@@ -154,8 +159,9 @@
 
 
 def gate_up_kernel(
-    at, arrived, gain, gate, gate_par, up, up_par, sent, incoming, weights, parcel, ins, outs
+    at, arrived, gain, gate, gate_par, up, up_par, *refs
 ):
+    *sent, near, far, incoming, weights, parcel, ins, outs = refs
     half, _, _, width, _ = weights.shape
     seq_devs, _, pair_slots, _ = incoming.shape
     z_count, _, lanes = parcel.shape
@@ -176,13 +182,15 @@
     first.wait()
     stores = []
 
-    def store(depth, size):
-        place = pl.ds(depth, size)
-        copy = pltpu.make_async_copy(
-            parcel.at[:, place, :], sent.at[:, place, :], outs.at[len(stores)]
-        )
+    def store(source, target):
+        copy = pltpu.make_async_copy(source, target, outs.at[len(stores)])
         copy.start()
         stores.append(copy)
+
+    def put(depth, size, block_of):
+        for chip in range(z_count):
+            steps = lax.rem(chip - at[3] + z_count, z_count)
+            parcel[steps, depth : depth + size, :] = block_of(chip)
 
     scaled = {}
     for e in range(half):
@@ -197,9 +205,7 @@
         line = lax.broadcasted_iota(jnp.int32, squares.shape, 0)
         both = jnp.where(line == 0, high.astype(F32), jnp.where(line == 1, low.astype(F32), 0.0))
         depth = 2 * half * rows + e * 8
-        for z in range(z_count):
-            parcel[z, depth : depth + 8, :] = both.astype(BF16)
-    store(2 * half * rows, half * 8)
+        put(depth, 8, lambda chip, both=both: both.astype(BF16))
     for e in range(half):
         for m in range(2):
             for part in range(2):
@@ -207,9 +213,14 @@
             sums = dot32(scaled[e, 0], weights[e, m, 0]) + dot32(scaled[e, 1], weights[e, m, 1])
             sums = sums.astype(BF16)
             depth = (half * m + e) * rows
-            for z in range(z_count):
-                parcel[z, depth : depth + rows, :] = sums[:, z * lanes : (z + 1) * lanes]
-            store(depth, rows)
+            put(depth, rows, lambda chip, sums=sums: sums[:, chip * lanes : (chip + 1) * lanes])
+    middle, split = z_count // 2, near.shape[0]
+    store(parcel.at[middle, pl.ds(0, split), :], near)
+    store(parcel.at[middle, pl.ds(split, far.shape[0]), :], far)
+    for steps in range(middle):
+        store(parcel.at[steps], sent[steps])
+    for steps in range(middle + 1, z_count):
+        store(parcel.at[steps], sent[steps - 1])
     for copy in stores:
         copy.wait()
 
@@ -225,14 +236,15 @@
     return pl.pallas_call(
         gate_up_kernel,
         in_specs=[smem, any_place, vmem, far, any_place, far, any_place],
-        out_specs=far,
-        out_shape=pltpu.HBM(parcel, BF16),
+        out_specs=(far,) * (z_count + 1),
+        out_shape=(pltpu.HBM(parcel[1:], BF16),) * (z_count - 1)
+        + (pltpu.HBM((parcel[1] // 2, parcel[2]), BF16),) * 2,
         scratch_shapes=[
             pltpu.VMEM(incoming.shape, BF16),
             pltpu.VMEM((half, 2, 2, width, units), BF16),
             pltpu.VMEM(parcel, BF16),
             pltpu.SemaphoreType.DMA((1 + 4 * half,)),
-            pltpu.SemaphoreType.DMA((1 + 2 * half,)),
+            pltpu.SemaphoreType.DMA((z_count + 1,)),
         ],
         compiler_params=pltpu.CompilerParams(vmem_limit_bytes=62 * 2**20),
         cost_estimate=cost(8 * pair_rows * width * units, 8 * half * width * units),
@@ -298,7 +310,7 @@
 
 
 def shared_kernel(at, pieces, gain, gate_t, up_t, down_t, kept, given):
-    c, z = at[0], at[1] // 2
+    c, z = at[0], at[3]
     seqs, width = kept.shape[1:]
     squares = jnp.zeros((seqs, 1), F32)
     gate = jnp.zeros((seqs, gate_t.shape[0]), F32)
@@ -360,14 +372,19 @@
     )(at, *flat, gain, gate_t, up_t, w_down, after)
 
 
-def inner_kernel(model_width, half, arrived, inner, parcels, arrival):
-    fetch(arrived, parcels, arrival)
-    totals = parcels[0].astype(F32)
-    z_count = parcels.shape[0]
-    for z in range(1, z_count):
-        totals = totals + parcels[z].astype(F32)
+def inner_kernel(model_width, half, *refs):
+    *arrived, inner, parcels, arrivals = refs
+    copies = [
+        pltpu.make_async_copy(source, parcels.at[i], arrivals.at[i])
+        for i, source in enumerate(arrived)
+    ]
+    for copy in copies:
+        copy.start()
+    for i, copy in enumerate(copies):
+        copy.wait()
+        totals = totals + parcels[i].astype(F32) if i > 0 else parcels[i].astype(F32)
     lanes = totals.shape[1]
-    pair_rows = inner.shape[1]
+    z_count, pair_rows, _ = inner.shape
     rows = pair_rows // half
     for e in range(half):
         line = 2 * pair_rows + 8 * e
@@ -381,19 +398,23 @@
             inner[z, e * rows : (e + 1) * rows, :] = done
 
 
-def inner_copies(parcels, model_width, half):
-    z_count, depth, lanes = parcels.shape
+def inner_copies(parcels, z_count, model_width, half):
+    depth, lanes = parcels[0].shape
     pair_rows = (depth - half * 8) // 2
+    count = len(parcels)
     return pl.pallas_call(
         functools.partial(inner_kernel, model_width, half),
         out_shape=jax.ShapeDtypeStruct((z_count, pair_rows, lanes), BF16),
-        in_specs=[pl.BlockSpec(memory_space=pl.ANY)],
+        in_specs=[pl.BlockSpec(memory_space=pl.ANY)] * count,
         out_specs=pl.BlockSpec(memory_space=pltpu.VMEM),
-        scratch_shapes=[pltpu.VMEM(parcels.shape, BF16), pltpu.SemaphoreType.DMA],
+        scratch_shapes=[
+            pltpu.VMEM((count, depth, lanes), BF16),
+            pltpu.SemaphoreType.DMA((count,)),
+        ],
         compiler_params=ROOM,
-        cost_estimate=cost(parcels.size * 4, parcels.size * 4),
+        cost_estimate=cost(depth * lanes * 32, depth * lanes * 32),
         name="inner",
-    )(parcels)
+    )(*parcels)
 
 
 def down_kernel(at, arrived, own, par, sent, inner, weights, results, ins, outs):
@@ -534,12 +555,26 @@
     outgoing = dispatch(spread, resid_own, resid_par, ep_count)
     incoming = lax.all_to_all(outgoing, "ep", split_axis=0, concat_axis=0, tiled=True)
 
-    at = jnp.array([1, 1, -1], jnp.int32) * c + jnp.array([0, 2, 2], jnp.int32) * z
-    at = at + jnp.array([0, 0, 1], jnp.int32)
+    at = jnp.array([1, 1, -1, 0], jnp.int32) * c + jnp.array([0, 2, 2, 1], jnp.int32) * z
+    at = at + jnp.array([0, 0, 1, 0], jnp.int32)
     gain = ffn_gain.reshape(1, -1)
-    parcel = gate_up(at, incoming, gain, expert_gate, gate_par, expert_up, up_par)
-    parcels = lax.all_to_all(parcel, "z", split_axis=0, concat_axis=0, tiled=True)
-    copies = inner_copies(parcels, model_width, half)
+    *sent, near, far = gate_up(at, incoming, gain, expert_gate, gate_par, expert_up, up_par)
+    middle = z_count // 2
+    chunks = dict(zip([k for k in range(z_count) if k != middle], sent, strict=True))
+    from_below = moved(near, "z", 1)
+    from_above = moved(far, "z", -1)
+    split = near.shape[0]
+    chunk = chunks[middle - 1]
+    chunk_low = (chunk[:split].astype(F32) + from_below.astype(F32)).astype(BF16)
+    chunks[middle - 1] = jnp.concatenate([chunk_low, chunk[split:]])
+    chunk = chunks[middle + 1]
+    chunk_high = (chunk[split:].astype(F32) + from_above.astype(F32)).astype(BF16)
+    chunks[middle + 1] = jnp.concatenate([chunk[:split], chunk_high])
+    parcels = [chunks[0]]
+    for steps in range(1, middle):
+        parcels.append(moved(chunks[steps], "z", steps))
+        parcels.append(moved(chunks[z_count - steps], "z", -steps))
+    copies = inner_copies(parcels, z_count, model_width, half)
     inner_all = lax.all_to_all(copies, "z", split_axis=0, concat_axis=0, tiled=True)
     results = down(at, inner_all, expert_down, down_par, ep_count, capacity)
     returned = lax.all_to_all(results, "ep", split_axis=0, concat_axis=0, tiled=True)

time: 157 us -> 141 us (0.90)
  waiting for transfers between devices: 80.2 us -> 52.9 us
  starting transfers between devices: 46.5 us -> 55.6 us
  other arithmetic: 4.02 us -> 6.78 us
    ppermute x6, waiting for transfers between devices: 52.9 us -> 21.3 us  [exchanged(): lax.ppermute(x, axis, [(i, i ^ bit) for i in range(lax.axis_size(axis))])]
    ppermute x0 -> x8, starting transfers between devices: none -> 8.5 us  [moved(): lax.ppermute(x, axis, [(i, (i + steps) % count) for i in range(count)])]
    ppermute x10, starting transfers between devices: 11.3 us -> 19.7 us  [swapped(): return lax.ppermute(x, 'c', [(0, 1), (1, 0)])]
    ppermute x0 -> x8, waiting for transfers between devices: none -> 8.24 us  [moved(): lax.ppermute(x, axis, [(i, (i + steps) % count) for i in range(count)])]
    unnamed x37 -> x31, local copies, waits for them, and re-layouts: 6.01 us -> 0.86 us
    ppermute x6, starting transfers between devices: 11.2 us -> 7.15 us  [exchanged(): lax.ppermute(x, axis, [(i, i ^ bit) for i in range(lax.axis_size(axis))])]
    all_to_all x1 -> x0, starting transfers between devices: 3.7 us -> none  [local(): lax.all_to_all(parcel, 'z', split_axis=0, concat_axis=0, tiled=True)]
    dynamic_slice x3, local copies, waits for them, and re-layouts: 1.2 us -> 3.62 us  [of_pair(): return lax.dynamic_slice_in_dim(x, which * width, width, dim)]
  transfers between devices with their start and end apart: 21 -> 28, of which waited for: 10 -> 10; matrix products, arithmetic and copies ran while one was open for 3% -> 9% of each run, Pallas kernels for 5% -> 9%
where the time goes in v1:
time: 141 us; the launch traced here: 140 us
  starting transfers between devices  55.6 us (39%)
  waiting for transfers between devices  52.9 us (38%)
  Pallas kernels  16.9 us (12%)
  local copies, waits for them, and re-layouts  6.97 us (5%)
  other arithmetic  6.78 us (5%)
    ppermute x6, waiting for transfers between devices, exchanged(): lax.ppermute(x, axis, [(i, i ^ bit) for i in range(lax.axis_size(axis))])  21.3 us
    ppermute x10, starting transfers between devices, swapped(): return lax.ppermute(x, 'c', [(0, 1), (1, 0)])  19.7 us
    ppermute x8, starting transfers between devices, moved(): lax.ppermute(x, axis, [(i, (i + steps) % count) for i in range(count)])  8.5 us
    ppermute x8, waiting for transfers between devices, moved(): lax.ppermute(x, axis, [(i, (i + steps) % count) for i in range(count)])  8.24 us
    all_to_all x1, waiting for transfers between devices, local(): lax.all_to_all(results, 'ep', split_axis=0, concat_axis=0, tiled=True)  7.66 us
    all_to_all x1, waiting for transfers between devices, local(): lax.all_to_all(both, 'z', split_axis=0, concat_axis=0, tiled=True)  7.62 us
    ppermute x6, starting transfers between devices, exchanged(): lax.ppermute(x, axis, [(i, i ^ bit) for i in range(lax.axis_size(axis))])  7.15 us
    all_to_all x1, starting transfers between devices, local(): lax.all_to_all(outgoing, 'ep', split_axis=0, concat_axis=0, tiled=True)  6.75 us
  transfers between devices with their start and end apart: 28, of which 10 were waited for; matrix products, arithmetic and copies ran while one was open for 9% of the time, Pallas kernels for 9%

profile of v1, /device:TPU:1, one launch (start us, length us, event | category | flops | bytes accessed | tf_op | source)
XLA Modules:
  0.0 140.3 jit_solution(10088527709016669152)
XLA Ops:
  0.7 4.3 %front.1 = (f32[64,512]{1,0:T(8,128)}, f32[64,512]{1,0:T(8,128)}, f32[8,64,256]{2,1,0:T(8,128)}, bf16[8,64,256]{2,1,0:T(8,128)(2,1)}) custom-call(s32[1]{0:T(128)} %bitcast.core, f32[8]{0:T(128)} %log_step.1, bf16[64,4096]{1,0:T(8,128)(2,1)} %tokens.1, f32[1,4096]{1,0:T(1,128)} %bitcast.46, bf16[4096,128]{1,0:T(8,128)(2,1)} %w_in.1, f32[1,512]{1,0:T(1,128)} %bitcast.47, ...), custom_call_target="tpu_custom_call" | custom-call | flops 134217728 | bytes 2097152 | tf_op jit(solution)/shard_map/front/pallas_call | solution.py:146
  4.9 3.2 %collective-permute-start = (bf16[8,64,256]{2,1,0:T(8,128)(2,1)}, bf16[8,64,256]{2,1,0:T(8,128)(2,1)S(1)}, u32[]{:S(2)}, u32[]{:S(2)}) collective-permute-start(bf16[8,64,256]{2,1,0:T(8,128)(2,1)} %get-tuple-element.21), channel_id=1, source_target_pairs={{0,1},{1,0},{2,3},{3,2},{4,5},{5,4},{6,7},{7,6},{8,9},{9,8},{10,11... | collective-permute-start | bytes 786440 | tf_op jit(solution)/shard_map/ppermute | solution.py:20
  10.3 6.5 %all-to-all-start = ((bf16[8,64,256]{2,1,0:T(8,128)(2,1)}), bf16[8,64,256]{2,1,0:T(8,128)(2,1)S(1)}, u32[]{:S(2)}, u32[]{:S(2)}) async-start(bf16[8,64,256]{2,1,0:T(8,128)(2,1)} %add_convert_fusion), calls=%async_computation | async-start | bytes 524288 | tf_op jit(solution)/shard_map/all_to_all | solution.py:532
  20.2 7.6 %all-to-all-done = bf16[8,64,256]{2,1,0:T(8,128)(2,1)S(1)} async-done(((bf16[8,64,256]{2,1,0:T(8,128)(2,1)}), bf16[8,64,256]{2,1,0:T(8,128)(2,1)S(1)}, u32[]{:S(2)}, u32[]{:S(2)}) %all-to-all-start) | async-done | bytes 262176 | tf_op jit(solution)/shard_map/all_to_all | solution.py:532
  29.4 1.7 %collective-permute-start.1 = (bf16[64,256]{1,0:T(8,128)(2,1)S(1)}, bf16[64,256]{1,0:T(8,128)(2,1)S(1)}, u32[]{:S(2)}, u32[]{:S(2)}) collective-permute-start(bf16[64,256]{1,0:T(8,128)(2,1)S(1)} %add_convert_fusion.3.own_in), channel_id=1, source_target_pairs={{0,1},{1,0},{2,3},{3,2},{4,5},{5,4},{6,7},{7,6},{8,9},{9,8},{10,11... | collective-permute-start | bytes 98312 | tf_op jit(solution)/shard_map/ppermute | solution.py:20
  31.1 4.2 %collective-permute-done.2.refs_2_ = bf16[1,64,256]{2,1,0:T(8,128)(2,1)S(1)} collective-permute-done((bf16[1,64,256]{2,1,0:T(8,128)(2,1)S(1)}, bf16[1,64,256]{2,1,0:T(8,128)(2,1)S(1)}, u32[]{:S(2)}, u32[]{:S(2)}) %collective-permute-start.2) | collective-permute-done | bytes 32800 | tf_op jit(solution)/shard_map/ppermute | solution.py:29
  36.7 6.8 %all-to-all-start.1 = ((bf16[16,2,16,256]{3,2,1,0:T(8,128)(2,1)}), bf16[16,2,16,256]{3,2,1,0:T(8,128)(2,1)S(1)}, u32[]{:S(2)}, u32[]{:S(2)}) async-start(bf16[16,2,16,256]{3,2,1,0:T(8,128)(2,1)} %dispatch.1), calls=%async_computation.1 | async-start | bytes 524288 | tf_op jit(solution)/shard_map/all_to_all | solution.py:556
  45.0 6.0 %all-to-all-done.1.arrived = bf16[16,2,16,256]{3,2,1,0:T(8,128)(2,1)S(1)} async-done(((bf16[16,2,16,256]{3,2,1,0:T(8,128)(2,1)}), bf16[16,2,16,256]{3,2,1,0:T(8,128)(2,1)S(1)}, u32[]{:S(2)}, u32[]{:S(2)}) %all-to-all-start.1) | async-done | bytes 262176 | tf_op jit(solution)/shard_map/all_to_all | solution.py:556
  51.7 4.5 %gate_up.1 = (bf16[528,128]{1,0:T(8,128)(2,1)}, bf16[528,128]{1,0:T(8,128)(2,1)}, bf16[528,128]{1,0:T(8,128)(2,1)}, bf16[528,128]{1,0:T(8,128)(2,1)}, bf16[528,1...) custom-call(s32[4]{0:T(128)} %add_add_fusion.at, ...), custom_call_target="tpu_custom_call" | custom-call | flops 536870912 | bytes 4194304 | tf_op jit(solution)/shard_map/gate_up/pallas_call | solution.py:236
  57.6 4.0 %collective-permute-start.5 = (bf16[2,64,256]{2,1,0:T(8,128)(2,1)S(1)}, bf16[2,64,256]{2,1,0:T(8,128)(2,1)S(1)}, u32[]{:S(2)}, u32[]{:S(2)}) collective-permute-start(bf16[2,64,256]{2,1,0:T(8,128)(2,1)S(1)} %collective-permute-done.4.refs_4_), channel_id=1, source_target_pairs={{0,1},{1,0},{2,3},{3,2},{4,5},{5,4},{6,7},{7,6},{8,9},{9,8},{10,11... | collective-permute-start | bytes 196616 | tf_op jit(solution)/shard_map/ppermute | solution.py:20
  70.5 2.7 %collective-permute-start.13 = (bf16[528,128]{1,0:T(8,128)(2,1)}, bf16[528,128]{1,0:T(8,128)(2,1)S(1)}, u32[]{:S(2)}, u32[]{:S(2)}) collective-permute-start(bf16[528,128]{1,0:T(8,128)(2,1)} %get-tuple-element.26), channel_id=1, source_target_pairs={{0,12},{2,14},{4,0},{6,2},{8,4},{10,6},{12,8},{14,10},{1,13},{3,15... | collective-permute-start | bytes 405512 | tf_op jit(solution)/shard_map/ppermute | solution.py:25
  73.3 4.9 %collective-permute-done.12.refs_3_ = bf16[528,128]{1,0:T(8,128)(2,1)S(1)} collective-permute-done((bf16[528,128]{1,0:T(8,128)(2,1)}, bf16[528,128]{1,0:T(8,128)(2,1)S(1)}, u32[]{:S(2)}, u32[]{:S(2)}) %collective-permute-start.12) | collective-permute-done | bytes 135200 | tf_op jit(solution)/shard_map/ppermute | solution.py:25
  78.2 2.2 %constant_dynamic-slice_fusion = bf16[2,1024,256]{2,1,0:T(8,128)(2,1)} fusion(bf16[4,1024,256]{2,1,0:T(8,128)(2,1)} %own.1, s32[]{:T(128)S(6)} %select_n.71), kind=kLoop, calls=%fused_computation.56 | loop fusion | bytes 2097156 | tf_op jit(solution)/shard_map/dynamic_slice | solution.py:34
  80.5 4.0 %collective-permute-start.22 = (bf16[2,1024,256]{2,1,0:T(8,128)(2,1)}, bf16[2,1024,256]{2,1,0:T(8,128)(2,1)}, u32[]{:S(2)}, u32[]{:S(2)}) collective-permute-start(bf16[2,1024,256]{2,1,0:T(8,128)(2,1)} %constant_dynamic-slice_fusion), channel_id=1, source_target_pairs={{0,1},{1,0},{2,3},{3,2},{4,5},{5,4},{6,7},{7,6},{8,9},{9,8},{10,11... | collective-permute-start | bytes 3145736 | tf_op jit(solution)/shard_map/ppermute | solution.py:20
  84.5 2.4 %collective-permute-done.17.refs_6_ = bf16[528,128]{1,0:T(8,128)(2,1)S(1)} collective-permute-done((bf16[528,128]{1,0:T(8,128)(2,1)S(1)}, bf16[528,128]{1,0:T(8,128)(2,1)S(1)}, u32[]{:S(2)}, u32[]{:S(2)}) %collective-permute-start.17) | collective-permute-done | bytes 135200 | tf_op jit(solution)/shard_map/ppermute | solution.py:25
  88.0 2.4 %inner.1.refs_12_ = bf16[8,256,128]{2,1,0:T(8,128)(2,1)} custom-call(bf16[528,128]{1,0:T(8,128)(2,1)S(1)} %copy-done.4, bf16[528,128]{1,0:T(8,128)(2,1)S(1)} %collective-permute-done.10.refs_1_, bf16[528,128]{1,0:T(8,128)(2,1)S(1)} %collective-permute-done.11.refs_2_, bf16[528,128]{1,0:T(8,128)(2,1)S(1)} %collective-permute-done.12.refs_3_, ...), custom_call_target="tpu_custom_call" | custom-call | flops 2162688 | bytes 2162688 | tf_op jit(solution)/shard_map/inner/pallas_call | solution.py:405
  91.8 3.1 %collective-permute-start.18 = (bf16[8,64,256]{2,1,0:T(8,128)(2,1)S(1)}, bf16[8,64,256]{2,1,0:T(8,128)(2,1)}, u32[]{:S(2)}, u32[]{:S(2)}) collective-permute-start(bf16[8,64,256]{2,1,0:T(8,128)(2,1)S(1)} %get-tuple-element.32), channel_id=1, source_target_pairs={{0,1},{1,0},{2,3},{3,2},{4,5},{5,4},{6,7},{7,6},{8,9},{9,8},{10,11... | collective-permute-start | bytes 786440 | tf_op jit(solution)/shard_map/ppermute | solution.py:20
  94.9 3.5 %all-to-all-start.2 = ((bf16[8,256,128]{2,1,0:T(8,128)(2,1)}), bf16[8,256,128]{2,1,0:T(8,128)(2,1)S(1)}, u32[]{:S(2)}, u32[]{:S(2)}) async-start(bf16[8,256,128]{2,1,0:T(8,128)(2,1)} %inner.1.refs_12_), calls=%async_computation.2 | async-start | bytes 1048576 | tf_op jit(solution)/shard_map/all_to_all | solution.py:578
  99.5 5.4 %collective-permute-start.19 = (bf16[4,64,256]{2,1,0:T(8,128)(2,1)S(1)}, bf16[4,64,256]{2,1,0:T(8,128)(2,1)S(1)}, u32[]{:S(2)}, u32[]{:S(2)}) collective-permute-start(bf16[4,64,256]{2,1,0:T(8,128)(2,1)S(1)} %slice.75), channel_id=1, source_target_pairs={{0,8},{2,10},{4,12},{6,14},{8,0},{10,2},{12,4},{14,6},{1,9},{3,11}... | collective-permute-start | bytes 393224 | tf_op jit(solution)/shard_map/ppermute | solution.py:29
  104.9 17.0 %collective-permute-done.19 = bf16[4,64,256]{2,1,0:T(8,128)(2,1)S(1)} collective-permute-done((bf16[4,64,256]{2,1,0:T(8,128)(2,1)S(1)}, bf16[4,64,256]{2,1,0:T(8,128)(2,1)S(1)}, u32[]{:S(2)}, u32[]{:S(2)}) %collective-permute-start.19) | collective-permute-done | bytes 131104 | tf_op jit(solution)/shard_map/ppermute | solution.py:29
  122.1 3.2 %down.1 = bf16[16,2,16,256]{3,2,1,0:T(8,128)(2,1)} custom-call(s32[4]{0:T(128)S(1)} %copy-done.6, bf16[8,256,128]{2,1,0:T(8,128)(2,1)S(1)} %all-to-all-done.2.arrived, bf16[4,1024,256]{2,1,0:T(8,128)(2,1)S(1)} %copy-done, bf16[2,1024,256]{2,1,0:T(8,128)(2,1)} %collective-permute-done.22.par), custom_call_target="tpu_custom_call" | custom-call | flops 268435456 | bytes 2097152 | tf_op jit(solution)/shard_map/down/pallas_call | solution.py:458
  125.3 3.5 %all-to-all-start.3 = ((bf16[16,2,16,256]{3,2,1,0:T(8,128)(2,1)}), bf16[16,2,16,256]{3,2,1,0:T(8,128)(2,1)S(1)}, u32[]{:S(2)}, u32[]{:S(2)}) async-start(bf16[16,2,16,256]{3,2,1,0:T(8,128)(2,1)} %down.1), calls=%async_computation.3 | async-start | bytes 524288 | tf_op jit(solution)/shard_map/all_to_all | solution.py:580
  129.2 7.7 %all-to-all-done.3.arrived = bf16[16,2,16,256]{3,2,1,0:T(8,128)(2,1)S(1)} async-done(((bf16[16,2,16,256]{3,2,1,0:T(8,128)(2,1)}), bf16[16,2,16,256]{3,2,1,0:T(8,128)(2,1)S(1)}, u32[]{:S(2)}, u32[]{:S(2)}) %all-to-all-start.3) | async-done | bytes 262176 | tf_op jit(solution)/shard_map/all_to_all | solution.py:580
  137.1 1.7 %collective-permute-start.23 = (bf16[64,256]{1,0:T(8,128)(2,1)S(1)}, bf16[64,256]{1,0:T(8,128)(2,1)S(1)}, u32[]{:S(2)}, u32[]{:S(2)}) collective-permute-start(bf16[64,256]{1,0:T(8,128)(2,1)S(1)} %get-tuple-element.34), channel_id=1, source_target_pairs={{0,1},{1,0},{2,3},{3,2},{4,5},{5,4},{6,7},{7,6},{8,9},{9,8},{10,11... | collective-permute-start | bytes 98312 | tf_op jit(solution)/shard_map/ppermute | solution.py:20
  (108 shorter events, 26.5 us)
Async XLA Ops:
  8.2 42.8 %collective-permute-start.8 = (bf16[2,256,1024]{2,1,0:T(8,128)(2,1)S(1)}, bf16[2,256,1024]{2,1,0:T(8,128)(2,1)}, u32[]{:S(2)}, u32[]{:S(2)}) collective-permute-start(bf16[2,256,1024]{2,1,0:T(8,128)(2,1)S(1)} %constant_dynamic-slice_fusion.2), channel_id=1, source_target_pairs={{0,1},{1,0},{2,3},{3,2},{4,5},{5,4},{6,7},{7,6},{8,9},{9,8},{10,11... | collective-permute-start | bytes 3145736 | tf_op jit(solution)/shard_map/ppermute | solution.py:20
  10.3 17.6 %all-to-all-start = ((bf16[8,64,256]{2,1,0:T(8,128)(2,1)}), bf16[8,64,256]{2,1,0:T(8,128)(2,1)S(1)}, u32[]{:S(2)}, u32[]{:S(2)}) async-start(bf16[8,64,256]{2,1,0:T(8,128)(2,1)} %add_convert_fusion), calls=%async_computation | async-start | bytes 524288 | tf_op jit(solution)/shard_map/all_to_all | solution.py:532
  18.1 33.0 %collective-permute-start.9 = (bf16[2,256,1024]{2,1,0:T(8,128)(2,1)S(1)}, bf16[2,256,1024]{2,1,0:T(8,128)(2,1)}, u32[]{:S(2)}, u32[]{:S(2)}) collective-permute-start(bf16[2,256,1024]{2,1,0:T(8,128)(2,1)S(1)} %constant_dynamic-slice_fusion.1), channel_id=1, source_target_pairs={{0,1},{1,0},{2,3},{3,2},{4,5},{5,4},{6,7},{7,6},{8,9},{9,8},{10,11... | collective-permute-start | bytes 3145736 | tf_op jit(solution)/shard_map/ppermute | solution.py:20
  28.7 6.7 %collective-permute-start.2 = (bf16[1,64,256]{2,1,0:T(8,128)(2,1)S(1)}, bf16[1,64,256]{2,1,0:T(8,128)(2,1)S(1)}, u32[]{:S(2)}, u32[]{:S(2)}) collective-permute-start(bf16[1,64,256]{2,1,0:T(8,128)(2,1)S(1)} %bitcast.37), channel_id=1, source_target_pairs={{0,8},{2,10},{4,12},{6,14},{8,0},{10,2},{12,4},{14,6},{1,9},{3,11}... | collective-permute-start | bytes 98312 | tf_op jit(solution)/shard_map/ppermute | solution.py:29
  29.4 6.3 %collective-permute-start.1 = (bf16[64,256]{1,0:T(8,128)(2,1)S(1)}, bf16[64,256]{1,0:T(8,128)(2,1)S(1)}, u32[]{:S(2)}, u32[]{:S(2)}) collective-permute-start(bf16[64,256]{1,0:T(8,128)(2,1)S(1)} %add_convert_fusion.3.own_in), channel_id=1, source_target_pairs={{0,1},{1,0},{2,3},{3,2},{4,5},{5,4},{6,7},{7,6},{8,9},{9,8},{10,11... | collective-permute-start | bytes 98312 | tf_op jit(solution)/shard_map/ppermute | solution.py:20
  35.4 8.1 %collective-permute-start.4 = (bf16[2,64,256]{2,1,0:T(8,128)(2,1)S(1)}, bf16[2,64,256]{2,1,0:T(8,128)(2,1)S(1)}, u32[]{:S(2)}, u32[]{:S(2)}) collective-permute-start(bf16[2,64,256]{2,1,0:T(8,128)(2,1)S(1)} %pad_maximum_fusion.3), channel_id=1, source_target_pairs={{0,2},{2,0},{4,6},{6,4},{8,10},{10,8},{12,14},{14,12},{1,3},{3,1},... | collective-permute-start | bytes 196616 | tf_op jit(solution)/shard_map/ppermute | solution.py:29
  36.7 14.3 %all-to-all-start.1 = ((bf16[16,2,16,256]{3,2,1,0:T(8,128)(2,1)}), bf16[16,2,16,256]{3,2,1,0:T(8,128)(2,1)S(1)}, u32[]{:S(2)}, u32[]{:S(2)}) async-start(bf16[16,2,16,256]{3,2,1,0:T(8,128)(2,1)} %dispatch.1), calls=%async_computation.1 | async-start | bytes 524288 | tf_op jit(solution)/shard_map/all_to_all | solution.py:556
  43.5 18.0 %collective-permute-start.6 = (bf16[4,64,256]{2,1,0:T(8,128)(2,1)S(1)}, bf16[4,64,256]{2,1,0:T(8,128)(2,1)S(1)}, u32[]{:S(2)}, u32[]{:S(2)}) collective-permute-start(bf16[4,64,256]{2,1,0:T(8,128)(2,1)S(1)} %pad_maximum_fusion.2), channel_id=1, source_target_pairs={{0,4},{2,6},{4,0},{6,2},{8,12},{10,14},{12,8},{14,10},{1,5},{3,7},... | collective-permute-start | bytes 393224 | tf_op jit(solution)/shard_map/ppermute | solution.py:29
  56.2 9.8 %collective-permute-start.16 = (bf16[264,128]{1,0:T(8,128)(2,1)}, bf16[264,128]{1,0:T(8,128)(2,1)S(1)}, u32[]{:S(2)}, u32[]{:S(2)}) collective-permute-start(bf16[264,128]{1,0:T(8,128)(2,1)} %get-tuple-element.30), channel_id=1, source_target_pairs={{0,14},{2,0},{4,2},{6,4},{8,6},{10,8},{12,10},{14,12},{1,15},{3,1}... | collective-permute-start | bytes 202760 | tf_op jit(solution)/shard_map/ppermute | solution.py:25
  57.6 32.9 %collective-permute-start.5 = (bf16[2,64,256]{2,1,0:T(8,128)(2,1)S(1)}, bf16[2,64,256]{2,1,0:T(8,128)(2,1)S(1)}, u32[]{:S(2)}, u32[]{:S(2)}) collective-permute-start(bf16[2,64,256]{2,1,0:T(8,128)(2,1)S(1)} %collective-permute-done.4.refs_4_), channel_id=1, source_target_pairs={{0,1},{1,0},{2,3},{3,2},{4,5},{5,4},{6,7},{7,6},{8,9},{9,8},{10,11... | collective-permute-start | bytes 196616 | tf_op jit(solution)/shard_map/ppermute | solution.py:20
  61.5 28.9 %collective-permute-start.7 = (bf16[4,64,256]{2,1,0:T(8,128)(2,1)S(1)}, bf16[4,64,256]{2,1,0:T(8,128)(2,1)S(1)}, u32[]{:S(2)}, u32[]{:S(2)}) collective-permute-start(bf16[4,64,256]{2,1,0:T(8,128)(2,1)S(1)} %collective-permute-done.6.refs_6_), channel_id=1, source_target_pairs={{0,1},{1,0},{2,3},{3,2},{4,5},{5,4},{6,7},{7,6},{8,9},{9,8},{10,11... | collective-permute-start | bytes 393224 | tf_op jit(solution)/shard_map/ppermute | solution.py:20
  62.4 5.9 %collective-permute-start.14 = (bf16[264,128]{1,0:T(8,128)(2,1)}, bf16[264,128]{1,0:T(8,128)(2,1)S(1)}, u32[]{:S(2)}, u32[]{:S(2)}) collective-permute-start(bf16[264,128]{1,0:T(8,128)(2,1)} %get-tuple-element.28), channel_id=1, source_target_pairs={{0,2},{2,4},{4,6},{6,8},{8,10},{10,12},{12,14},{14,0},{1,3},{3,5},... | collective-permute-start | bytes 202760 | tf_op jit(solution)/shard_map/ppermute | solution.py:25
  66.0 7.3 %collective-permute-start.11 = (bf16[528,128]{1,0:T(8,128)(2,1)}, bf16[528,128]{1,0:T(8,128)(2,1)S(1)}, u32[]{:S(2)}, u32[]{:S(2)}) collective-permute-start(bf16[528,128]{1,0:T(8,128)(2,1)} %get-tuple-element.24), channel_id=1, source_target_pairs={{0,14},{2,0},{4,2},{6,4},{8,6},{10,8},{12,10},{14,12},{1,15},{3,1}... | collective-permute-start | bytes 405512 | tf_op jit(solution)/shard_map/ppermute | solution.py:25
  68.4 9.9 %collective-permute-start.12 = (bf16[528,128]{1,0:T(8,128)(2,1)}, bf16[528,128]{1,0:T(8,128)(2,1)S(1)}, u32[]{:S(2)}, u32[]{:S(2)}) collective-permute-start(bf16[528,128]{1,0:T(8,128)(2,1)} %get-tuple-element.25), channel_id=1, source_target_pairs={{0,4},{2,6},{4,8},{6,10},{8,12},{10,14},{12,0},{14,2},{1,5},{3,7},... | collective-permute-start | bytes 405512 | tf_op jit(solution)/shard_map/ppermute | solution.py:25
  70.5 10.0 %collective-permute-start.13 = (bf16[528,128]{1,0:T(8,128)(2,1)}, bf16[528,128]{1,0:T(8,128)(2,1)S(1)}, u32[]{:S(2)}, u32[]{:S(2)}) collective-permute-start(bf16[528,128]{1,0:T(8,128)(2,1)} %get-tuple-element.26), channel_id=1, source_target_pairs={{0,12},{2,14},{4,0},{6,2},{8,4},{10,6},{12,8},{14,10},{1,13},{3,15... | collective-permute-start | bytes 405512 | tf_op jit(solution)/shard_map/ppermute | solution.py:25
  73.3 13.6 %collective-permute-start.17 = (bf16[528,128]{1,0:T(8,128)(2,1)S(1)}, bf16[528,128]{1,0:T(8,128)(2,1)S(1)}, u32[]{:S(2)}, u32[]{:S(2)}) collective-permute-start(bf16[528,128]{1,0:T(8,128)(2,1)S(1)} %pad_maximum_fusion.1), channel_id=1, source_target_pairs={{0,10},{2,12},{4,14},{6,0},{8,2},{10,4},{12,6},{14,8},{1,11},{3,13... | collective-permute-start | bytes 405512 | tf_op jit(solution)/shard_map/ppermute | solution.py:25
  78.2 9.8 %collective-permute-start.15 = (bf16[528,128]{1,0:T(8,128)(2,1)S(1)}, bf16[528,128]{1,0:T(8,128)(2,1)S(1)}, u32[]{:S(2)}, u32[]{:S(2)}) collective-permute-start(bf16[528,128]{1,0:T(8,128)(2,1)S(1)} %pad_maximum_fusion), channel_id=1, source_target_pairs={{0,6},{2,8},{4,10},{6,12},{8,14},{10,0},{12,2},{14,4},{1,7},{3,9},... | collective-permute-start | bytes 405512 | tf_op jit(solution)/shard_map/ppermute | solution.py:25
  80.5 41.6 %collective-permute-start.22 = (bf16[2,1024,256]{2,1,0:T(8,128)(2,1)}, bf16[2,1024,256]{2,1,0:T(8,128)(2,1)}, u32[]{:S(2)}, u32[]{:S(2)}) collective-permute-start(bf16[2,1024,256]{2,1,0:T(8,128)(2,1)} %constant_dynamic-slice_fusion), channel_id=1, source_target_pairs={{0,1},{1,0},{2,3},{3,2},{4,5},{5,4},{6,7},{7,6},{8,9},{9,8},{10,11... | collective-permute-start | bytes 3145736 | tf_op jit(solution)/shard_map/ppermute | solution.py:20
  91.8 6.6 %collective-permute-start.18 = (bf16[8,64,256]{2,1,0:T(8,128)(2,1)S(1)}, bf16[8,64,256]{2,1,0:T(8,128)(2,1)}, u32[]{:S(2)}, u32[]{:S(2)}) collective-permute-start(bf16[8,64,256]{2,1,0:T(8,128)(2,1)S(1)} %get-tuple-element.32), channel_id=1, source_target_pairs={{0,1},{1,0},{2,3},{3,2},{4,5},{5,4},{6,7},{7,6},{8,9},{9,8},{10,11... | collective-permute-start | bytes 786440 | tf_op jit(solution)/shard_map/ppermute | solution.py:20
  94.9 27.2 %all-to-all-start.2 = ((bf16[8,256,128]{2,1,0:T(8,128)(2,1)}), bf16[8,256,128]{2,1,0:T(8,128)(2,1)S(1)}, u32[]{:S(2)}, u32[]{:S(2)}) async-start(bf16[8,256,128]{2,1,0:T(8,128)(2,1)} %inner.1.refs_12_), calls=%async_computation.2 | async-start | bytes 1048576 | tf_op jit(solution)/shard_map/all_to_all | solution.py:578
  99.5 22.5 %collective-permute-start.19 = (bf16[4,64,256]{2,1,0:T(8,128)(2,1)S(1)}, bf16[4,64,256]{2,1,0:T(8,128)(2,1)S(1)}, u32[]{:S(2)}, u32[]{:S(2)}) collective-permute-start(bf16[4,64,256]{2,1,0:T(8,128)(2,1)S(1)} %slice.75), channel_id=1, source_target_pairs={{0,8},{2,10},{4,12},{6,14},{8,0},{10,2},{12,4},{14,6},{1,9},{3,11}... | collective-permute-start | bytes 393224 | tf_op jit(solution)/shard_map/ppermute | solution.py:29
  122.0 7.1 %collective-permute-start.20 = (bf16[2,64,256]{2,1,0:T(8,128)(2,1)S(1)}, bf16[2,64,256]{2,1,0:T(8,128)(2,1)S(1)}, u32[]{:S(2)}, u32[]{:S(2)}) collective-permute-start(bf16[2,64,256]{2,1,0:T(8,128)(2,1)S(1)} %slice.76), channel_id=1, source_target_pairs={{0,4},{2,6},{4,0},{6,2},{8,12},{10,14},{12,8},{14,10},{1,5},{3,7},... | collective-permute-start | bytes 196616 | tf_op jit(solution)/shard_map/ppermute | solution.py:29
  125.3 11.5 %all-to-all-start.3 = ((bf16[16,2,16,256]{3,2,1,0:T(8,128)(2,1)}), bf16[16,2,16,256]{3,2,1,0:T(8,128)(2,1)S(1)}, u32[]{:S(2)}, u32[]{:S(2)}) async-start(bf16[16,2,16,256]{3,2,1,0:T(8,128)(2,1)} %down.1), calls=%async_computation.3 | async-start | bytes 524288 | tf_op jit(solution)/shard_map/all_to_all | solution.py:580
  129.1 9.8 %collective-permute-start.21 = (bf16[1,64,256]{2,1,0:T(8,128)(2,1)S(1)}, bf16[1,64,256]{2,1,0:T(8,128)(2,1)S(1)}, u32[]{:S(2)}, u32[]{:S(2)}) collective-permute-start(bf16[1,64,256]{2,1,0:T(8,128)(2,1)S(1)} %slice.77), channel_id=1, source_target_pairs={{0,2},{2,0},{4,6},{6,4},{8,10},{10,8},{12,14},{14,12},{1,3},{3,1},... | collective-permute-start | bytes 98312 | tf_op jit(solution)/shard_map/ppermute | solution.py:29
  (19 other events, 294.3 us)

commit v2 on v1

--- a/solution.py
+++ b/solution.py
@@ -13,6 +13,7 @@
 ROUTED_SCALE = 2.5
 TP = ("z", "c")
 F32, BF16 = jnp.float32, jnp.bfloat16
+FULL = 53 * 2**20
 ROOM = pltpu.CompilerParams(vmem_limit_bytes=20 * 2**20)
 
 
@@ -29,9 +30,10 @@
     return lax.ppermute(x, axis, [(i, i ^ bit) for i in range(lax.axis_size(axis))])
 
 
-def of_pair(x, which, dim):
-    width = x.shape[dim] // 2
-    return lax.dynamic_slice_in_dim(x, which * width, width, dim)
+def added(x, part, first):
+    rest = x.shape[0] - first - part.shape[0]
+    part = lax.pad(part.astype(F32), jnp.zeros((), F32), ((first, rest, 0), (0, 0, 0)))
+    return (x.astype(F32) + part).astype(BF16)
 
 
 def rms_scale(values_in, gains):
@@ -148,7 +150,7 @@
         out_shape=(
             jax.ShapeDtypeStruct(state.shape, F32),
             jax.ShapeDtypeStruct(state.shape, F32),
-            jax.ShapeDtypeStruct(part, F32),
+            jax.ShapeDtypeStruct(part, BF16),
             jax.ShapeDtypeStruct(part, BF16),
         ),
         in_specs=[smem, smem] + [vmem] * len(arrays),
@@ -172,7 +174,7 @@
     loads = {}
     for e in range(half):
         for m, (own, par) in enumerate(((gate, gate_par), (up, up_par))):
-            for part, source in enumerate((own.at[half * at[0] + e], par.at[e])):
+            for part, source in enumerate((own.at[half * at[0] + e], par.at[half * at[0] + e])):
                 arrival = ins.at[1 + 4 * e + 2 * m + part]
                 copy = pltpu.make_async_copy(source, weights.at[e, m, part], arrival)
                 copy.start()
@@ -227,7 +229,7 @@
 
 def gate_up(at, incoming, gain, gate, gate_par, up, up_par):
     seq_devs, _, pair_slots, width = incoming.shape
-    half, _, units = gate_par.shape
+    half, units = gate.shape[0] // 2, gate.shape[2]
     z_count = lax.axis_size("z")
     pair_rows = seq_devs * pair_slots
     parcel = (z_count, 2 * pair_rows + half * 8, units // z_count)
@@ -236,9 +238,9 @@
     return pl.pallas_call(
         gate_up_kernel,
         in_specs=[smem, any_place, vmem, far, any_place, far, any_place],
-        out_specs=(far,) * (z_count + 1),
-        out_shape=(pltpu.HBM(parcel[1:], BF16),) * (z_count - 1)
-        + (pltpu.HBM((parcel[1] // 2, parcel[2]), BF16),) * 2,
+        out_specs=(any_place,) * (z_count + 1),
+        out_shape=(jax.ShapeDtypeStruct(parcel[1:], BF16),) * (z_count - 1)
+        + (jax.ShapeDtypeStruct((parcel[1] // 2, parcel[2]), BF16),) * 2,
         scratch_shapes=[
             pltpu.VMEM(incoming.shape, BF16),
             pltpu.VMEM((half, 2, 2, width, units), BF16),
@@ -246,7 +248,7 @@
             pltpu.SemaphoreType.DMA((1 + 4 * half,)),
             pltpu.SemaphoreType.DMA((z_count + 1,)),
         ],
-        compiler_params=pltpu.CompilerParams(vmem_limit_bytes=62 * 2**20),
+        compiler_params=pltpu.CompilerParams(vmem_limit_bytes=52 * 2**20),
         cost_estimate=cost(8 * pair_rows * width * units, 8 * half * width * units),
         name="gate_up",
     )(at, incoming, gain, gate, gate_par, up, up_par)
@@ -309,7 +311,15 @@
     )(weights, returned)
 
 
-def shared_kernel(at, pieces, gain, gate_t, up_t, down_t, kept, given):
+def shared_kernel(at, pieces, gain, sources, kept, given, gate_t, up_t, down_t, arrivals):
+    copies = [
+        pltpu.make_async_copy(source, target, arrivals.at[i])
+        for i, (source, target) in enumerate(zip(sources, (gate_t, up_t, down_t), strict=True))
+    ]
+    for copy in copies:
+        copy.start()
+    for copy in copies:
+        copy.wait()
     c, z = at[0], at[3]
     seqs, width = kept.shape[1:]
     squares = jnp.zeros((seqs, 1), F32)
@@ -337,8 +347,7 @@
 
 
 def growing(chips):
-    far = chips // 2
-    return [far] + [1 << i for i in range(far.bit_length() - 1)]
+    return [1] + [chips >> i for i in range(1, chips.bit_length() - 1)]
 
 
 def grown_order(chips):
@@ -354,9 +363,9 @@
     (seqs, width), z_count = flat[0].shape[1:], sum(rows.shape[0] for rows in flat) // 2
 
     def kernel(at, *refs):
-        rows, rest = refs[: len(flat)], refs[len(flat) :]
+        rows, (gain, *rest) = refs[: len(flat)], refs[len(flat) :]
         paired = [(rows[i], rows[i + 1]) for i in range(0, len(flat), 2)]
-        shared_kernel(at, paired, *rest[:4], *rest[5:])
+        shared_kernel(at, paired, gain, rest[:3], *rest[4:])
 
     return pl.pallas_call(
         kernel,
@@ -364,9 +373,15 @@
             jax.ShapeDtypeStruct((z_count, seqs, width), F32),
             jax.ShapeDtypeStruct((z_count, seqs, width), BF16),
         ),
-        in_specs=[smem] + [vmem] * (len(flat) + 4) + [pl.BlockSpec(memory_space=pl.ANY)],
+        in_specs=[smem] + [vmem] * (len(flat) + 1) + [pl.BlockSpec(memory_space=pl.ANY)] * 4,
         out_specs=(vmem, vmem),
-        compiler_params=ROOM,
+        scratch_shapes=[
+            pltpu.VMEM(gate_t.shape, BF16),
+            pltpu.VMEM(up_t.shape, BF16),
+            pltpu.VMEM(w_down.shape, BF16),
+            pltpu.SemaphoreType.DMA((3,)),
+        ],
+        compiler_params=pltpu.CompilerParams(vmem_limit_bytes=FULL),
         cost_estimate=cost(seqs * 6 * w_down.size, 6 * w_down.size),
         name="shared",
     )(at, *flat, gain, gate_t, up_t, w_down, after)
@@ -380,9 +395,11 @@
     ]
     for copy in copies:
         copy.start()
-    for i, copy in enumerate(copies):
+    for copy in copies:
         copy.wait()
-        totals = totals + parcels[i].astype(F32) if i > 0 else parcels[i].astype(F32)
+    totals = parcels[0].astype(F32)
+    for i in range(1, len(copies)):
+        totals = totals + parcels[i].astype(F32)
     lanes = totals.shape[1]
     z_count, pair_rows, _ = inner.shape
     rows = pair_rows // half
@@ -423,7 +440,7 @@
     first.start()
     loads = []
     for e in range(half):
-        for part, source in enumerate((own.at[half * at[0] + e], par.at[e])):
+        for part, source in enumerate((own.at[half * at[0] + e], par.at[half * at[0] + e])):
             arrival = ins.at[1 + 2 * e + part]
             copy = pltpu.make_async_copy(source, weights.at[e, part], arrival)
             copy.start()
@@ -452,7 +469,7 @@
 
 
 def down(at, inner, w_down, w_par, seq_devs, capacity):
-    half, units, width = w_par.shape
+    half, units, width = w_par.shape[0] // 2, *w_par.shape[1:]
     results = (seq_devs, 2, half * capacity, width)
     smem, any_place = pl.BlockSpec(memory_space=pltpu.SMEM), pl.BlockSpec(memory_space=pl.ANY)
     return pl.pallas_call(
@@ -505,12 +522,6 @@
     slice_width = model_width // (2 * z_count)
     offset = (2 * z + c) * slice_width
 
-    partner = []
-    for w in (expert_gate, expert_up, expert_down):
-        cut = of_pair(w, 1 - c, 0)
-        partner.append(swapped(cut))
-    gate_par, up_par, down_par = partner
-
     new_real, new_imag, kept, given = front(
         core,
         log_step,
@@ -528,7 +539,11 @@
         state_imag,
         w_out,
     )
-    both = (kept + swapped(given).astype(F32)).astype(BF16)
+    got = swapped(given)
+    both = (kept.astype(F32) + got.astype(F32)).astype(BF16)
+
+    gate_par, up_par, down_par = (swapped(w) for w in (expert_gate, expert_up, expert_down))
+
     mixer_own = lax.all_to_all(both, "z", split_axis=0, concat_axis=0, tiled=True)
     mixer_own = mixer_own.astype(F32).sum(axis=0)
     own_tokens = lax.dynamic_slice_in_dim(tokens, offset, slice_width, 1)
@@ -563,13 +578,8 @@
     chunks = dict(zip([k for k in range(z_count) if k != middle], sent, strict=True))
     from_below = moved(near, "z", 1)
     from_above = moved(far, "z", -1)
-    split = near.shape[0]
-    chunk = chunks[middle - 1]
-    chunk_low = (chunk[:split].astype(F32) + from_below.astype(F32)).astype(BF16)
-    chunks[middle - 1] = jnp.concatenate([chunk_low, chunk[split:]])
-    chunk = chunks[middle + 1]
-    chunk_high = (chunk[split:].astype(F32) + from_above.astype(F32)).astype(BF16)
-    chunks[middle + 1] = jnp.concatenate([chunk[:split], chunk_high])
+    chunks[middle - 1] = added(chunks[middle - 1], from_below, 0)
+    chunks[middle + 1] = added(chunks[middle + 1], from_above, near.shape[0])
     parcels = [chunks[0]]
     for steps in range(1, middle):
         parcels.append(moved(chunks[steps], "z", steps))

time: 141 us -> 137 us (0.972)
  starting transfers between devices: 55.6 us -> 62.2 us
  local copies, waits for them, and re-layouts: 6.97 us -> 0.85 us
  waiting for transfers between devices: 52.9 us -> 47.6 us
  Pallas kernels: 16.9 us -> 18.9 us
    ppermute x8, waiting for transfers between devices: 8.24 us -> 0.37 us  [moved(): lax.ppermute(x, axis, [(i, (i + steps) % count) for i in range(count)])]
    dynamic_slice x3 -> x0, local copies, waits for them, and re-layouts: 3.62 us -> none  [of_pair(): return lax.dynamic_slice_in_dim(x, which * width, width, dim)]
    ppermute x10, starting transfers between devices: 19.7 us -> 22.9 us  [swapped(): return lax.ppermute(x, 'c', [(0, 1), (1, 0)])]
    all_to_all x1, waiting for transfers between devices: 7.62 us -> 9.9 us  [local(): lax.all_to_all(both, 'z', split_axis=0, concat_axis=0, tiled=True)]
    ppermute x6, waiting for transfers between devices: 21.3 us -> 19.1 us  [exchanged(): lax.ppermute(x, axis, [(i, i ^ bit) for i in range(lax.axis_size(axis))])]
    pallas_call x1, Pallas kernels: 1.28 us -> 3.44 us  [shared_parts(): pl.pallas_call(kernel, out_shape=(jax.ShapeDtypeStruct((z_count, seqs, wi...]
    ppermute x6, starting transfers between devices: 7.15 us -> 8.98 us  [exchanged(): lax.ppermute(x, axis, [(i, i ^ bit) for i in range(lax.axis_size(axis))])]
    slice x3 -> x1, local copies, waits for them, and re-layouts: 1.96 us -> 0.18 us  [the longest x1 0.89 us: local(): chunks[middle + 1] = jnp.concatenate([chunk[:split], chunk_high])]
  transfers between devices with their start and end apart: 28 -> 28, of which waited for: 10 -> 9; matrix products, arithmetic and copies ran while one was open for 9% -> 4% of each run, Pallas kernels for 9% -> 14%
where the time goes in v2:
time: 137 us; the launch traced here: 136 us
  starting transfers between devices  62.2 us (45%)
  waiting for transfers between devices  47.6 us (35%)
  Pallas kernels  18.9 us (14%)
  other arithmetic  5.48 us (4%)
    ppermute x10, starting transfers between devices, swapped(): return lax.ppermute(x, 'c', [(0, 1), (1, 0)])  22.9 us
    ppermute x6, waiting for transfers between devices, exchanged(): lax.ppermute(x, axis, [(i, i ^ bit) for i in range(lax.axis_size(axis))])  19.1 us
    all_to_all x1, waiting for transfers between devices, local(): lax.all_to_all(both, 'z', split_axis=0, concat_axis=0, tiled=True)  9.9 us
    ppermute x8, starting transfers between devices, moved(): lax.ppermute(x, axis, [(i, (i + steps) % count) for i in range(count)])  9.35 us
    ppermute x6, starting transfers between devices, exchanged(): lax.ppermute(x, axis, [(i, i ^ bit) for i in range(lax.axis_size(axis))])  8.98 us
    all_to_all x1, waiting for transfers between devices, local(): lax.all_to_all(results, 'ep', split_axis=0, concat_axis=0, tiled=True)  7.56 us
    all_to_all x1, waiting for transfers between devices, local(): lax.all_to_all(outgoing, 'ep', split_axis=0, concat_axis=0, tiled=True)  7.14 us
    all_to_all x1, starting transfers between devices, local(): lax.all_to_all(outgoing, 'ep', split_axis=0, concat_axis=0, tiled=True)  6.77 us
  transfers between devices with their start and end apart: 28, of which 9 were waited for; matrix products, arithmetic and copies ran while one was open for 4% of the time, Pallas kernels for 14%

profile of v2, /device:TPU:1, one launch (start us, length us, event | category | flops | bytes accessed | tf_op | source)
XLA Modules:
  0.0 136.0 jit_solution(13736975167008223082)
XLA Ops:
  0.7 3.3 %collective-permute-start.8 = (bf16[4,256,1024]{2,1,0:T(8,128)(2,1)}, bf16[4,256,1024]{2,1,0:T(8,128)(2,1)}, u32[]{:S(2)}, u32[]{:S(2)}) collective-permute-start(bf16[4,256,1024]{2,1,0:T(8,128)(2,1)} %gate.1), channel_id=1, source_target_pairs={{0,1},{1,0},{2,3},{3,2},{4,5},{5,4},{6,7},{7,6},{8,9},{9,8},{10,11... | collective-permute-start | bytes 6291464 | tf_op jit(solution)/shard_map/ppermute | solution.py:21
  4.0 4.0 %front.1 = (f32[64,512]{1,0:T(8,128)}, f32[64,512]{1,0:T(8,128)}, bf16[8,64,256]{2,1,0:T(8,128)(2,1)}, bf16[8,64,256]{2,1,0:T(8,128)(2,1)}) custom-call(s32[1]{0:T(128)} %bitcast.core, f32[8]{0:T(128)} %log_step.1, bf16[64,4096]{1,0:T(8,128)(2,1)} %tokens.1, f32[1,4096]{1,0:T(1,128)} %bitcast.46, bf16[4096,128]{1,0:T(8,128)(2,1)} %w_in.1, ...), custom_call_target="tpu_custom_call" | custom-call | flops 134217728 | bytes 2097152 | tf_op jit(solution)/shard_map/front/pallas_call | solution.py:148
  9.1 2.2 %collective-permute-done = bf16[8,64,256]{2,1,0:T(8,128)(2,1)S(1)} collective-permute-done((bf16[8,64,256]{2,1,0:T(8,128)(2,1)}, bf16[8,64,256]{2,1,0:T(8,128)(2,1)S(1)}, u32[]{:S(2)}, u32[]{:S(2)}) %collective-permute-start) | collective-permute-done | bytes 262176 | tf_op jit(solution)/shard_map/ppermute | solution.py:21
  11.3 1.7 %add_convert_fusion = bf16[8,64,256]{2,1,0:T(8,128)(2,1)} fusion(bf16[8,64,256]{2,1,0:T(8,128)(2,1)S(1)} %collective-permute-done, bf16[8,64,256]{2,1,0:T(8,128)(2,1)} %get-tuple-element.20), kind=kLoop, calls=%fused_computation.2 | loop fusion | flops 524288 | bytes 786432 | tf_op jit(solution)/shard_map/convert_element_type | solution.py:543
  13.0 6.5 %all-to-all-start = ((bf16[8,64,256]{2,1,0:T(8,128)(2,1)}), bf16[8,64,256]{2,1,0:T(8,128)(2,1)S(1)}, u32[]{:S(2)}, u32[]{:S(2)}) async-start(bf16[8,64,256]{2,1,0:T(8,128)(2,1)} %add_convert_fusion), calls=%async_computation | async-start | bytes 524288 | tf_op jit(solution)/shard_map/all_to_all | solution.py:547
  20.7 9.9 %all-to-all-done = bf16[8,64,256]{2,1,0:T(8,128)(2,1)S(1)} async-done(((bf16[8,64,256]{2,1,0:T(8,128)(2,1)}), bf16[8,64,256]{2,1,0:T(8,128)(2,1)S(1)}, u32[]{:S(2)}, u32[]{:S(2)}) %all-to-all-start) | async-done | bytes 262176 | tf_op jit(solution)/shard_map/all_to_all | solution.py:547
  31.4 1.7 %collective-permute-start.1 = (bf16[64,256]{1,0:T(8,128)(2,1)S(1)}, bf16[64,256]{1,0:T(8,128)(2,1)S(1)}, u32[]{:S(2)}, u32[]{:S(2)}) collective-permute-start(bf16[64,256]{1,0:T(8,128)(2,1)S(1)} %add_convert_fusion.3.own_in), channel_id=1, source_target_pairs={{0,1},{1,0},{2,3},{3,2},{4,5},{5,4},{6,7},{7,6},{8,9},{9,8},{10,11... | collective-permute-start | bytes 98312 | tf_op jit(solution)/shard_map/ppermute | solution.py:21
  35.0 6.8 %all-to-all-start.1 = ((bf16[16,2,16,256]{3,2,1,0:T(8,128)(2,1)}), bf16[16,2,16,256]{3,2,1,0:T(8,128)(2,1)S(1)}, u32[]{:S(2)}, u32[]{:S(2)}) async-start(bf16[16,2,16,256]{3,2,1,0:T(8,128)(2,1)} %dispatch.1), calls=%async_computation.1 | async-start | bytes 524288 | tf_op jit(solution)/shard_map/all_to_all | solution.py:571
  42.8 7.1 %all-to-all-done.1.arrived = bf16[16,2,16,256]{3,2,1,0:T(8,128)(2,1)S(1)} async-done(((bf16[16,2,16,256]{3,2,1,0:T(8,128)(2,1)}), bf16[16,2,16,256]{3,2,1,0:T(8,128)(2,1)S(1)}, u32[]{:S(2)}, u32[]{:S(2)}) %all-to-all-start.1) | async-done | bytes 262176 | tf_op jit(solution)/shard_map/all_to_all | solution.py:571
  49.9 4.7 %gate_up.1 = (bf16[528,128]{1,0:T(8,128)(2,1)S(1)}, bf16[528,128]{1,0:T(8,128)(2,1)S(1)}, bf16[528,128]{1,0:T(8,128)(2,1)S(1)}, bf16[528,128]{1,0:T(8,128)(2,1)S...) custom-call(s32[4]{0:T(128)S(1)} %add_add_fusion.at, ...), custom_call_target="tpu_custom_call" | custom-call | flops 536870912 | bytes 4194304 | tf_op jit(solution)/shard_map/gate_up/pallas_call | solution.py:238
  54.8 2.1 %collective-permute-start.6 = (bf16[4,64,256]{2,1,0:T(8,128)(2,1)S(1)}, bf16[4,64,256]{2,1,0:T(8,128)(2,1)S(1)}, u32[]{:S(2)}, u32[]{:S(2)}) collective-permute-start(bf16[4,64,256]{2,1,0:T(8,128)(2,1)S(1)} %pad_maximum_fusion), channel_id=1, source_target_pairs={{0,4},{2,6},{4,0},{6,2},{8,12},{10,14},{12,8},{14,10},{1,5},{3,7},... | collective-permute-start | bytes 393224 | tf_op jit(solution)/shard_map/ppermute | solution.py:30
  59.6 2.2 %collective-permute-done.6.refs_6_ = bf16[4,64,256]{2,1,0:T(8,128)(2,1)S(1)} collective-permute-done((bf16[4,64,256]{2,1,0:T(8,128)(2,1)S(1)}, bf16[4,64,256]{2,1,0:T(8,128)(2,1)S(1)}, u32[]{:S(2)}, u32[]{:S(2)}) %collective-permute-start.6) | collective-permute-done | bytes 131104 | tf_op jit(solution)/shard_map/ppermute | solution.py:30
  61.8 3.6 %collective-permute-start.13 = (bf16[528,128]{1,0:T(8,128)(2,1)S(1)}, bf16[528,128]{1,0:T(8,128)(2,1)S(1)}, u32[]{:S(2)}, u32[]{:S(2)}) collective-permute-start(bf16[528,128]{1,0:T(8,128)(2,1)S(1)} %get-tuple-element.26), channel_id=1, source_target_pairs={{0,12},{2,14},{4,0},{6,2},{8,4},{10,6},{12,8},{14,10},{1,13},{3,15... | collective-permute-start | bytes 405512 | tf_op jit(solution)/shard_map/ppermute | solution.py:26
  66.8 1.9 %collective-permute-start.15 = (bf16[528,128]{1,0:T(8,128)(2,1)S(1)}, bf16[528,128]{1,0:T(8,128)(2,1)S(1)}, u32[]{:S(2)}, u32[]{:S(2)}) collective-permute-start(bf16[528,128]{1,0:T(8,128)(2,1)S(1)} %add_convert_fusion.2), channel_id=1, source_target_pairs={{0,6},{2,8},{4,10},{6,12},{8,14},{10,0},{12,2},{14,4},{1,7},{3,9},... | collective-permute-start | bytes 405512 | tf_op jit(solution)/shard_map/ppermute | solution.py:26
  68.7 14.6 %collective-permute-start.7 = (bf16[4,64,256]{2,1,0:T(8,128)(2,1)S(1)}, bf16[4,64,256]{2,1,0:T(8,128)(2,1)S(1)}, u32[]{:S(2)}, u32[]{:S(2)}) collective-permute-start(bf16[4,64,256]{2,1,0:T(8,128)(2,1)S(1)} %collective-permute-done.6.refs_6_), channel_id=1, source_target_pairs={{0,1},{1,0},{2,3},{3,2},{4,5},{5,4},{6,7},{7,6},{8,9},{9,8},{10,11... | collective-permute-start | bytes 393224 | tf_op jit(solution)/shard_map/ppermute | solution.py:21
  83.9 2.3 %inner.1.refs_12_ = bf16[8,256,128]{2,1,0:T(8,128)(2,1)} custom-call(bf16[528,128]{1,0:T(8,128)(2,1)S(1)} %get-tuple-element.22.refs_0_, bf16[528,128]{1,0:T(8,128)(2,1)S(1)} %collective-permute-done.10.refs_1_, bf16[528,128]{1,0:T(8,128)(2,1)S(1)} %collective-permute-done.11.refs_2_, bf16[528,128]{1,0:T(8,128)(2,1)S(1)} %collective-permute-done.12.refs_3_, ...), custom_call_target="tpu_custom_call" | custom-call | flops 2162688 | bytes 2162688 | tf_op jit(solution)/shard_map/inner/pallas_call | solution.py:422
  86.2 3.4 %shared.1 = (f32[8,64,256]{2,1,0:T(8,128)}, bf16[8,64,256]{2,1,0:T(8,128)(2,1)S(1)}) custom-call(s32[4]{0:T(128)S(1)} %add_add_fusion.at, bf16[1,64,256]{2,1,0:T(8,128)(2,1)S(1)} %bitcast.40, bf16[1,64,256]{2,1,0:T(8,128)(2,1)S(1)} %bitcast.41, bf16[1,64,256]{2,1,0:T(8,128)(2,1)S(1)} %collective-permute-done.2.refs_2_, ...), custom_call_target="tpu_custom_call" | custom-call | flops 100663296 | bytes 1572864 | tf_op jit(solution)/shard_map/shared/pallas_call | solution.py:370
  89.8 4.2 %all-to-all-start.2 = ((bf16[8,256,128]{2,1,0:T(8,128)(2,1)}), bf16[8,256,128]{2,1,0:T(8,128)(2,1)S(1)}, u32[]{:S(2)}, u32[]{:S(2)}) async-start(bf16[8,256,128]{2,1,0:T(8,128)(2,1)} %inner.1.refs_12_), calls=%async_computation.2 | async-start | bytes 1048576 | tf_op jit(solution)/shard_map/all_to_all | solution.py:588
  95.2 5.4 %collective-permute-start.19 = (bf16[4,64,256]{2,1,0:T(8,128)(2,1)S(1)}, bf16[4,64,256]{2,1,0:T(8,128)(2,1)S(1)}, u32[]{:S(2)}, u32[]{:S(2)}) collective-permute-start(bf16[4,64,256]{2,1,0:T(8,128)(2,1)S(1)} %slice.57), channel_id=1, source_target_pairs={{0,8},{2,10},{4,12},{6,14},{8,0},{10,2},{12,4},{14,6},{1,9},{3,11}... | collective-permute-start | bytes 393224 | tf_op jit(solution)/shard_map/ppermute | solution.py:30
  100.6 17.0 %collective-permute-done.19 = bf16[4,64,256]{2,1,0:T(8,128)(2,1)S(1)} collective-permute-done((bf16[4,64,256]{2,1,0:T(8,128)(2,1)S(1)}, bf16[4,64,256]{2,1,0:T(8,128)(2,1)S(1)}, u32[]{:S(2)}, u32[]{:S(2)}) %collective-permute-start.19) | collective-permute-done | bytes 131104 | tf_op jit(solution)/shard_map/ppermute | solution.py:30
  117.7 3.3 %down.1 = bf16[16,2,16,256]{3,2,1,0:T(8,128)(2,1)} custom-call(s32[4]{0:T(128)S(1)} %add_add_fusion.at, bf16[8,256,128]{2,1,0:T(8,128)(2,1)S(1)} %all-to-all-done.2.arrived, bf16[4,1024,256]{2,1,0:T(8,128)(2,1)S(1)} %copy-done, bf16[4,1024,256]{2,1,0:T(8,128)(2,1)} %collective-permute-done.22.par), custom_call_target="tpu_custom_call" | custom-call | flops 268435456 | bytes 2097152 | tf_op jit(solution)/shard_map/down/pallas_call | solution.py:475
  121.0 3.5 %all-to-all-start.3 = ((bf16[16,2,16,256]{3,2,1,0:T(8,128)(2,1)}), bf16[16,2,16,256]{3,2,1,0:T(8,128)(2,1)S(1)}, u32[]{:S(2)}, u32[]{:S(2)}) async-start(bf16[16,2,16,256]{3,2,1,0:T(8,128)(2,1)} %down.1), calls=%async_computation.3 | async-start | bytes 524288 | tf_op jit(solution)/shard_map/all_to_all | solution.py:590
  124.9 7.6 %all-to-all-done.3.arrived = bf16[16,2,16,256]{3,2,1,0:T(8,128)(2,1)S(1)} async-done(((bf16[16,2,16,256]{3,2,1,0:T(8,128)(2,1)}), bf16[16,2,16,256]{3,2,1,0:T(8,128)(2,1)S(1)}, u32[]{:S(2)}, u32[]{:S(2)}) %all-to-all-start.3) | async-done | bytes 262176 | tf_op jit(solution)/shard_map/all_to_all | solution.py:590
  132.7 1.8 %collective-permute-start.23 = (bf16[64,256]{1,0:T(8,128)(2,1)S(1)}, bf16[64,256]{1,0:T(8,128)(2,1)S(1)}, u32[]{:S(2)}, u32[]{:S(2)}) collective-permute-start(bf16[64,256]{1,0:T(8,128)(2,1)S(1)} %get-tuple-element.34), channel_id=1, source_target_pairs={{0,1},{1,0},{2,3},{3,2},{4,5},{5,4},{6,7},{7,6},{8,9},{9,8},{10,11... | collective-permute-start | bytes 98312 | tf_op jit(solution)/shard_map/ppermute | solution.py:21
  (85 shorter events, 14.2 us)
Async XLA Ops:
  0.7 49.3 %collective-permute-start.8 = (bf16[4,256,1024]{2,1,0:T(8,128)(2,1)}, bf16[4,256,1024]{2,1,0:T(8,128)(2,1)}, u32[]{:S(2)}, u32[]{:S(2)}) collective-permute-start(bf16[4,256,1024]{2,1,0:T(8,128)(2,1)} %gate.1), channel_id=1, source_target_pairs={{0,1},{1,0},{2,3},{3,2},{4,5},{5,4},{6,7},{7,6},{8,9},{9,8},{10,11... | collective-permute-start | bytes 6291464 | tf_op jit(solution)/shard_map/ppermute | solution.py:21
  3.9 46.0 %collective-permute-start.9 = (bf16[4,256,1024]{2,1,0:T(8,128)(2,1)}, bf16[4,256,1024]{2,1,0:T(8,128)(2,1)}, u32[]{:S(2)}, u32[]{:S(2)}) collective-permute-start(bf16[4,256,1024]{2,1,0:T(8,128)(2,1)} %up.1), channel_id=1, source_target_pairs={{0,1},{1,0},{2,3},{3,2},{4,5},{5,4},{6,7},{7,6},{8,9},{9,8},{10,11... | collective-permute-start | bytes 6291464 | tf_op jit(solution)/shard_map/ppermute | solution.py:21
  8.1 3.2 %collective-permute-start = (bf16[8,64,256]{2,1,0:T(8,128)(2,1)}, bf16[8,64,256]{2,1,0:T(8,128)(2,1)S(1)}, u32[]{:S(2)}, u32[]{:S(2)}) collective-permute-start(bf16[8,64,256]{2,1,0:T(8,128)(2,1)} %get-tuple-element.21), channel_id=1, source_target_pairs={{0,1},{1,0},{2,3},{3,2},{4,5},{5,4},{6,7},{7,6},{8,9},{9,8},{10,11... | collective-permute-start | bytes 786440 | tf_op jit(solution)/shard_map/ppermute | solution.py:21
  8.6 109.1 %collective-permute-start.22 = (bf16[4,1024,256]{2,1,0:T(8,128)(2,1)S(1)}, bf16[4,1024,256]{2,1,0:T(8,128)(2,1)}, u32[]{:S(2)}, u32[]{:S(2)}) collective-permute-start(bf16[4,1024,256]{2,1,0:T(8,128)(2,1)S(1)} %copy-done), channel_id=1, source_target_pairs={{0,1},{1,0},{2,3},{3,2},{4,5},{5,4},{6,7},{7,6},{8,9},{9,8},{10,11... | collective-permute-start | bytes 6291464 | tf_op jit(solution)/shard_map/ppermute | solution.py:21
  13.0 17.6 %all-to-all-start = ((bf16[8,64,256]{2,1,0:T(8,128)(2,1)}), bf16[8,64,256]{2,1,0:T(8,128)(2,1)S(1)}, u32[]{:S(2)}, u32[]{:S(2)}) async-start(bf16[8,64,256]{2,1,0:T(8,128)(2,1)} %add_convert_fusion), calls=%async_computation | async-start | bytes 524288 | tf_op jit(solution)/shard_map/all_to_all | solution.py:547
  33.2 8.6 %collective-permute-start.2 = (bf16[1,64,256]{2,1,0:T(8,128)(2,1)S(1)}, bf16[1,64,256]{2,1,0:T(8,128)(2,1)S(1)}, u32[]{:S(2)}, u32[]{:S(2)}) collective-permute-start(bf16[1,64,256]{2,1,0:T(8,128)(2,1)S(1)} %bitcast.37), channel_id=1, source_target_pairs={{0,2},{2,0},{4,6},{6,4},{8,10},{10,8},{12,14},{14,12},{1,3},{3,1},... | collective-permute-start | bytes 98312 | tf_op jit(solution)/shard_map/ppermute | solution.py:30
  35.0 14.9 %all-to-all-start.1 = ((bf16[16,2,16,256]{3,2,1,0:T(8,128)(2,1)}), bf16[16,2,16,256]{3,2,1,0:T(8,128)(2,1)S(1)}, u32[]{:S(2)}, u32[]{:S(2)}) async-start(bf16[16,2,16,256]{3,2,1,0:T(8,128)(2,1)} %dispatch.1), calls=%async_computation.1 | async-start | bytes 524288 | tf_op jit(solution)/shard_map/all_to_all | solution.py:571
  41.8 12.9 %collective-permute-start.4 = (bf16[2,64,256]{2,1,0:T(8,128)(2,1)S(1)}, bf16[2,64,256]{2,1,0:T(8,128)(2,1)S(1)}, u32[]{:S(2)}, u32[]{:S(2)}) collective-permute-start(bf16[2,64,256]{2,1,0:T(8,128)(2,1)S(1)} %pad_maximum_fusion.1), channel_id=1, source_target_pairs={{0,8},{2,10},{4,12},{6,14},{8,0},{10,2},{12,4},{14,6},{1,9},{3,11}... | collective-permute-start | bytes 196616 | tf_op jit(solution)/shard_map/ppermute | solution.py:30
  54.6 3.2 %collective-permute-start.16 = (bf16[264,128]{1,0:T(8,128)(2,1)S(1)}, bf16[264,128]{1,0:T(8,128)(2,1)S(1)}, u32[]{:S(2)}, u32[]{:S(2)}) collective-permute-start(bf16[264,128]{1,0:T(8,128)(2,1)S(1)} %get-tuple-element.30), channel_id=1, source_target_pairs={{0,14},{2,0},{4,2},{6,4},{8,6},{10,8},{12,10},{14,12},{1,15},{3,1}... | collective-permute-start | bytes 202760 | tf_op jit(solution)/shard_map/ppermute | solution.py:26
  54.8 7.0 %collective-permute-start.6 = (bf16[4,64,256]{2,1,0:T(8,128)(2,1)S(1)}, bf16[4,64,256]{2,1,0:T(8,128)(2,1)S(1)}, u32[]{:S(2)}, u32[]{:S(2)}) collective-permute-start(bf16[4,64,256]{2,1,0:T(8,128)(2,1)S(1)} %pad_maximum_fusion), channel_id=1, source_target_pairs={{0,4},{2,6},{4,0},{6,2},{8,12},{10,14},{12,8},{14,10},{1,5},{3,7},... | collective-permute-start | bytes 393224 | tf_op jit(solution)/shard_map/ppermute | solution.py:30
  56.9 4.9 %collective-permute-start.14 = (bf16[264,128]{1,0:T(8,128)(2,1)S(1)}, bf16[264,128]{1,0:T(8,128)(2,1)S(1)}, u32[]{:S(2)}, u32[]{:S(2)}) collective-permute-start(bf16[264,128]{1,0:T(8,128)(2,1)S(1)} %get-tuple-element.28), channel_id=1, source_target_pairs={{0,2},{2,4},{4,6},{6,8},{8,10},{10,12},{12,14},{14,0},{1,3},{3,5},... | collective-permute-start | bytes 202760 | tf_op jit(solution)/shard_map/ppermute | solution.py:26
  56.9 8.5 %collective-permute-start.10 = (bf16[528,128]{1,0:T(8,128)(2,1)S(1)}, bf16[528,128]{1,0:T(8,128)(2,1)S(1)}, u32[]{:S(2)}, u32[]{:S(2)}) collective-permute-start(bf16[528,128]{1,0:T(8,128)(2,1)S(1)} %get-tuple-element.23), channel_id=1, source_target_pairs={{0,2},{2,4},{4,6},{6,8},{8,10},{10,12},{12,14},{14,0},{1,3},{3,5},... | collective-permute-start | bytes 405512 | tf_op jit(solution)/shard_map/ppermute | solution.py:26
  57.9 9.0 %collective-permute-start.11 = (bf16[528,128]{1,0:T(8,128)(2,1)S(1)}, bf16[528,128]{1,0:T(8,128)(2,1)S(1)}, u32[]{:S(2)}, u32[]{:S(2)}) collective-permute-start(bf16[528,128]{1,0:T(8,128)(2,1)S(1)} %get-tuple-element.24), channel_id=1, source_target_pairs={{0,14},{2,0},{4,2},{6,4},{8,6},{10,8},{12,10},{14,12},{1,15},{3,1}... | collective-permute-start | bytes 405512 | tf_op jit(solution)/shard_map/ppermute | solution.py:26
  61.8 7.0 %collective-permute-start.12 = (bf16[528,128]{1,0:T(8,128)(2,1)S(1)}, bf16[528,128]{1,0:T(8,128)(2,1)S(1)}, u32[]{:S(2)}, u32[]{:S(2)}) collective-permute-start(bf16[528,128]{1,0:T(8,128)(2,1)S(1)} %get-tuple-element.25), channel_id=1, source_target_pairs={{0,4},{2,6},{4,8},{6,10},{8,12},{10,14},{12,0},{14,2},{1,5},{3,7},... | collective-permute-start | bytes 405512 | tf_op jit(solution)/shard_map/ppermute | solution.py:26
  61.8 21.6 %collective-permute-start.13 = (bf16[528,128]{1,0:T(8,128)(2,1)S(1)}, bf16[528,128]{1,0:T(8,128)(2,1)S(1)}, u32[]{:S(2)}, u32[]{:S(2)}) collective-permute-start(bf16[528,128]{1,0:T(8,128)(2,1)S(1)} %get-tuple-element.26), channel_id=1, source_target_pairs={{0,12},{2,14},{4,0},{6,2},{8,4},{10,6},{12,8},{14,10},{1,13},{3,15... | collective-permute-start | bytes 405512 | tf_op jit(solution)/shard_map/ppermute | solution.py:26
  65.3 18.0 %collective-permute-start.17 = (bf16[528,128]{1,0:T(8,128)(2,1)S(1)}, bf16[528,128]{1,0:T(8,128)(2,1)S(1)}, u32[]{:S(2)}, u32[]{:S(2)}) collective-permute-start(bf16[528,128]{1,0:T(8,128)(2,1)S(1)} %add_convert_fusion.1), channel_id=1, source_target_pairs={{0,10},{2,12},{4,14},{6,0},{8,2},{10,4},{12,6},{14,8},{1,11},{3,13... | collective-permute-start | bytes 405512 | tf_op jit(solution)/shard_map/ppermute | solution.py:26
  66.8 17.0 %collective-permute-start.15 = (bf16[528,128]{1,0:T(8,128)(2,1)S(1)}, bf16[528,128]{1,0:T(8,128)(2,1)S(1)}, u32[]{:S(2)}, u32[]{:S(2)}) collective-permute-start(bf16[528,128]{1,0:T(8,128)(2,1)S(1)} %add_convert_fusion.2), channel_id=1, source_target_pairs={{0,6},{2,8},{4,10},{6,12},{8,14},{10,0},{12,2},{14,4},{1,7},{3,9},... | collective-permute-start | bytes 405512 | tf_op jit(solution)/shard_map/ppermute | solution.py:26
  68.7 17.4 %collective-permute-start.7 = (bf16[4,64,256]{2,1,0:T(8,128)(2,1)S(1)}, bf16[4,64,256]{2,1,0:T(8,128)(2,1)S(1)}, u32[]{:S(2)}, u32[]{:S(2)}) collective-permute-start(bf16[4,64,256]{2,1,0:T(8,128)(2,1)S(1)} %collective-permute-done.6.refs_6_), channel_id=1, source_target_pairs={{0,1},{1,0},{2,3},{3,2},{4,5},{5,4},{6,7},{7,6},{8,9},{9,8},{10,11... | collective-permute-start | bytes 393224 | tf_op jit(solution)/shard_map/ppermute | solution.py:21
  89.6 4.4 %collective-permute-start.18 = (bf16[8,64,256]{2,1,0:T(8,128)(2,1)S(1)}, bf16[8,64,256]{2,1,0:T(8,128)(2,1)S(1)}, u32[]{:S(2)}, u32[]{:S(2)}) collective-permute-start(bf16[8,64,256]{2,1,0:T(8,128)(2,1)S(1)} %get-tuple-element.32), channel_id=1, source_target_pairs={{0,1},{1,0},{2,3},{3,2},{4,5},{5,4},{6,7},{7,6},{8,9},{9,8},{10,11... | collective-permute-start | bytes 786440 | tf_op jit(solution)/shard_map/ppermute | solution.py:21
  89.8 27.9 %all-to-all-start.2 = ((bf16[8,256,128]{2,1,0:T(8,128)(2,1)}), bf16[8,256,128]{2,1,0:T(8,128)(2,1)S(1)}, u32[]{:S(2)}, u32[]{:S(2)}) async-start(bf16[8,256,128]{2,1,0:T(8,128)(2,1)} %inner.1.refs_12_), calls=%async_computation.2 | async-start | bytes 1048576 | tf_op jit(solution)/shard_map/all_to_all | solution.py:588
  95.2 22.4 %collective-permute-start.19 = (bf16[4,64,256]{2,1,0:T(8,128)(2,1)S(1)}, bf16[4,64,256]{2,1,0:T(8,128)(2,1)S(1)}, u32[]{:S(2)}, u32[]{:S(2)}) collective-permute-start(bf16[4,64,256]{2,1,0:T(8,128)(2,1)S(1)} %slice.57), channel_id=1, source_target_pairs={{0,8},{2,10},{4,12},{6,14},{8,0},{10,2},{12,4},{14,6},{1,9},{3,11}... | collective-permute-start | bytes 393224 | tf_op jit(solution)/shard_map/ppermute | solution.py:30
  117.6 7.1 %collective-permute-start.20 = (bf16[2,64,256]{2,1,0:T(8,128)(2,1)S(1)}, bf16[2,64,256]{2,1,0:T(8,128)(2,1)S(1)}, u32[]{:S(2)}, u32[]{:S(2)}) collective-permute-start(bf16[2,64,256]{2,1,0:T(8,128)(2,1)S(1)} %slice.58), channel_id=1, source_target_pairs={{0,4},{2,6},{4,0},{6,2},{8,12},{10,14},{12,8},{14,10},{1,5},{3,7},... | collective-permute-start | bytes 196616 | tf_op jit(solution)/shard_map/ppermute | solution.py:30
  121.0 11.4 %all-to-all-start.3 = ((bf16[16,2,16,256]{3,2,1,0:T(8,128)(2,1)}), bf16[16,2,16,256]{3,2,1,0:T(8,128)(2,1)S(1)}, u32[]{:S(2)}, u32[]{:S(2)}) async-start(bf16[16,2,16,256]{3,2,1,0:T(8,128)(2,1)} %down.1), calls=%async_computation.3 | async-start | bytes 524288 | tf_op jit(solution)/shard_map/all_to_all | solution.py:590
  124.8 9.8 %collective-permute-start.21 = (bf16[1,64,256]{2,1,0:T(8,128)(2,1)S(1)}, bf16[1,64,256]{2,1,0:T(8,128)(2,1)S(1)}, u32[]{:S(2)}, u32[]{:S(2)}) collective-permute-start(bf16[1,64,256]{2,1,0:T(8,128)(2,1)S(1)} %slice.59), channel_id=1, source_target_pairs={{0,2},{2,0},{4,6},{6,4},{8,10},{10,8},{12,14},{14,12},{1,3},{3,1},... | collective-permute-start | bytes 98312 | tf_op jit(solution)/shard_map/ppermute | solution.py:30
  (11 other events, 180.8 us)

commit v3 on v2

--- a/solution.py
+++ b/solution.py
@@ -26,8 +26,11 @@
     return lax.ppermute(x, axis, [(i, (i + steps) % count) for i in range(count)])
 
 
-def exchanged(x, axis, bit):
-    return lax.ppermute(x, axis, [(i, i ^ bit) for i in range(lax.axis_size(axis))])
+def both_ways(x, steps):
+    count = lax.axis_size("z")
+    ups = [(2 * i, 2 * ((i + steps) % count)) for i in range(count)]
+    downs = [(2 * i + 1, 2 * ((i - steps) % count) + 1) for i in range(count)]
+    return lax.ppermute(x, TP, ups + downs)
 
 
 def added(x, part, first):
@@ -287,93 +290,96 @@
     )(spread, own, par)
 
 
-def combine_kernel(weights, arrived, own, given, returned, arrival):
+def combine_kernel(weights, arrived, base, *refs):
+    *parts, own, given, returned, arrival = refs
     fetch(arrived, returned, arrival)
     high, low = two_parts(weights[...])
     rows, width = weights.shape[1], returned.shape[3]
-    for part, out in enumerate((own, given)):
-        values = returned[:, part].reshape(rows, width)
-        out[...] = (dot32(high, values) + dot32(low, values)).astype(out.dtype)
-
-
-def combined(weights, returned):
+    for slot, out in enumerate((own, given)):
+        values = returned[:, slot].reshape(rows, width)
+        total = dot32(high, values) + dot32(low, values)
+        if slot == 0:
+            total = total + base[...]
+        for part in parts:
+            if slot < part.shape[0]:
+                total = total + part[slot].astype(F32)
+        out[...] = total.astype(out.dtype)
+
+
+def combined(weights, returned, base, parts):
     shape = (weights.shape[0], returned.shape[3])
     vmem = pl.BlockSpec(memory_space=pltpu.VMEM)
     return pl.pallas_call(
         combine_kernel,
         out_shape=(jax.ShapeDtypeStruct(shape, F32), jax.ShapeDtypeStruct(shape, BF16)),
-        in_specs=[vmem, pl.BlockSpec(memory_space=pl.ANY)],
+        in_specs=[vmem, pl.BlockSpec(memory_space=pl.ANY)] + [vmem] * (1 + len(parts)),
         out_specs=(vmem, vmem),
         scratch_shapes=[pltpu.VMEM(returned.shape, BF16), pltpu.SemaphoreType.DMA],
         compiler_params=ROOM,
         cost_estimate=cost(8 * weights.size * shape[1], 2 * returned.size),
         name="combine",
-    )(weights, returned)
-
-
-def shared_kernel(at, pieces, gain, sources, kept, given, gate_t, up_t, down_t, arrivals):
+    )(weights, returned, base, *parts)
+
+
+def shared_kernel(at, own, par, mine, theirs, gain, sources, kept, given, *scratch):
+    *weights, arrivals = scratch
     copies = [
         pltpu.make_async_copy(source, target, arrivals.at[i])
-        for i, (source, target) in enumerate(zip(sources, (gate_t, up_t, down_t), strict=True))
+        for i, (source, target) in enumerate(zip(sources, weights, strict=True))
     ]
     for copy in copies:
         copy.start()
     for copy in copies:
         copy.wait()
+    gate_t, up_t, down_t = weights
     c, z = at[0], at[3]
     seqs, width = kept.shape[1:]
+    chips = gain.shape[1] // (2 * width)
+    way = 1 - 2 * c
+
+    def features(steps, place):
+        chip = lax.rem(z + way * steps + 2 * chips, chips)
+        return pl.ds(pl.multiple_of((2 * chip + place) * width, width), width)
+
     squares = jnp.zeros((seqs, 1), F32)
     gate = jnp.zeros((seqs, gate_t.shape[0]), F32)
     up = gate
-    chips = grown_order(kept.shape[0])
-    for part, place in ((0, c), (1, 1 - c)):
-        rows = [piece[part][i] for piece in pieces for i in range(piece[part].shape[0])]
-        for chip, values in zip(chips, rows, strict=True):
-            values = values.astype(F32)
-            squares = squares + jnp.sum(values * values, axis=-1, keepdims=True)
-            first = (2 * jnp.bitwise_xor(z, chip) + place) * width
-            features = pl.ds(pl.multiple_of(first, width), width)
-            scaled = (values * gain[:, features]).astype(BF16)
-            gate = gate + dot_nt(scaled, gate_t[:, features])
-            up = up + dot_nt(scaled, up_t[:, features])
-    factor = lax.rsqrt(squares / (2 * len(chips) * width) + EPS)
+    rows = [(own[...], features(0, c)), (par[...], features(0, 1 - c))]
+    for pieces, first, sign in ((mine, c, -1), (theirs, 1 - c, 1)):
+        for k, piece in enumerate(pieces):
+            rows.append((piece[0], features(sign * (k + 1), first)))
+            if piece.shape[0] > 1:
+                rows.append((piece[1], features(sign * (k + 1), 1 - first)))
+    for values, place in rows:
+        values = values.astype(F32)
+        squares = squares + jnp.sum(values * values, axis=-1, keepdims=True)
+        scaled = (values * gain[:, place]).astype(BF16)
+        gate = gate + dot_nt(scaled, gate_t[:, place])
+        up = up + dot_nt(scaled, up_t[:, place])
+    factor = lax.rsqrt(squares / gain.shape[1] + EPS)
     gate, up = gate * factor, up * factor
     inner = (gate / (1.0 + jnp.exp(-gate)) * up).astype(BF16)
-    for chip in range(len(chips)):
-        for out, place in ((kept, c), (given, 1 - c)):
-            first = (2 * jnp.bitwise_xor(z, chip) + place) * width
-            features = pl.ds(pl.multiple_of(first, width), width)
-            out[chip] = dot32(inner, down_t[:, features]).astype(out.dtype)
-
-
-def growing(chips):
-    return [1] + [chips >> i for i in range(1, chips.bit_length() - 1)]
-
-
-def grown_order(chips):
-    order = [0]
-    for bit in growing(chips):
-        order = order + [owner ^ bit for owner in order]
-    return order
-
-
-def shared_parts(at, pieces, gain, gate_t, up_t, w_down, after):
+    for out, first, sign in ((kept, c, 1), (given, 1 - c, -1)):
+        order = [(sign * k, place) for k in range(chips // 2 - 1, 0, -1) for place in (first, 1 - first)]
+        for i, (steps, place) in enumerate([*order, (chips // 2, first), (0, first)]):
+            out[i] = dot32(inner, down_t[:, features(steps, place)]).astype(out.dtype)
+
+
+def shared_parts(at, own, par, mine, theirs, gain, gate_t, up_t, w_down, after):
     smem, vmem = pl.BlockSpec(memory_space=pltpu.SMEM), pl.BlockSpec(memory_space=pltpu.VMEM)
-    flat = [rows for piece in pieces for rows in piece]
-    (seqs, width), z_count = flat[0].shape[1:], sum(rows.shape[0] for rows in flat) // 2
-
-    def kernel(at, *refs):
-        rows, (gain, *rest) = refs[: len(flat)], refs[len(flat) :]
-        paired = [(rows[i], rows[i + 1]) for i in range(0, len(flat), 2)]
-        shared_kernel(at, paired, gain, rest[:3], *rest[4:])
+    (seqs, width), count = own.shape, len(mine)
+
+    def kernel(at, own, par, *refs):
+        first, second, (gain, *rest) = refs[:count], refs[count : 2 * count], refs[2 * count :]
+        shared_kernel(at, own, par, first, second, gain, rest[:3], *rest[4:])
 
     return pl.pallas_call(
         kernel,
         out_shape=(
-            jax.ShapeDtypeStruct((z_count, seqs, width), F32),
-            jax.ShapeDtypeStruct((z_count, seqs, width), BF16),
+            jax.ShapeDtypeStruct((2 * count, seqs, width), F32),
+            jax.ShapeDtypeStruct((2 * count, seqs, width), BF16),
         ),
-        in_specs=[smem] + [vmem] * (len(flat) + 1) + [pl.BlockSpec(memory_space=pl.ANY)] * 4,
+        in_specs=[smem] + [vmem] * (2 * count + 3) + [pl.BlockSpec(memory_space=pl.ANY)] * 4,
         out_specs=(vmem, vmem),
         scratch_shapes=[
             pltpu.VMEM(gate_t.shape, BF16),
@@ -384,7 +390,7 @@
         compiler_params=pltpu.CompilerParams(vmem_limit_bytes=FULL),
         cost_estimate=cost(seqs * 6 * w_down.size, 6 * w_down.size),
         name="shared",
-    )(at, *flat, gain, gate_t, up_t, w_down, after)
+    )(at, own, par, *mine, *theirs, gain, gate_t, up_t, w_down, after)
 
 
 def inner_kernel(model_width, half, *refs):
@@ -589,29 +595,38 @@
     results = down(at, inner_all, expert_down, down_par, ep_count, capacity)
     returned = lax.all_to_all(results, "ep", split_axis=0, concat_axis=0, tiled=True)
 
-    pieces = [(resid_own[None], resid_par[None])]
-    for bit in growing(z_count):
-        held = jnp.concatenate([piece[0] for piece in pieces])
-        theirs = exchanged(held, "z", bit)
-        pieces.append((theirs, swapped(theirs)))
+    held = jnp.stack([resid_own, resid_par])
+    mine, theirs = [], []
+    for steps in range(1, middle + 1):
+        mine.append(both_ways(held if steps < middle else resid_own[None], steps))
+        theirs.append(swapped(mine[-1]))
     kept, given = shared_parts(
-        at, pieces, gain, shared_gate.T, shared_up.T, shared_down, copies
+        at,
+        resid_own,
+        resid_par,
+        mine,
+        theirs,
+        gain,
+        shared_gate.T,
+        shared_up.T,
+        shared_down,
+        copies,
     )
     got = swapped(given)
-    shared_own = kept + got.astype(F32)
-    count = z_count // 2
-    while count > 0:
-        theirs = exchanged(shared_own[count:].astype(BF16), "z", count)
-        shared_own = shared_own[:count] + theirs.astype(F32)
-        count //= 2
-    shared_own = shared_own[0]
+    shared_sums = kept + got.astype(F32)
+    leaving = shared_sums.astype(BF16)
+    shared_chip = []
+    for steps in range(1, middle + 1):
+        first = 2 * (middle - 1 - steps) if steps < middle else 2 * (middle - 1)
+        part = leaving[first : first + (2 if steps < middle else 1)]
+        shared_chip.append(both_ways(part, steps))
 
     weights = route_weight / jnp.sum(route_weight, axis=1, keepdims=True) * ROUTED_SCALE
     chosen = target.reshape(seq_count, top_count)[:, :, None] == slot_ids[None, None, :]
     combine = jnp.sum(jnp.where(chosen, weights[:, :, None], 0.0), axis=1)
-    routed, routed_par = combined(combine, returned)
-    routed = routed + swapped(routed_par).astype(F32)
-    mixed = (resid_own.astype(F32) + shared_own + routed).astype(BF16)
+    own, given = combined(combine, returned, shared_sums[-1], shared_chip)
+    got = swapped(given)
+    mixed = (resid_own.astype(F32) + own + got.astype(F32)).astype(BF16)
     return (mixed, new_real, new_imag)
 
 

time: 137 us -> 141 us (1.029)
  starting transfers between devices: 62.2 us -> 70.1 us
  waiting for transfers between devices: 47.6 us -> 42.1 us
    ppermute x6 -> x8, waiting for transfers between devices: 19.1 us -> 6.97 us  [both_ways(): return lax.ppermute(x, TP, ups + downs)]
    ppermute x8, waiting for transfers between devices: 0.37 us -> 11.4 us  [moved(): lax.ppermute(x, axis, [(i, (i + steps) % count) for i in range(count)])]
    all_to_all x1, waiting for transfers between devices: 7.56 us -> 0.01 us  [local(): lax.all_to_all(results, 'ep', split_axis=0, concat_axis=0, tiled=True)]
    ppermute x6 -> x8, starting transfers between devices: 8.98 us -> 16.5 us  [both_ways(): return lax.ppermute(x, TP, ups + downs)]
    ppermute x10 -> x11, starting transfers between devices: 22.9 us -> 19.3 us  [swapped(): return lax.ppermute(x, 'c', [(0, 1), (1, 0)])]
    all_to_all x1, starting transfers between devices: 4.19 us -> 6.64 us  [local(): lax.all_to_all(copies, 'z', split_axis=0, concat_axis=0, tiled=True)]
    ppermute x10 -> x11, waiting for transfers between devices: 3.47 us -> 5.65 us  [swapped(): return lax.ppermute(x, 'c', [(0, 1), (1, 0)])]
    convert_element_type x1 -> x2, other arithmetic: 0.63 us -> 2.54 us  [the longest x1 1.92 us: local(): leaving = shared_sums.astype(BF16)]
  transfers between devices with their start and end apart: 28 -> 31, of which waited for: 9 -> 14; matrix products, arithmetic and copies ran while one was open for 4% -> 5% of each run, Pallas kernels for 14% -> 11%
where the time goes in v3:
time: 141 us; the launch traced here: 140 us
  starting transfers between devices  70.1 us (50%)
  waiting for transfers between devices  42.1 us (30%)
  Pallas kernels  18.9 us (13%)
  other arithmetic  6.24 us (4%)
  local copies, waits for them, and re-layouts  1.68 us (1%)
    ppermute x11, starting transfers between devices, swapped(): return lax.ppermute(x, 'c', [(0, 1), (1, 0)])  19.3 us
    ppermute x8, starting transfers between devices, both_ways(): return lax.ppermute(x, TP, ups + downs)  16.5 us
    ppermute x8, waiting for transfers between devices, moved(): lax.ppermute(x, axis, [(i, (i + steps) % count) for i in range(count)])  11.4 us
    ppermute x8, starting transfers between devices, moved(): lax.ppermute(x, axis, [(i, (i + steps) % count) for i in range(count)])  10.9 us
    all_to_all x1, waiting for transfers between devices, local(): lax.all_to_all(both, 'z', split_axis=0, concat_axis=0, tiled=True)  9.9 us
    all_to_all x1, waiting for transfers between devices, local(): lax.all_to_all(outgoing, 'ep', split_axis=0, concat_axis=0, tiled=True)  8.1 us
    ppermute x8, waiting for transfers between devices, both_ways(): return lax.ppermute(x, TP, ups + downs)  6.97 us
    all_to_all x1, starting transfers between devices, local(): lax.all_to_all(outgoing, 'ep', split_axis=0, concat_axis=0, tiled=True)  6.76 us
  transfers between devices with their start and end apart: 31, of which 14 were waited for; matrix products, arithmetic and copies ran while one was open for 5% of the time, Pallas kernels for 11%

profile of v3, /device:TPU:1, one launch (start us, length us, event | category | flops | bytes accessed | tf_op | source)
XLA Modules:
  0.0 139.9 jit_solution(15931230530048195765)
XLA Ops:
  0.7 3.3 %collective-permute-start.2 = (bf16[4,256,1024]{2,1,0:T(8,128)(2,1)}, bf16[4,256,1024]{2,1,0:T(8,128)(2,1)}, u32[]{:S(2)}, u32[]{:S(2)}) collective-permute-start(bf16[4,256,1024]{2,1,0:T(8,128)(2,1)} %gate.1), channel_id=1, source_target_pairs={{0,1},{1,0},{2,3},{3,2},{4,5},{5,4},{6,7},{7,6},{8,9},{9,8},{10,11... | collective-permute-start | bytes 6291464 | tf_op jit(solution)/shard_map/ppermute | solution.py:21
  4.0 4.0 %front.1 = (f32[64,512]{1,0:T(8,128)}, f32[64,512]{1,0:T(8,128)}, bf16[8,64,256]{2,1,0:T(8,128)(2,1)}, bf16[8,64,256]{2,1,0:T(8,128)(2,1)}) custom-call(s32[1]{0:T(128)} %bitcast.core, f32[8]{0:T(128)} %log_step.1, bf16[64,4096]{1,0:T(8,128)(2,1)} %tokens.1, f32[1,4096]{1,0:T(1,128)} %bitcast.38, bf16[4096,128]{1,0:T(8,128)(2,1)} %w_in.1, ...), custom_call_target="tpu_custom_call" | custom-call | flops 134217728 | bytes 2097152 | tf_op jit(solution)/shard_map/front/pallas_call | solution.py:151
  13.0 6.5 %all-to-all-start = ((bf16[8,64,256]{2,1,0:T(8,128)(2,1)}), bf16[8,64,256]{2,1,0:T(8,128)(2,1)S(1)}, u32[]{:S(2)}, u32[]{:S(2)}) async-start(bf16[8,64,256]{2,1,0:T(8,128)(2,1)} %add_convert_fusion), calls=%async_computation | async-start | bytes 524288 | tf_op jit(solution)/shard_map/all_to_all | solution.py:553
  20.7 9.9 %all-to-all-done = bf16[8,64,256]{2,1,0:T(8,128)(2,1)S(1)} async-done(((bf16[8,64,256]{2,1,0:T(8,128)(2,1)}), bf16[8,64,256]{2,1,0:T(8,128)(2,1)S(1)}, u32[]{:S(2)}, u32[]{:S(2)}) %all-to-all-start) | async-done | bytes 262176 | tf_op jit(solution)/shard_map/all_to_all | solution.py:553
  35.0 6.8 %all-to-all-start.1 = ((bf16[16,2,16,256]{3,2,1,0:T(8,128)(2,1)}), bf16[16,2,16,256]{3,2,1,0:T(8,128)(2,1)S(1)}, u32[]{:S(2)}, u32[]{:S(2)}) async-start(bf16[16,2,16,256]{3,2,1,0:T(8,128)(2,1)} %dispatch.1), calls=%async_computation.1 | async-start | bytes 524288 | tf_op jit(solution)/shard_map/all_to_all | solution.py:577
  41.8 8.1 %all-to-all-done.1.arrived = bf16[16,2,16,256]{3,2,1,0:T(8,128)(2,1)S(1)} async-done(((bf16[16,2,16,256]{3,2,1,0:T(8,128)(2,1)}), bf16[16,2,16,256]{3,2,1,0:T(8,128)(2,1)S(1)}, u32[]{:S(2)}, u32[]{:S(2)}) %all-to-all-start.1) | async-done | bytes 262176 | tf_op jit(solution)/shard_map/all_to_all | solution.py:577
  49.9 4.7 %gate_up.1 = (bf16[528,128]{1,0:T(8,128)(2,1)S(1)}, bf16[528,128]{1,0:T(8,128)(2,1)S(1)}, bf16[528,128]{1,0:T(8,128)(2,1)S(1)}, bf16[528,128]{1,0:T(8,128)(2,1)S...) custom-call(s32[4]{0:T(128)S(1)} %add_add_fusion.at, ...), custom_call_target="tpu_custom_call" | custom-call | flops 536870912 | bytes 4194304 | tf_op jit(solution)/shard_map/gate_up/pallas_call | solution.py:241
  56.5 2.4 %collective-permute-start.5 = (bf16[528,128]{1,0:T(8,128)(2,1)S(1)}, bf16[528,128]{1,0:T(8,128)(2,1)S(1)}, u32[]{:S(2)}, u32[]{:S(2)}) collective-permute-start(bf16[528,128]{1,0:T(8,128)(2,1)S(1)} %get-tuple-element.24), channel_id=1, source_target_pairs={{0,14},{2,0},{4,2},{6,4},{8,6},{10,8},{12,10},{14,12},{1,15},{3,1}... | collective-permute-start | bytes 405512 | tf_op jit(solution)/shard_map/ppermute | solution.py:26
  59.2 3.4 %collective-permute-start.7 = (bf16[528,128]{1,0:T(8,128)(2,1)S(1)}, bf16[528,128]{1,0:T(8,128)(2,1)S(1)}, u32[]{:S(2)}, u32[]{:S(2)}) collective-permute-start(bf16[528,128]{1,0:T(8,128)(2,1)S(1)} %get-tuple-element.26), channel_id=1, source_target_pairs={{0,12},{2,14},{4,0},{6,2},{8,4},{10,6},{12,8},{14,10},{1,13},{3,15... | collective-permute-start | bytes 405512 | tf_op jit(solution)/shard_map/ppermute | solution.py:26
  62.7 3.2 %collective-permute-start.9 = (bf16[528,128]{1,0:T(8,128)(2,1)S(1)}, bf16[528,128]{1,0:T(8,128)(2,1)S(1)}, u32[]{:S(2)}, u32[]{:S(2)}) collective-permute-start(bf16[528,128]{1,0:T(8,128)(2,1)S(1)} %add_convert_fusion.2), channel_id=1, source_target_pairs={{0,6},{2,8},{4,10},{6,12},{8,14},{10,0},{12,2},{14,4},{1,7},{3,9},... | collective-permute-start | bytes 405512 | tf_op jit(solution)/shard_map/ppermute | solution.py:26
  68.5 8.6 %collective-permute-done.11.refs_6_ = bf16[528,128]{1,0:T(8,128)(2,1)S(1)} collective-permute-done((bf16[528,128]{1,0:T(8,128)(2,1)S(1)}, bf16[528,128]{1,0:T(8,128)(2,1)S(1)}, u32[]{:S(2)}, u32[]{:S(2)}) %collective-permute-start.11) | collective-permute-done | bytes 135200 | tf_op jit(solution)/shard_map/ppermute | solution.py:26
  79.4 6.6 %all-to-all-start.2 = ((bf16[8,256,128]{2,1,0:T(8,128)(2,1)}), bf16[8,256,128]{2,1,0:T(8,128)(2,1)S(1)}, u32[]{:S(2)}, u32[]{:S(2)}) async-start(bf16[8,256,128]{2,1,0:T(8,128)(2,1)} %inner.1.refs_12_), calls=%async_computation.2 | async-start | bytes 1048576 | tf_op jit(solution)/shard_map/all_to_all | solution.py:594
  86.1 2.8 %collective-permute-start.13 = (bf16[2,64,256]{2,1,0:T(8,128)(2,1)S(1)}, bf16[2,64,256]{2,1,0:T(8,128)(2,1)S(1)}, u32[]{:S(2)}, u32[]{:S(2)}) collective-permute-start(bf16[2,64,256]{2,1,0:T(8,128)(2,1)S(1)} %pad_maximum_fusion), channel_id=1, source_target_pairs={{0,2},{2,4},{4,6},{6,8},{8,10},{10,12},{12,14},{14,0},{1,15},{3,1}... | collective-permute-start | bytes 196616 | tf_op jit(solution)/shard_map/ppermute | solution.py:33
  92.1 3.3 %collective-permute-start.16 = (bf16[1,64,256]{2,1,0:T(8,128)(2,1)S(1)}, bf16[1,64,256]{2,1,0:T(8,128)(2,1)S(1)}, u32[]{:S(2)}, u32[]{:S(2)}) collective-permute-start(bf16[1,64,256]{2,1,0:T(8,128)(2,1)S(1)} %bitcast.32), channel_id=1, source_target_pairs={{0,8},{2,10},{4,12},{6,14},{8,0},{10,2},{12,4},{14,6},{1,9},{3,11}... | collective-permute-start | bytes 98312 | tf_op jit(solution)/shard_map/ppermute | solution.py:33
  95.4 2.9 %collective-permute-done.13.refs_0_ = bf16[2,64,256]{2,1,0:T(8,128)(2,1)S(1)} collective-permute-done((bf16[2,64,256]{2,1,0:T(8,128)(2,1)S(1)}, bf16[2,64,256]{2,1,0:T(8,128)(2,1)S(1)}, u32[]{:S(2)}, u32[]{:S(2)}) %collective-permute-start.13) | collective-permute-done | bytes 65568 | tf_op jit(solution)/shard_map/ppermute | solution.py:33
  100.9 4.0 %collective-permute-start.18 = (bf16[2,64,256]{2,1,0:T(8,128)(2,1)S(1)}, bf16[2,64,256]{2,1,0:T(8,128)(2,1)S(1)}, u32[]{:S(2)}, u32[]{:S(2)}) collective-permute-start(bf16[2,64,256]{2,1,0:T(8,128)(2,1)S(1)} %collective-permute-done.14.refs_1_), channel_id=1, source_target_pairs={{0,1},{1,0},{2,3},{3,2},{4,5},{5,4},{6,7},{7,6},{8,9},{9,8},{10,11... | collective-permute-start | bytes 196616 | tf_op jit(solution)/shard_map/ppermute | solution.py:21
  104.9 2.4 %collective-permute-start.19 = (bf16[2,64,256]{2,1,0:T(8,128)(2,1)S(1)}, bf16[2,64,256]{2,1,0:T(8,128)(2,1)S(1)}, u32[]{:S(2)}, u32[]{:S(2)}) collective-permute-start(bf16[2,64,256]{2,1,0:T(8,128)(2,1)S(1)} %collective-permute-done.15.refs_2_), channel_id=1, source_target_pairs={{0,1},{1,0},{2,3},{3,2},{4,5},{5,4},{6,7},{7,6},{8,9},{9,8},{10,11... | collective-permute-start | bytes 196616 | tf_op jit(solution)/shard_map/ppermute | solution.py:21
  110.1 3.4 %shared.1 = (f32[8,64,256]{2,1,0:T(8,128)}, bf16[8,64,256]{2,1,0:T(8,128)(2,1)S(1)}) custom-call(s32[4]{0:T(128)S(1)} %add_add_fusion.at, bf16[64,256]{1,0:T(8,128)(2,1)S(1)} %add_convert_fusion.4.own_in.own, bf16[64,256]{1,0:T(8,128)(2,1)S(1)} %collective-permute-done.1.par_in.par, bf16[2,64,256]{2,1,0:T(8,128)(2,1)S(1)} %collective-permute-done.13.refs_0_, ...), custom_call_target="tpu_custom_call" | custom-call | flops 100663296 | bytes 1572864 | tf_op jit(solution)/shard_map/shared/pallas_call | solution.py:376
  117.1 3.3 %down.1 = bf16[16,2,16,256]{3,2,1,0:T(8,128)(2,1)} custom-call(s32[4]{0:T(128)S(1)} %add_add_fusion.at, bf16[8,256,128]{2,1,0:T(8,128)(2,1)S(1)} %all-to-all-done.2.arrived, bf16[4,1024,256]{2,1,0:T(8,128)(2,1)S(1)} %copy-done, bf16[4,1024,256]{2,1,0:T(8,128)(2,1)} %collective-permute-done.12.par), custom_call_target="tpu_custom_call" | custom-call | flops 268435456 | bytes 2097152 | tf_op jit(solution)/shard_map/down/pallas_call | solution.py:481
  120.4 3.5 %all-to-all-start.3 = ((bf16[16,2,16,256]{3,2,1,0:T(8,128)(2,1)}), bf16[16,2,16,256]{3,2,1,0:T(8,128)(2,1)S(1)}, u32[]{:S(2)}, u32[]{:S(2)}) async-start(bf16[16,2,16,256]{3,2,1,0:T(8,128)(2,1)} %down.1), calls=%async_computation.3 | async-start | bytes 524288 | tf_op jit(solution)/shard_map/all_to_all | solution.py:596
  125.6 2.6 %collective-permute-start.24 = (bf16[2,64,256]{2,1,0:T(8,128)(2,1)S(1)}, bf16[2,64,256]{2,1,0:T(8,128)(2,1)S(1)}, u32[]{:S(2)}, u32[]{:S(2)}) collective-permute-start(bf16[2,64,256]{2,1,0:T(8,128)(2,1)S(1)} %get-tuple-element.39), channel_id=1, source_target_pairs={{0,6},{2,8},{4,10},{6,12},{8,14},{10,0},{12,2},{14,4},{1,11},{3,13... | collective-permute-start | bytes 196616 | tf_op jit(solution)/shard_map/ppermute | solution.py:33
  128.2 2.9 %collective-permute-start.25 = (bf16[1,64,256]{2,1,0:T(8,128)(2,1)S(1)}, bf16[1,64,256]{2,1,0:T(8,128)(2,1)S(1)}, u32[]{:S(2)}, u32[]{:S(2)}) collective-permute-start(bf16[1,64,256]{2,1,0:T(8,128)(2,1)S(1)} %slice.33), channel_id=1, source_target_pairs={{0,8},{2,10},{4,12},{6,14},{8,0},{10,2},{12,4},{14,6},{1,9},{3,11}... | collective-permute-start | bytes 98312 | tf_op jit(solution)/shard_map/ppermute | solution.py:33
  132.0 3.6 %collective-permute-done.25.refs_3_ = bf16[1,64,256]{2,1,0:T(8,128)(2,1)S(1)} collective-permute-done((bf16[1,64,256]{2,1,0:T(8,128)(2,1)S(1)}, bf16[1,64,256]{2,1,0:T(8,128)(2,1)S(1)}, u32[]{:S(2)}, u32[]{:S(2)}) %collective-permute-start.25) | collective-permute-done | bytes 32800 | tf_op jit(solution)/shard_map/ppermute | solution.py:33
  135.9 2.5 %collective-permute-start.26 = (bf16[64,256]{1,0:T(8,128)(2,1)S(1)}, bf16[64,256]{1,0:T(8,128)(2,1)S(1)}, u32[]{:S(2)}, u32[]{:S(2)}) collective-permute-start(bf16[64,256]{1,0:T(8,128)(2,1)S(1)} %get-tuple-element.34), channel_id=1, source_target_pairs={{0,1},{1,0},{2,3},{3,2},{4,5},{5,4},{6,7},{7,6},{8,9},{9,8},{10,11... | collective-permute-start | bytes 98312 | tf_op jit(solution)/shard_map/ppermute | solution.py:21
  (88 shorter events, 34.1 us)
Async XLA Ops:
  0.7 49.3 %collective-permute-start.2 = (bf16[4,256,1024]{2,1,0:T(8,128)(2,1)}, bf16[4,256,1024]{2,1,0:T(8,128)(2,1)}, u32[]{:S(2)}, u32[]{:S(2)}) collective-permute-start(bf16[4,256,1024]{2,1,0:T(8,128)(2,1)} %gate.1), channel_id=1, source_target_pairs={{0,1},{1,0},{2,3},{3,2},{4,5},{5,4},{6,7},{7,6},{8,9},{9,8},{10,11... | collective-permute-start | bytes 6291464 | tf_op jit(solution)/shard_map/ppermute | solution.py:21
  3.9 46.0 %collective-permute-start.3 = (bf16[4,256,1024]{2,1,0:T(8,128)(2,1)}, bf16[4,256,1024]{2,1,0:T(8,128)(2,1)}, u32[]{:S(2)}, u32[]{:S(2)}) collective-permute-start(bf16[4,256,1024]{2,1,0:T(8,128)(2,1)} %up.1), channel_id=1, source_target_pairs={{0,1},{1,0},{2,3},{3,2},{4,5},{5,4},{6,7},{7,6},{8,9},{9,8},{10,11... | collective-permute-start | bytes 6291464 | tf_op jit(solution)/shard_map/ppermute | solution.py:21
  8.6 108.5 %collective-permute-start.12 = (bf16[4,1024,256]{2,1,0:T(8,128)(2,1)S(1)}, bf16[4,1024,256]{2,1,0:T(8,128)(2,1)}, u32[]{:S(2)}, u32[]{:S(2)}) collective-permute-start(bf16[4,1024,256]{2,1,0:T(8,128)(2,1)S(1)} %copy-done), channel_id=1, source_target_pairs={{0,1},{1,0},{2,3},{3,2},{4,5},{5,4},{6,7},{7,6},{8,9},{9,8},{10,11... | collective-permute-start | bytes 6291464 | tf_op jit(solution)/shard_map/ppermute | solution.py:21
  13.0 17.6 %all-to-all-start = ((bf16[8,64,256]{2,1,0:T(8,128)(2,1)}), bf16[8,64,256]{2,1,0:T(8,128)(2,1)S(1)}, u32[]{:S(2)}, u32[]{:S(2)}) async-start(bf16[8,64,256]{2,1,0:T(8,128)(2,1)} %add_convert_fusion), calls=%async_computation | async-start | bytes 524288 | tf_op jit(solution)/shard_map/all_to_all | solution.py:553
  35.0 14.9 %all-to-all-start.1 = ((bf16[16,2,16,256]{3,2,1,0:T(8,128)(2,1)}), bf16[16,2,16,256]{3,2,1,0:T(8,128)(2,1)S(1)}, u32[]{:S(2)}, u32[]{:S(2)}) async-start(bf16[16,2,16,256]{3,2,1,0:T(8,128)(2,1)} %dispatch.1), calls=%async_computation.1 | async-start | bytes 524288 | tf_op jit(solution)/shard_map/all_to_all | solution.py:577
  56.2 6.4 %collective-permute-start.4 = (bf16[528,128]{1,0:T(8,128)(2,1)S(1)}, bf16[528,128]{1,0:T(8,128)(2,1)S(1)}, u32[]{:S(2)}, u32[]{:S(2)}) collective-permute-start(bf16[528,128]{1,0:T(8,128)(2,1)S(1)} %get-tuple-element.23), channel_id=1, source_target_pairs={{0,2},{2,4},{4,6},{6,8},{8,10},{10,12},{12,14},{14,0},{1,3},{3,5},... | collective-permute-start | bytes 405512 | tf_op jit(solution)/shard_map/ppermute | solution.py:26
  56.5 6.2 %collective-permute-start.5 = (bf16[528,128]{1,0:T(8,128)(2,1)S(1)}, bf16[528,128]{1,0:T(8,128)(2,1)S(1)}, u32[]{:S(2)}, u32[]{:S(2)}) collective-permute-start(bf16[528,128]{1,0:T(8,128)(2,1)S(1)} %get-tuple-element.24), channel_id=1, source_target_pairs={{0,14},{2,0},{4,2},{6,4},{8,6},{10,8},{12,10},{14,12},{1,15},{3,1}... | collective-permute-start | bytes 405512 | tf_op jit(solution)/shard_map/ppermute | solution.py:26
  58.9 7.9 %collective-permute-start.6 = (bf16[528,128]{1,0:T(8,128)(2,1)S(1)}, bf16[528,128]{1,0:T(8,128)(2,1)S(1)}, u32[]{:S(2)}, u32[]{:S(2)}) collective-permute-start(bf16[528,128]{1,0:T(8,128)(2,1)S(1)} %get-tuple-element.25), channel_id=1, source_target_pairs={{0,4},{2,6},{4,8},{6,10},{8,12},{10,14},{12,0},{14,2},{1,5},{3,7},... | collective-permute-start | bytes 405512 | tf_op jit(solution)/shard_map/ppermute | solution.py:26
  59.2 9.3 %collective-permute-start.7 = (bf16[528,128]{1,0:T(8,128)(2,1)S(1)}, bf16[528,128]{1,0:T(8,128)(2,1)S(1)}, u32[]{:S(2)}, u32[]{:S(2)}) collective-permute-start(bf16[528,128]{1,0:T(8,128)(2,1)S(1)} %get-tuple-element.26), channel_id=1, source_target_pairs={{0,12},{2,14},{4,0},{6,2},{8,4},{10,6},{12,8},{14,10},{1,13},{3,15... | collective-permute-start | bytes 405512 | tf_op jit(solution)/shard_map/ppermute | solution.py:26
  62.6 14.5 %collective-permute-start.11 = (bf16[528,128]{1,0:T(8,128)(2,1)S(1)}, bf16[528,128]{1,0:T(8,128)(2,1)S(1)}, u32[]{:S(2)}, u32[]{:S(2)}) collective-permute-start(bf16[528,128]{1,0:T(8,128)(2,1)S(1)} %add_convert_fusion.1), channel_id=1, source_target_pairs={{0,10},{2,12},{4,14},{6,0},{8,2},{10,4},{12,6},{14,8},{1,11},{3,13... | collective-permute-start | bytes 405512 | tf_op jit(solution)/shard_map/ppermute | solution.py:26
  62.7 14.4 %collective-permute-start.9 = (bf16[528,128]{1,0:T(8,128)(2,1)S(1)}, bf16[528,128]{1,0:T(8,128)(2,1)S(1)}, u32[]{:S(2)}, u32[]{:S(2)}) collective-permute-start(bf16[528,128]{1,0:T(8,128)(2,1)S(1)} %add_convert_fusion.2), channel_id=1, source_target_pairs={{0,6},{2,8},{4,10},{6,12},{8,14},{10,0},{12,2},{14,4},{1,7},{3,9},... | collective-permute-start | bytes 405512 | tf_op jit(solution)/shard_map/ppermute | solution.py:26
  79.4 37.7 %all-to-all-start.2 = ((bf16[8,256,128]{2,1,0:T(8,128)(2,1)}), bf16[8,256,128]{2,1,0:T(8,128)(2,1)S(1)}, u32[]{:S(2)}, u32[]{:S(2)}) async-start(bf16[8,256,128]{2,1,0:T(8,128)(2,1)} %inner.1.refs_12_), calls=%async_computation.2 | async-start | bytes 1048576 | tf_op jit(solution)/shard_map/all_to_all | solution.py:594
  86.1 12.2 %collective-permute-start.13 = (bf16[2,64,256]{2,1,0:T(8,128)(2,1)S(1)}, bf16[2,64,256]{2,1,0:T(8,128)(2,1)S(1)}, u32[]{:S(2)}, u32[]{:S(2)}) collective-permute-start(bf16[2,64,256]{2,1,0:T(8,128)(2,1)S(1)} %pad_maximum_fusion), channel_id=1, source_target_pairs={{0,2},{2,4},{4,6},{6,8},{8,10},{10,12},{12,14},{14,0},{1,15},{3,1}... | collective-permute-start | bytes 196616 | tf_op jit(solution)/shard_map/ppermute | solution.py:33
  88.8 12.0 %collective-permute-start.14 = (bf16[2,64,256]{2,1,0:T(8,128)(2,1)S(1)}, bf16[2,64,256]{2,1,0:T(8,128)(2,1)S(1)}, u32[]{:S(2)}, u32[]{:S(2)}) collective-permute-start(bf16[2,64,256]{2,1,0:T(8,128)(2,1)S(1)} %pad_maximum_fusion), channel_id=1, source_target_pairs={{0,4},{2,6},{4,8},{6,10},{8,12},{10,14},{12,0},{14,2},{1,13},{3,15... | collective-permute-start | bytes 196616 | tf_op jit(solution)/shard_map/ppermute | solution.py:33
  90.9 14.0 %collective-permute-start.15 = (bf16[2,64,256]{2,1,0:T(8,128)(2,1)S(1)}, bf16[2,64,256]{2,1,0:T(8,128)(2,1)S(1)}, u32[]{:S(2)}, u32[]{:S(2)}) collective-permute-start(bf16[2,64,256]{2,1,0:T(8,128)(2,1)S(1)} %pad_maximum_fusion), channel_id=1, source_target_pairs={{0,6},{2,8},{4,10},{6,12},{8,14},{10,0},{12,2},{14,4},{1,11},{3,13... | collective-permute-start | bytes 196616 | tf_op jit(solution)/shard_map/ppermute | solution.py:33
  92.1 15.2 %collective-permute-start.16 = (bf16[1,64,256]{2,1,0:T(8,128)(2,1)S(1)}, bf16[1,64,256]{2,1,0:T(8,128)(2,1)S(1)}, u32[]{:S(2)}, u32[]{:S(2)}) collective-permute-start(bf16[1,64,256]{2,1,0:T(8,128)(2,1)S(1)} %bitcast.32), channel_id=1, source_target_pairs={{0,8},{2,10},{4,12},{6,14},{8,0},{10,2},{12,4},{14,6},{1,9},{3,11}... | collective-permute-start | bytes 98312 | tf_op jit(solution)/shard_map/ppermute | solution.py:33
  98.3 11.8 %collective-permute-start.17 = (bf16[2,64,256]{2,1,0:T(8,128)(2,1)S(1)}, bf16[2,64,256]{2,1,0:T(8,128)(2,1)S(1)}, u32[]{:S(2)}, u32[]{:S(2)}) collective-permute-start(bf16[2,64,256]{2,1,0:T(8,128)(2,1)S(1)} %collective-permute-done.13.refs_0_), channel_id=1, source_target_pairs={{0,1},{1,0},{2,3},{3,2},{4,5},{5,4},{6,7},{7,6},{8,9},{9,8},{10,11... | collective-permute-start | bytes 196616 | tf_op jit(solution)/shard_map/ppermute | solution.py:21
  100.9 9.3 %collective-permute-start.18 = (bf16[2,64,256]{2,1,0:T(8,128)(2,1)S(1)}, bf16[2,64,256]{2,1,0:T(8,128)(2,1)S(1)}, u32[]{:S(2)}, u32[]{:S(2)}) collective-permute-start(bf16[2,64,256]{2,1,0:T(8,128)(2,1)S(1)} %collective-permute-done.14.refs_1_), channel_id=1, source_target_pairs={{0,1},{1,0},{2,3},{3,2},{4,5},{5,4},{6,7},{7,6},{8,9},{9,8},{10,11... | collective-permute-start | bytes 196616 | tf_op jit(solution)/shard_map/ppermute | solution.py:21
  104.9 5.3 %collective-permute-start.19 = (bf16[2,64,256]{2,1,0:T(8,128)(2,1)S(1)}, bf16[2,64,256]{2,1,0:T(8,128)(2,1)S(1)}, u32[]{:S(2)}, u32[]{:S(2)}) collective-permute-start(bf16[2,64,256]{2,1,0:T(8,128)(2,1)S(1)} %collective-permute-done.15.refs_2_), channel_id=1, source_target_pairs={{0,1},{1,0},{2,3},{3,2},{4,5},{5,4},{6,7},{7,6},{8,9},{9,8},{10,11... | collective-permute-start | bytes 196616 | tf_op jit(solution)/shard_map/ppermute | solution.py:21
  120.4 15.3 %all-to-all-start.3 = ((bf16[16,2,16,256]{3,2,1,0:T(8,128)(2,1)}), bf16[16,2,16,256]{3,2,1,0:T(8,128)(2,1)S(1)}, u32[]{:S(2)}, u32[]{:S(2)}) async-start(bf16[16,2,16,256]{3,2,1,0:T(8,128)(2,1)} %down.1), calls=%async_computation.3 | async-start | bytes 524288 | tf_op jit(solution)/shard_map/all_to_all | solution.py:596
  123.9 11.7 %collective-permute-start.22 = (bf16[2,64,256]{2,1,0:T(8,128)(2,1)S(1)}, bf16[2,64,256]{2,1,0:T(8,128)(2,1)S(1)}, u32[]{:S(2)}, u32[]{:S(2)}) collective-permute-start(bf16[2,64,256]{2,1,0:T(8,128)(2,1)S(1)} %get-tuple-element.41), channel_id=1, source_target_pairs={{0,2},{2,4},{4,6},{6,8},{8,10},{10,12},{12,14},{14,0},{1,15},{3,1}... | collective-permute-start | bytes 196616 | tf_op jit(solution)/shard_map/ppermute | solution.py:33
  124.1 11.5 %collective-permute-start.23 = (bf16[2,64,256]{2,1,0:T(8,128)(2,1)S(1)}, bf16[2,64,256]{2,1,0:T(8,128)(2,1)S(1)}, u32[]{:S(2)}, u32[]{:S(2)}) collective-permute-start(bf16[2,64,256]{2,1,0:T(8,128)(2,1)S(1)} %get-tuple-element.40), channel_id=1, source_target_pairs={{0,4},{2,6},{4,8},{6,10},{8,12},{10,14},{12,0},{14,2},{1,13},{3,15... | collective-permute-start | bytes 196616 | tf_op jit(solution)/shard_map/ppermute | solution.py:33
  125.6 10.0 %collective-permute-start.24 = (bf16[2,64,256]{2,1,0:T(8,128)(2,1)S(1)}, bf16[2,64,256]{2,1,0:T(8,128)(2,1)S(1)}, u32[]{:S(2)}, u32[]{:S(2)}) collective-permute-start(bf16[2,64,256]{2,1,0:T(8,128)(2,1)S(1)} %get-tuple-element.39), channel_id=1, source_target_pairs={{0,6},{2,8},{4,10},{6,12},{8,14},{10,0},{12,2},{14,4},{1,11},{3,13... | collective-permute-start | bytes 196616 | tf_op jit(solution)/shard_map/ppermute | solution.py:33
  128.2 7.4 %collective-permute-start.25 = (bf16[1,64,256]{2,1,0:T(8,128)(2,1)S(1)}, bf16[1,64,256]{2,1,0:T(8,128)(2,1)S(1)}, u32[]{:S(2)}, u32[]{:S(2)}) collective-permute-start(bf16[1,64,256]{2,1,0:T(8,128)(2,1)S(1)} %slice.33), channel_id=1, source_target_pairs={{0,8},{2,10},{4,12},{6,14},{8,0},{10,2},{12,4},{14,6},{1,9},{3,11}... | collective-permute-start | bytes 98312 | tf_op jit(solution)/shard_map/ppermute | solution.py:33
  (14 other events, 236.0 us)

commit v4 on v3

--- a/solution.py
+++ b/solution.py
@@ -166,7 +166,7 @@
 def gate_up_kernel(
     at, arrived, gain, gate, gate_par, up, up_par, *refs
 ):
-    *sent, near, far, incoming, weights, parcel, ins, outs = refs
+    *sent, incoming, weights, parcel, ins, outs = refs
     half, _, _, width, _ = weights.shape
     seq_devs, _, pair_slots, _ = incoming.shape
     z_count, _, lanes = parcel.shape
@@ -219,13 +219,16 @@
             sums = sums.astype(BF16)
             depth = (half * m + e) * rows
             put(depth, rows, lambda chip, sums=sums: sums[:, chip * lanes : (chip + 1) * lanes])
-    middle, split = z_count // 2, near.shape[0]
-    store(parcel.at[middle, pl.ds(0, split), :], near)
-    store(parcel.at[middle, pl.ds(split, far.shape[0]), :], far)
-    for steps in range(middle):
-        store(parcel.at[steps], sent[steps])
-    for steps in range(middle + 1, z_count):
-        store(parcel.at[steps], sent[steps - 1])
+    middle, depth = z_count // 2, parcel.shape[1]
+    split = depth // 2
+    targets = [sent[0], *sent[1:middle], None, *sent[middle:]]
+    for steps, target in enumerate(targets):
+        if steps in (1, z_count - 1):
+            first = 0 if steps == 1 else split
+            store(parcel.at[middle, pl.ds(first, split), :], target.at[pl.ds(depth, split), :])
+            target = target.at[pl.ds(0, depth), :]
+        if steps != middle:
+            store(parcel.at[steps], target)
     for copy in stores:
         copy.wait()
 
@@ -236,14 +239,17 @@
     z_count = lax.axis_size("z")
     pair_rows = seq_devs * pair_slots
     parcel = (z_count, 2 * pair_rows + half * 8, units // z_count)
+    long = parcel[1] + parcel[1] // 2
     smem, vmem = pl.BlockSpec(memory_space=pltpu.SMEM), pl.BlockSpec(memory_space=pltpu.VMEM)
     far, any_place = pl.BlockSpec(memory_space=pltpu.HBM), pl.BlockSpec(memory_space=pl.ANY)
     return pl.pallas_call(
         gate_up_kernel,
         in_specs=[smem, any_place, vmem, far, any_place, far, any_place],
-        out_specs=(any_place,) * (z_count + 1),
-        out_shape=(jax.ShapeDtypeStruct(parcel[1:], BF16),) * (z_count - 1)
-        + (jax.ShapeDtypeStruct((parcel[1] // 2, parcel[2]), BF16),) * 2,
+        out_specs=(any_place,) * (z_count - 1),
+        out_shape=tuple(
+            jax.ShapeDtypeStruct((depth, parcel[2]), BF16)
+            for depth in (parcel[1], long, *(parcel[1],) * (z_count - 4), long)
+        ),
         scratch_shapes=[
             pltpu.VMEM(incoming.shape, BF16),
             pltpu.VMEM((half, 2, 2, width, units), BF16),
@@ -299,7 +305,7 @@
         values = returned[:, slot].reshape(rows, width)
         total = dot32(high, values) + dot32(low, values)
         if slot == 0:
-            total = total + base[...]
+            total = total + base[...].astype(F32)
         for part in parts:
             if slot < part.shape[0]:
                 total = total + part[slot].astype(F32)
@@ -365,21 +371,21 @@
             out[i] = dot32(inner, down_t[:, features(steps, place)]).astype(out.dtype)
 
 
-def shared_parts(at, own, par, mine, theirs, gain, gate_t, up_t, w_down, after):
+def shared_parts(at, own, par, mine, theirs, gain, gate_t, up_t, w_down):
     smem, vmem = pl.BlockSpec(memory_space=pltpu.SMEM), pl.BlockSpec(memory_space=pltpu.VMEM)
     (seqs, width), count = own.shape, len(mine)
 
     def kernel(at, own, par, *refs):
         first, second, (gain, *rest) = refs[:count], refs[count : 2 * count], refs[2 * count :]
-        shared_kernel(at, own, par, first, second, gain, rest[:3], *rest[4:])
+        shared_kernel(at, own, par, first, second, gain, rest[:3], *rest[3:])
 
     return pl.pallas_call(
         kernel,
         out_shape=(
-            jax.ShapeDtypeStruct((2 * count, seqs, width), F32),
+            jax.ShapeDtypeStruct((2 * count, seqs, width), BF16),
             jax.ShapeDtypeStruct((2 * count, seqs, width), BF16),
         ),
-        in_specs=[smem] + [vmem] * (2 * count + 3) + [pl.BlockSpec(memory_space=pl.ANY)] * 4,
+        in_specs=[smem] + [vmem] * (2 * count + 3) + [pl.BlockSpec(memory_space=pl.ANY)] * 3,
         out_specs=(vmem, vmem),
         scratch_shapes=[
             pltpu.VMEM(gate_t.shape, BF16),
@@ -390,13 +396,15 @@
         compiler_params=pltpu.CompilerParams(vmem_limit_bytes=FULL),
         cost_estimate=cost(seqs * 6 * w_down.size, 6 * w_down.size),
         name="shared",
-    )(at, own, par, *mine, *theirs, gain, gate_t, up_t, w_down, after)
+    )(at, own, par, *mine, *theirs, gain, gate_t, up_t, w_down)
 
 
 def inner_kernel(model_width, half, *refs):
     *arrived, inner, parcels, arrivals = refs
     copies = [
-        pltpu.make_async_copy(source, parcels.at[i], arrivals.at[i])
+        pltpu.make_async_copy(
+            source.at[pl.ds(0, parcels.shape[1]), :], parcels.at[i], arrivals.at[i]
+        )
         for i, source in enumerate(arrived)
     ]
     for copy in copies:
@@ -579,15 +587,14 @@
     at = jnp.array([1, 1, -1, 0], jnp.int32) * c + jnp.array([0, 2, 2, 1], jnp.int32) * z
     at = at + jnp.array([0, 0, 1, 0], jnp.int32)
     gain = ffn_gain.reshape(1, -1)
-    *sent, near, far = gate_up(at, incoming, gain, expert_gate, gate_par, expert_up, up_par)
-    middle = z_count // 2
+    sent = gate_up(at, incoming, gain, expert_gate, gate_par, expert_up, up_par)
+    middle, depth = z_count // 2, sent[0].shape[0]
     chunks = dict(zip([k for k in range(z_count) if k != middle], sent, strict=True))
-    from_below = moved(near, "z", 1)
-    from_above = moved(far, "z", -1)
-    chunks[middle - 1] = added(chunks[middle - 1], from_below, 0)
-    chunks[middle + 1] = added(chunks[middle + 1], from_above, near.shape[0])
     parcels = [chunks[0]]
     for steps in range(1, middle):
+        if steps == middle - 1:
+            chunks[steps] = added(chunks[steps], parcels[1][depth:], 0)
+            chunks[z_count - steps] = added(chunks[z_count - steps], parcels[2][depth:], depth // 2)
         parcels.append(moved(chunks[steps], "z", steps))
         parcels.append(moved(chunks[z_count - steps], "z", -steps))
     copies = inner_copies(parcels, z_count, model_width, half)
@@ -598,7 +605,10 @@
     held = jnp.stack([resid_own, resid_par])
     mine, theirs = [], []
     for steps in range(1, middle + 1):
-        mine.append(both_ways(held if steps < middle else resid_own[None], steps))
+        if steps < middle:
+            mine.append(both_ways(held, steps))
+        else:
+            mine.append(both_ways(mine[-1][:1], 1))
         theirs.append(swapped(mine[-1]))
     kept, given = shared_parts(
         at,
@@ -610,11 +620,9 @@
         shared_gate.T,
         shared_up.T,
         shared_down,
-        copies,
     )
     got = swapped(given)
-    shared_sums = kept + got.astype(F32)
-    leaving = shared_sums.astype(BF16)
+    leaving = (kept.astype(F32) + got.astype(F32)).astype(BF16)
     shared_chip = []
     for steps in range(1, middle + 1):
         first = 2 * (middle - 1 - steps) if steps < middle else 2 * (middle - 1)
@@ -624,7 +632,7 @@
     weights = route_weight / jnp.sum(route_weight, axis=1, keepdims=True) * ROUTED_SCALE
     chosen = target.reshape(seq_count, top_count)[:, :, None] == slot_ids[None, None, :]
     combine = jnp.sum(jnp.where(chosen, weights[:, :, None], 0.0), axis=1)
-    own, given = combined(combine, returned, shared_sums[-1], shared_chip)
+    own, given = combined(combine, returned, leaving[-1], shared_chip)
     got = swapped(given)
     mixed = (resid_own.astype(F32) + own + got.astype(F32)).astype(BF16)
     return (mixed, new_real, new_imag)

time: 141 us -> 137 us (0.972)
  waiting for transfers between devices: 42.1 us -> 39.8 us
    ppermute x8 -> x6, waiting for transfers between devices: 11.4 us -> 8.15 us  [moved(): lax.ppermute(x, axis, [(i, (i + steps) % count) for i in range(count)])]
    ppermute x11, starting transfers between devices: 19.3 us -> 17.5 us  [swapped(): return lax.ppermute(x, 'c', [(0, 1), (1, 0)])]
    ppermute x8, starting transfers between devices: 16.5 us -> 18 us  [both_ways(): return lax.ppermute(x, TP, ups + downs)]
    ppermute x8 -> x6, starting transfers between devices: 10.9 us -> 10.9 us  [moved(): lax.ppermute(x, axis, [(i, (i + steps) % count) for i in range(count)])]
  transfers between devices with their start and end apart: 31 -> 29, of which waited for: 14 -> 14; matrix products, arithmetic and copies ran while one was open for 5% -> 4% of each run, Pallas kernels for 11% -> 14%
where the time goes in v4:
time: 137 us; the launch traced here: 136 us
  starting transfers between devices  70.1 us (51%)
  waiting for transfers between devices  39.8 us (29%)
  Pallas kernels  18.7 us (14%)
  other arithmetic  5.33 us (4%)
  local copies, waits for them, and re-layouts  1.57 us (1%)
    ppermute x8, starting transfers between devices, both_ways(): return lax.ppermute(x, TP, ups + downs)  18 us
    ppermute x11, starting transfers between devices, swapped(): return lax.ppermute(x, 'c', [(0, 1), (1, 0)])  17.5 us
    ppermute x6, starting transfers between devices, moved(): lax.ppermute(x, axis, [(i, (i + steps) % count) for i in range(count)])  10.9 us
    all_to_all x1, waiting for transfers between devices, local(): lax.all_to_all(both, 'z', split_axis=0, concat_axis=0, tiled=True)  9.9 us
    ppermute x6, waiting for transfers between devices, moved(): lax.ppermute(x, axis, [(i, (i + steps) % count) for i in range(count)])  8.15 us
    all_to_all x1, waiting for transfers between devices, local(): lax.all_to_all(outgoing, 'ep', split_axis=0, concat_axis=0, tiled=True)  8.11 us
    ppermute x8, waiting for transfers between devices, both_ways(): return lax.ppermute(x, TP, ups + downs)  6.98 us
    all_to_all x1, starting transfers between devices, local(): lax.all_to_all(copies, 'z', split_axis=0, concat_axis=0, tiled=True)  6.83 us
  transfers between devices with their start and end apart: 29, of which 14 were waited for; matrix products, arithmetic and copies ran while one was open for 4% of the time, Pallas kernels for 14%

profile of v4, /device:TPU:1, one launch (start us, length us, event | category | flops | bytes accessed | tf_op | source)
XLA Modules:
  0.0 136.5 jit_solution(4195628979397191969)
XLA Ops:
  0.7 3.3 %collective-permute-start.2 = (bf16[4,256,1024]{2,1,0:T(8,128)(2,1)}, bf16[4,256,1024]{2,1,0:T(8,128)(2,1)}, u32[]{:S(2)}, u32[]{:S(2)}) collective-permute-start(bf16[4,256,1024]{2,1,0:T(8,128)(2,1)} %gate.1), channel_id=1, source_target_pairs={{0,1},{1,0},{2,3},{3,2},{4,5},{5,4},{6,7},{7,6},{8,9},{9,8},{10,11... | collective-permute-start | bytes 6291464 | tf_op jit(solution)/shard_map/ppermute | solution.py:21
  4.0 4.0 %front.1 = (f32[64,512]{1,0:T(8,128)}, f32[64,512]{1,0:T(8,128)}, bf16[8,64,256]{2,1,0:T(8,128)(2,1)}, bf16[8,64,256]{2,1,0:T(8,128)(2,1)}) custom-call(s32[1]{0:T(128)} %bitcast.core, f32[8]{0:T(128)} %log_step.1, bf16[64,4096]{1,0:T(8,128)(2,1)} %tokens.1, f32[1,4096]{1,0:T(1,128)} %bitcast.37, bf16[4096,128]{1,0:T(8,128)(2,1)} %w_in.1, ...), custom_call_target="tpu_custom_call" | custom-call | flops 134217728 | bytes 2097152 | tf_op jit(solution)/shard_map/front/pallas_call | solution.py:151
  9.1 2.2 %collective-permute-done = bf16[8,64,256]{2,1,0:T(8,128)(2,1)S(1)} collective-permute-done((bf16[8,64,256]{2,1,0:T(8,128)(2,1)}, bf16[8,64,256]{2,1,0:T(8,128)(2,1)S(1)}, u32[]{:S(2)}, u32[]{:S(2)}) %collective-permute-start) | collective-permute-done | bytes 262176 | tf_op jit(solution)/shard_map/ppermute | solution.py:21
  13.0 6.5 %all-to-all-start = ((bf16[8,64,256]{2,1,0:T(8,128)(2,1)}), bf16[8,64,256]{2,1,0:T(8,128)(2,1)S(1)}, u32[]{:S(2)}, u32[]{:S(2)}) async-start(bf16[8,64,256]{2,1,0:T(8,128)(2,1)} %add_convert_fusion.1), calls=%async_computation | async-start | bytes 524288 | tf_op jit(solution)/shard_map/all_to_all | solution.py:561
  20.7 9.9 %all-to-all-done = bf16[8,64,256]{2,1,0:T(8,128)(2,1)S(1)} async-done(((bf16[8,64,256]{2,1,0:T(8,128)(2,1)}), bf16[8,64,256]{2,1,0:T(8,128)(2,1)S(1)}, u32[]{:S(2)}, u32[]{:S(2)}) %all-to-all-start) | async-done | bytes 262176 | tf_op jit(solution)/shard_map/all_to_all | solution.py:561
  35.0 6.8 %all-to-all-start.1 = ((bf16[16,2,16,256]{3,2,1,0:T(8,128)(2,1)}), bf16[16,2,16,256]{3,2,1,0:T(8,128)(2,1)S(1)}, u32[]{:S(2)}, u32[]{:S(2)}) async-start(bf16[16,2,16,256]{3,2,1,0:T(8,128)(2,1)} %dispatch.1), calls=%async_computation.1 | async-start | bytes 524288 | tf_op jit(solution)/shard_map/all_to_all | solution.py:585
  41.8 8.1 %all-to-all-done.1.arrived = bf16[16,2,16,256]{3,2,1,0:T(8,128)(2,1)S(1)} async-done(((bf16[16,2,16,256]{3,2,1,0:T(8,128)(2,1)}), bf16[16,2,16,256]{3,2,1,0:T(8,128)(2,1)S(1)}, u32[]{:S(2)}, u32[]{:S(2)}) %all-to-all-start.1) | async-done | bytes 262176 | tf_op jit(solution)/shard_map/all_to_all | solution.py:585
  50.0 4.6 %gate_up.1 = (bf16[528,128]{1,0:T(8,128)(2,1)S(1)}, bf16[792,128]{1,0:T(8,128)(2,1)S(1)}, bf16[528,128]{1,0:T(8,128)(2,1)S(1)}, bf16[528,128]{1,0:T(8,128)(2,1)S...) custom-call(s32[4]{0:T(128)S(1)} %add_add_fusion.at, ...), custom_call_target="tpu_custom_call" | custom-call | flops 536870912 | bytes 4194304 | tf_op jit(solution)/shard_map/gate_up/pallas_call | solution.py:245
  54.9 2.4 %collective-permute-start.5 = (bf16[792,128]{1,0:T(8,128)(2,1)S(1)}, bf16[792,128]{1,0:T(8,128)(2,1)S(1)}, u32[]{:S(2)}, u32[]{:S(2)}) collective-permute-start(bf16[792,128]{1,0:T(8,128)(2,1)S(1)} %get-tuple-element.22), channel_id=1, source_target_pairs={{0,14},{2,0},{4,2},{6,4},{8,6},{10,8},{12,10},{14,12},{1,15},{3,1}... | collective-permute-start | bytes 608264 | tf_op jit(solution)/shard_map/ppermute | solution.py:26
  57.3 3.6 %collective-permute-start.7 = (bf16[528,128]{1,0:T(8,128)(2,1)S(1)}, bf16[528,128]{1,0:T(8,128)(2,1)S(1)}, u32[]{:S(2)}, u32[]{:S(2)}) collective-permute-start(bf16[528,128]{1,0:T(8,128)(2,1)S(1)} %get-tuple-element.24), channel_id=1, source_target_pairs={{0,12},{2,14},{4,0},{6,2},{8,4},{10,6},{12,8},{14,10},{1,13},{3,15... | collective-permute-start | bytes 405512 | tf_op jit(solution)/shard_map/ppermute | solution.py:26
  61.2 4.5 %collective-permute-start.9 = (bf16[528,128]{1,0:T(8,128)(2,1)S(1)}, bf16[528,128]{1,0:T(8,128)(2,1)S(1)}, u32[]{:S(2)}, u32[]{:S(2)}) collective-permute-start(bf16[528,128]{1,0:T(8,128)(2,1)S(1)} %add_convert_fusion.2), channel_id=1, source_target_pairs={{0,10},{2,12},{4,14},{6,0},{8,2},{10,4},{12,6},{14,8},{1,11},{3,13... | collective-permute-start | bytes 405512 | tf_op jit(solution)/shard_map/ppermute | solution.py:26
  66.8 4.0 %collective-permute-done.8.refs_5_ = bf16[528,128]{1,0:T(8,128)(2,1)S(1)} collective-permute-done((bf16[528,128]{1,0:T(8,128)(2,1)S(1)}, bf16[528,128]{1,0:T(8,128)(2,1)S(1)}, u32[]{:S(2)}, u32[]{:S(2)}) %collective-permute-start.8) | collective-permute-done | bytes 135200 | tf_op jit(solution)/shard_map/ppermute | solution.py:26
  70.8 2.9 %collective-permute-done.9.refs_6_ = bf16[528,128]{1,0:T(8,128)(2,1)S(1)} collective-permute-done((bf16[528,128]{1,0:T(8,128)(2,1)S(1)}, bf16[528,128]{1,0:T(8,128)(2,1)S(1)}, u32[]{:S(2)}, u32[]{:S(2)}) %collective-permute-start.9) | collective-permute-done | bytes 135200 | tf_op jit(solution)/shard_map/ppermute | solution.py:26
  76.0 6.8 %all-to-all-start.2 = ((bf16[8,256,128]{2,1,0:T(8,128)(2,1)}), bf16[8,256,128]{2,1,0:T(8,128)(2,1)S(1)}, u32[]{:S(2)}, u32[]{:S(2)}) async-start(bf16[8,256,128]{2,1,0:T(8,128)(2,1)} %inner.1), calls=%async_computation.2 | async-start | bytes 1048576 | tf_op jit(solution)/shard_map/all_to_all | solution.py:601
  82.9 4.7 %collective-permute-start.13 = (bf16[2,64,256]{2,1,0:T(8,128)(2,1)S(1)}, bf16[2,64,256]{2,1,0:T(8,128)(2,1)S(1)}, u32[]{:S(2)}, u32[]{:S(2)}) collective-permute-start(bf16[2,64,256]{2,1,0:T(8,128)(2,1)S(1)} %pad_maximum_fusion), channel_id=1, source_target_pairs={{0,6},{2,8},{4,10},{6,12},{8,14},{10,0},{12,2},{14,4},{1,11},{3,13... | collective-permute-start | bytes 196616 | tf_op jit(solution)/shard_map/ppermute | solution.py:33
  89.1 4.6 %collective-permute-done.13.refs_2_ = bf16[2,64,256]{2,1,0:T(8,128)(2,1)S(1)} collective-permute-done((bf16[2,64,256]{2,1,0:T(8,128)(2,1)S(1)}, bf16[2,64,256]{2,1,0:T(8,128)(2,1)S(1)}, u32[]{:S(2)}, u32[]{:S(2)}) %collective-permute-start.13) | collective-permute-done | bytes 65568 | tf_op jit(solution)/shard_map/ppermute | solution.py:33
  93.6 3.2 %collective-permute-start.14 = (bf16[1,64,256]{2,1,0:T(8,128)(2,1)S(1)}, bf16[1,64,256]{2,1,0:T(8,128)(2,1)S(1)}, u32[]{:S(2)}, u32[]{:S(2)}) collective-permute-start(bf16[1,64,256]{2,1,0:T(8,128)(2,1)S(1)} %slice.43), channel_id=1, source_target_pairs={{0,2},{2,4},{4,6},{6,8},{8,10},{10,12},{12,14},{14,0},{1,15},{3,1}... | collective-permute-start | bytes 98312 | tf_op jit(solution)/shard_map/ppermute | solution.py:33
  96.9 5.7 %collective-permute-start.15 = (bf16[2,64,256]{2,1,0:T(8,128)(2,1)S(1)}, bf16[2,64,256]{2,1,0:T(8,128)(2,1)S(1)}, u32[]{:S(2)}, u32[]{:S(2)}) collective-permute-start(bf16[2,64,256]{2,1,0:T(8,128)(2,1)S(1)} %collective-permute-done.11.refs_0_), channel_id=1, source_target_pairs={{0,1},{1,0},{2,3},{3,2},{4,5},{5,4},{6,7},{7,6},{8,9},{9,8},{10,11... | collective-permute-start | bytes 196616 | tf_op jit(solution)/shard_map/ppermute | solution.py:21
  105.8 3.4 %shared.1 = (bf16[8,64,256]{2,1,0:T(8,128)(2,1)S(1)}, bf16[8,64,256]{2,1,0:T(8,128)(2,1)}) custom-call(s32[4]{0:T(128)S(1)} %add_add_fusion.at, bf16[64,256]{1,0:T(8,128)(2,1)S(1)} %add_convert_fusion.5.own_in.own, bf16[64,256]{1,0:T(8,128)(2,1)S(1)} %collective-permute-done.1.par_in.par, bf16[2,64,256]{2,1,0:T(8,128)(2,1)S(1)} %collective-permute-done.11.refs_0_, ...), custom_call_target="tpu_custom_call" | custom-call | flops 100663296 | bytes 1572864 | tf_op jit(solution)/shard_map/shared/pallas_call | solution.py:382
  117.1 3.3 %down.1 = bf16[16,2,16,256]{3,2,1,0:T(8,128)(2,1)} custom-call(s32[4]{0:T(128)S(1)} %add_add_fusion.at, bf16[8,256,128]{2,1,0:T(8,128)(2,1)S(1)} %all-to-all-done.2.arrived, bf16[4,1024,256]{2,1,0:T(8,128)(2,1)S(1)} %copy-done, bf16[4,1024,256]{2,1,0:T(8,128)(2,1)} %collective-permute-done.10.par), custom_call_target="tpu_custom_call" | custom-call | flops 268435456 | bytes 2097152 | tf_op jit(solution)/shard_map/down/pallas_call | solution.py:489
  120.4 3.5 %all-to-all-start.3 = ((bf16[16,2,16,256]{3,2,1,0:T(8,128)(2,1)}), bf16[16,2,16,256]{3,2,1,0:T(8,128)(2,1)S(1)}, u32[]{:S(2)}, u32[]{:S(2)}) async-start(bf16[16,2,16,256]{3,2,1,0:T(8,128)(2,1)} %down.1), calls=%async_computation.3 | async-start | bytes 524288 | tf_op jit(solution)/shard_map/all_to_all | solution.py:603
  124.0 4.2 %collective-permute-start.23 = (bf16[1,64,256]{2,1,0:T(8,128)(2,1)S(1)}, bf16[1,64,256]{2,1,0:T(8,128)(2,1)S(1)}, u32[]{:S(2)}, u32[]{:S(2)}) collective-permute-start(bf16[1,64,256]{2,1,0:T(8,128)(2,1)S(1)} %get-tuple-element.33), channel_id=1, source_target_pairs={{0,8},{2,10},{4,12},{6,14},{8,0},{10,2},{12,4},{14,6},{1,9},{3,11}... | collective-permute-start | bytes 98312 | tf_op jit(solution)/shard_map/ppermute | solution.py:33
  128.3 2.4 %collective-permute-done.23.refs_3_ = bf16[1,64,256]{2,1,0:T(8,128)(2,1)S(1)} collective-permute-done((bf16[1,64,256]{2,1,0:T(8,128)(2,1)S(1)}, bf16[1,64,256]{2,1,0:T(8,128)(2,1)S(1)}, u32[]{:S(2)}, u32[]{:S(2)}) %collective-permute-start.23) | collective-permute-done | bytes 32800 | tf_op jit(solution)/shard_map/ppermute | solution.py:33
  131.7 3.3 %collective-permute-start.24 = (bf16[64,256]{1,0:T(8,128)(2,1)S(1)}, bf16[64,256]{1,0:T(8,128)(2,1)S(1)}, u32[]{:S(2)}, u32[]{:S(2)}) collective-permute-start(bf16[64,256]{1,0:T(8,128)(2,1)S(1)} %get-tuple-element.30), channel_id=1, source_target_pairs={{0,1},{1,0},{2,3},{3,2},{4,5},{5,4},{6,7},{7,6},{8,9},{9,8},{10,11... | collective-permute-start | bytes 98312 | tf_op jit(solution)/shard_map/ppermute | solution.py:21
  (88 shorter events, 27.6 us)
Async XLA Ops:
  0.7 49.3 %collective-permute-start.2 = (bf16[4,256,1024]{2,1,0:T(8,128)(2,1)}, bf16[4,256,1024]{2,1,0:T(8,128)(2,1)}, u32[]{:S(2)}, u32[]{:S(2)}) collective-permute-start(bf16[4,256,1024]{2,1,0:T(8,128)(2,1)} %gate.1), channel_id=1, source_target_pairs={{0,1},{1,0},{2,3},{3,2},{4,5},{5,4},{6,7},{7,6},{8,9},{9,8},{10,11... | collective-permute-start | bytes 6291464 | tf_op jit(solution)/shard_map/ppermute | solution.py:21
  3.9 46.0 %collective-permute-start.3 = (bf16[4,256,1024]{2,1,0:T(8,128)(2,1)}, bf16[4,256,1024]{2,1,0:T(8,128)(2,1)}, u32[]{:S(2)}, u32[]{:S(2)}) collective-permute-start(bf16[4,256,1024]{2,1,0:T(8,128)(2,1)} %up.1), channel_id=1, source_target_pairs={{0,1},{1,0},{2,3},{3,2},{4,5},{5,4},{6,7},{7,6},{8,9},{9,8},{10,11... | collective-permute-start | bytes 6291464 | tf_op jit(solution)/shard_map/ppermute | solution.py:21
  8.1 3.2 %collective-permute-start = (bf16[8,64,256]{2,1,0:T(8,128)(2,1)}, bf16[8,64,256]{2,1,0:T(8,128)(2,1)S(1)}, u32[]{:S(2)}, u32[]{:S(2)}) collective-permute-start(bf16[8,64,256]{2,1,0:T(8,128)(2,1)} %get-tuple-element.19), channel_id=1, source_target_pairs={{0,1},{1,0},{2,3},{3,2},{4,5},{5,4},{6,7},{7,6},{8,9},{9,8},{10,11... | collective-permute-start | bytes 786440 | tf_op jit(solution)/shard_map/ppermute | solution.py:21
  8.6 108.5 %collective-permute-start.10 = (bf16[4,1024,256]{2,1,0:T(8,128)(2,1)S(1)}, bf16[4,1024,256]{2,1,0:T(8,128)(2,1)}, u32[]{:S(2)}, u32[]{:S(2)}) collective-permute-start(bf16[4,1024,256]{2,1,0:T(8,128)(2,1)S(1)} %copy-done), channel_id=1, source_target_pairs={{0,1},{1,0},{2,3},{3,2},{4,5},{5,4},{6,7},{7,6},{8,9},{9,8},{10,11... | collective-permute-start | bytes 6291464 | tf_op jit(solution)/shard_map/ppermute | solution.py:21
  13.0 17.6 %all-to-all-start = ((bf16[8,64,256]{2,1,0:T(8,128)(2,1)}), bf16[8,64,256]{2,1,0:T(8,128)(2,1)S(1)}, u32[]{:S(2)}, u32[]{:S(2)}) async-start(bf16[8,64,256]{2,1,0:T(8,128)(2,1)} %add_convert_fusion.1), calls=%async_computation | async-start | bytes 524288 | tf_op jit(solution)/shard_map/all_to_all | solution.py:561
  35.0 14.9 %all-to-all-start.1 = ((bf16[16,2,16,256]{3,2,1,0:T(8,128)(2,1)}), bf16[16,2,16,256]{3,2,1,0:T(8,128)(2,1)S(1)}, u32[]{:S(2)}, u32[]{:S(2)}) async-start(bf16[16,2,16,256]{3,2,1,0:T(8,128)(2,1)} %dispatch.1), calls=%async_computation.1 | async-start | bytes 524288 | tf_op jit(solution)/shard_map/all_to_all | solution.py:585
  54.6 6.4 %collective-permute-start.4 = (bf16[792,128]{1,0:T(8,128)(2,1)S(1)}, bf16[792,128]{1,0:T(8,128)(2,1)S(1)}, u32[]{:S(2)}, u32[]{:S(2)}) collective-permute-start(bf16[792,128]{1,0:T(8,128)(2,1)S(1)} %get-tuple-element.21), channel_id=1, source_target_pairs={{0,2},{2,4},{4,6},{6,8},{8,10},{10,12},{12,14},{14,0},{1,3},{3,5},... | collective-permute-start | bytes 608264 | tf_op jit(solution)/shard_map/ppermute | solution.py:26
  54.9 6.2 %collective-permute-start.5 = (bf16[792,128]{1,0:T(8,128)(2,1)S(1)}, bf16[792,128]{1,0:T(8,128)(2,1)S(1)}, u32[]{:S(2)}, u32[]{:S(2)}) collective-permute-start(bf16[792,128]{1,0:T(8,128)(2,1)S(1)} %get-tuple-element.22), channel_id=1, source_target_pairs={{0,14},{2,0},{4,2},{6,4},{8,6},{10,8},{12,10},{14,12},{1,15},{3,1}... | collective-permute-start | bytes 608264 | tf_op jit(solution)/shard_map/ppermute | solution.py:26
  57.3 8.4 %collective-permute-start.6 = (bf16[528,128]{1,0:T(8,128)(2,1)S(1)}, bf16[528,128]{1,0:T(8,128)(2,1)S(1)}, u32[]{:S(2)}, u32[]{:S(2)}) collective-permute-start(bf16[528,128]{1,0:T(8,128)(2,1)S(1)} %get-tuple-element.23), channel_id=1, source_target_pairs={{0,4},{2,6},{4,8},{6,10},{8,12},{10,14},{12,0},{14,2},{1,5},{3,7},... | collective-permute-start | bytes 405512 | tf_op jit(solution)/shard_map/ppermute | solution.py:26
  57.3 9.5 %collective-permute-start.7 = (bf16[528,128]{1,0:T(8,128)(2,1)S(1)}, bf16[528,128]{1,0:T(8,128)(2,1)S(1)}, u32[]{:S(2)}, u32[]{:S(2)}) collective-permute-start(bf16[528,128]{1,0:T(8,128)(2,1)S(1)} %get-tuple-element.24), channel_id=1, source_target_pairs={{0,12},{2,14},{4,0},{6,2},{8,4},{10,6},{12,8},{14,10},{1,13},{3,15... | collective-permute-start | bytes 405512 | tf_op jit(solution)/shard_map/ppermute | solution.py:26
  61.0 9.8 %collective-permute-start.8 = (bf16[528,128]{1,0:T(8,128)(2,1)S(1)}, bf16[528,128]{1,0:T(8,128)(2,1)S(1)}, u32[]{:S(2)}, u32[]{:S(2)}) collective-permute-start(bf16[528,128]{1,0:T(8,128)(2,1)S(1)} %add_convert_fusion.3), channel_id=1, source_target_pairs={{0,6},{2,8},{4,10},{6,12},{8,14},{10,0},{12,2},{14,4},{1,7},{3,9},... | collective-permute-start | bytes 405512 | tf_op jit(solution)/shard_map/ppermute | solution.py:26
  61.2 12.6 %collective-permute-start.9 = (bf16[528,128]{1,0:T(8,128)(2,1)S(1)}, bf16[528,128]{1,0:T(8,128)(2,1)S(1)}, u32[]{:S(2)}, u32[]{:S(2)}) collective-permute-start(bf16[528,128]{1,0:T(8,128)(2,1)S(1)} %add_convert_fusion.2), channel_id=1, source_target_pairs={{0,10},{2,12},{4,14},{6,0},{8,2},{10,4},{12,6},{14,8},{1,11},{3,13... | collective-permute-start | bytes 405512 | tf_op jit(solution)/shard_map/ppermute | solution.py:26
  76.0 41.1 %all-to-all-start.2 = ((bf16[8,256,128]{2,1,0:T(8,128)(2,1)}), bf16[8,256,128]{2,1,0:T(8,128)(2,1)S(1)}, u32[]{:S(2)}, u32[]{:S(2)}) async-start(bf16[8,256,128]{2,1,0:T(8,128)(2,1)} %inner.1), calls=%async_computation.2 | async-start | bytes 1048576 | tf_op jit(solution)/shard_map/all_to_all | solution.py:601
  82.9 10.8 %collective-permute-start.13 = (bf16[2,64,256]{2,1,0:T(8,128)(2,1)S(1)}, bf16[2,64,256]{2,1,0:T(8,128)(2,1)S(1)}, u32[]{:S(2)}, u32[]{:S(2)}) collective-permute-start(bf16[2,64,256]{2,1,0:T(8,128)(2,1)S(1)} %pad_maximum_fusion), channel_id=1, source_target_pairs={{0,6},{2,8},{4,10},{6,12},{8,14},{10,0},{12,2},{14,4},{1,11},{3,13... | collective-permute-start | bytes 196616 | tf_op jit(solution)/shard_map/ppermute | solution.py:33
  87.6 9.3 %collective-permute-start.11 = (bf16[2,64,256]{2,1,0:T(8,128)(2,1)S(1)}, bf16[2,64,256]{2,1,0:T(8,128)(2,1)S(1)}, u32[]{:S(2)}, u32[]{:S(2)}) collective-permute-start(bf16[2,64,256]{2,1,0:T(8,128)(2,1)S(1)} %pad_maximum_fusion), channel_id=1, source_target_pairs={{0,2},{2,4},{4,6},{6,8},{8,10},{10,12},{12,14},{14,0},{1,15},{3,1}... | collective-permute-start | bytes 196616 | tf_op jit(solution)/shard_map/ppermute | solution.py:33
  88.8 13.8 %collective-permute-start.12 = (bf16[2,64,256]{2,1,0:T(8,128)(2,1)S(1)}, bf16[2,64,256]{2,1,0:T(8,128)(2,1)S(1)}, u32[]{:S(2)}, u32[]{:S(2)}) collective-permute-start(bf16[2,64,256]{2,1,0:T(8,128)(2,1)S(1)} %pad_maximum_fusion), channel_id=1, source_target_pairs={{0,4},{2,6},{4,8},{6,10},{8,12},{10,14},{12,0},{14,2},{1,13},{3,15... | collective-permute-start | bytes 196616 | tf_op jit(solution)/shard_map/ppermute | solution.py:33
  93.6 9.7 %collective-permute-start.14 = (bf16[1,64,256]{2,1,0:T(8,128)(2,1)S(1)}, bf16[1,64,256]{2,1,0:T(8,128)(2,1)S(1)}, u32[]{:S(2)}, u32[]{:S(2)}) collective-permute-start(bf16[1,64,256]{2,1,0:T(8,128)(2,1)S(1)} %slice.43), channel_id=1, source_target_pairs={{0,2},{2,4},{4,6},{6,8},{8,10},{10,12},{12,14},{14,0},{1,15},{3,1}... | collective-permute-start | bytes 98312 | tf_op jit(solution)/shard_map/ppermute | solution.py:33
  96.9 8.1 %collective-permute-start.15 = (bf16[2,64,256]{2,1,0:T(8,128)(2,1)S(1)}, bf16[2,64,256]{2,1,0:T(8,128)(2,1)S(1)}, u32[]{:S(2)}, u32[]{:S(2)}) collective-permute-start(bf16[2,64,256]{2,1,0:T(8,128)(2,1)S(1)} %collective-permute-done.11.refs_0_), channel_id=1, source_target_pairs={{0,1},{1,0},{2,3},{3,2},{4,5},{5,4},{6,7},{7,6},{8,9},{9,8},{10,11... | collective-permute-start | bytes 196616 | tf_op jit(solution)/shard_map/ppermute | solution.py:21
  112.7 18.0 %collective-permute-start.20 = (bf16[2,64,256]{2,1,0:T(8,128)(2,1)S(1)}, bf16[2,64,256]{2,1,0:T(8,128)(2,1)S(1)}, u32[]{:S(2)}, u32[]{:S(2)}) collective-permute-start(bf16[2,64,256]{2,1,0:T(8,128)(2,1)S(1)} %get-tuple-element.37), channel_id=1, source_target_pairs={{0,2},{2,4},{4,6},{6,8},{8,10},{10,12},{12,14},{14,0},{1,15},{3,1}... | collective-permute-start | bytes 196616 | tf_op jit(solution)/shard_map/ppermute | solution.py:33
  114.2 16.6 %collective-permute-start.21 = (bf16[2,64,256]{2,1,0:T(8,128)(2,1)S(1)}, bf16[2,64,256]{2,1,0:T(8,128)(2,1)S(1)}, u32[]{:S(2)}, u32[]{:S(2)}) collective-permute-start(bf16[2,64,256]{2,1,0:T(8,128)(2,1)S(1)} %get-tuple-element.36), channel_id=1, source_target_pairs={{0,4},{2,6},{4,8},{6,10},{8,12},{10,14},{12,0},{14,2},{1,13},{3,15... | collective-permute-start | bytes 196616 | tf_op jit(solution)/shard_map/ppermute | solution.py:33
  115.7 15.1 %collective-permute-start.22 = (bf16[2,64,256]{2,1,0:T(8,128)(2,1)S(1)}, bf16[2,64,256]{2,1,0:T(8,128)(2,1)S(1)}, u32[]{:S(2)}, u32[]{:S(2)}) collective-permute-start(bf16[2,64,256]{2,1,0:T(8,128)(2,1)S(1)} %get-tuple-element.35), channel_id=1, source_target_pairs={{0,6},{2,8},{4,10},{6,12},{8,14},{10,0},{12,2},{14,4},{1,11},{3,13... | collective-permute-start | bytes 196616 | tf_op jit(solution)/shard_map/ppermute | solution.py:33
  120.4 11.1 %all-to-all-start.3 = ((bf16[16,2,16,256]{3,2,1,0:T(8,128)(2,1)}), bf16[16,2,16,256]{3,2,1,0:T(8,128)(2,1)S(1)}, u32[]{:S(2)}, u32[]{:S(2)}) async-start(bf16[16,2,16,256]{3,2,1,0:T(8,128)(2,1)} %down.1), calls=%async_computation.3 | async-start | bytes 524288 | tf_op jit(solution)/shard_map/all_to_all | solution.py:603
  124.0 6.8 %collective-permute-start.23 = (bf16[1,64,256]{2,1,0:T(8,128)(2,1)S(1)}, bf16[1,64,256]{2,1,0:T(8,128)(2,1)S(1)}, u32[]{:S(2)}, u32[]{:S(2)}) collective-permute-start(bf16[1,64,256]{2,1,0:T(8,128)(2,1)S(1)} %get-tuple-element.33), channel_id=1, source_target_pairs={{0,8},{2,10},{4,12},{6,14},{8,0},{10,2},{12,4},{14,6},{1,9},{3,11}... | collective-permute-start | bytes 98312 | tf_op jit(solution)/shard_map/ppermute | solution.py:33
  131.7 4.1 %collective-permute-start.24 = (bf16[64,256]{1,0:T(8,128)(2,1)S(1)}, bf16[64,256]{1,0:T(8,128)(2,1)S(1)}, u32[]{:S(2)}, u32[]{:S(2)}) collective-permute-start(bf16[64,256]{1,0:T(8,128)(2,1)S(1)} %get-tuple-element.30), channel_id=1, source_target_pairs={{0,1},{1,0},{2,3},{3,2},{4,5},{5,4},{6,7},{7,6},{8,9},{9,8},{10,11... | collective-permute-start | bytes 98312 | tf_op jit(solution)/shard_map/ppermute | solution.py:21
  (13 other events, 206.5 us)

commit v5 on v4

--- a/solution.py
+++ b/solution.py
@@ -33,6 +33,15 @@
     return lax.ppermute(x, TP, ups + downs)
 
 
+def ring_sums(kept, got):
+    sums = (kept.astype(F32) + got.astype(F32)).astype(BF16)
+    middle, arrived = kept.shape[0] // 2, []
+    for steps in range(1, middle + 1):
+        first, count = (2 * (middle - 1 - steps), 2) if steps < middle else (2 * (middle - 1), 1)
+        arrived.append(both_ways(sums[first : first + count], steps))
+    return sums[-1], arrived
+
+
 def added(x, part, first):
     rest = x.shape[0] - first - part.shape[0]
     part = lax.pad(part.astype(F32), jnp.zeros((), F32), ((first, rest, 0), (0, 0, 0)))
@@ -68,8 +77,24 @@
     copy.wait()
 
 
+def along_ring(z, c, chips, width):
+    way = 1 - 2 * c
+
+    def features(steps, place):
+        chip = lax.rem(z + way * steps + 2 * chips, chips)
+        return pl.ds(pl.multiple_of((2 * chip + place) * width, width), width)
+
+    return features
+
+
+def ring_order(chips, first, sign):
+    order = [(sign * k, at) for k in range(chips // 2 - 1, 0, -1) for at in (first, 1 - first)]
+    return [*order, (chips // 2, first), (0, first)]
+
+
 def front_kernel(
     core,
+    chip,
     log_step,
     tokens,
     norm_gain,
@@ -135,14 +160,14 @@
     read = read + skip_gain[...] * drive.astype(F32)
     bent = jnp.tanh(0.7978845608028654 * (read + 0.044715 * (read * read * read)))
     activated = (0.5 * read * (1.0 + bent)).astype(BF16)
-    wide = kept.shape[2]
-    for z in range(kept.shape[0]):
-        for out, c in ((kept, core[0]), (given, 1 - core[0])):
-            at = pl.multiple_of((2 * z + c) * wide, wide)
-            out[z] = dot32(activated, w_out[:, pl.ds(at, wide)]).astype(out.dtype)
-
-
-def front(core, log_step, *arrays):
+    c, chips = core[0], kept.shape[0]
+    features = along_ring(chip[0], c, chips, kept.shape[2])
+    for out, first, sign in ((kept, c, 1), (given, 1 - c, -1)):
+        for i, place in enumerate(ring_order(chips, first, sign)):
+            out[i] = dot32(activated, w_out[:, features(*place)]).astype(out.dtype)
+
+
+def front(core, chip, log_step, *arrays):
     tokens, w_out, state = arrays[0], arrays[-1], arrays[-2]
     seqs, model_width = tokens.shape
     z_count = lax.axis_size("z")
@@ -156,11 +181,11 @@
             jax.ShapeDtypeStruct(part, BF16),
             jax.ShapeDtypeStruct(part, BF16),
         ),
-        in_specs=[smem, smem] + [vmem] * len(arrays),
+        in_specs=[smem] * 3 + [vmem] * len(arrays),
         out_specs=(vmem,) * 4,
         cost_estimate=cost(4 * seqs * model_width * w_out.shape[0], 2 * w_out.size * 2),
         name="front",
-    )(core, log_step, *arrays)
+    )(core, chip, log_step, *arrays)
 
 
 def gate_up_kernel(
@@ -341,12 +366,7 @@
     c, z = at[0], at[3]
     seqs, width = kept.shape[1:]
     chips = gain.shape[1] // (2 * width)
-    way = 1 - 2 * c
-
-    def features(steps, place):
-        chip = lax.rem(z + way * steps + 2 * chips, chips)
-        return pl.ds(pl.multiple_of((2 * chip + place) * width, width), width)
-
+    features = along_ring(z, c, chips, width)
     squares = jnp.zeros((seqs, 1), F32)
     gate = jnp.zeros((seqs, gate_t.shape[0]), F32)
     up = gate
@@ -366,9 +386,8 @@
     gate, up = gate * factor, up * factor
     inner = (gate / (1.0 + jnp.exp(-gate)) * up).astype(BF16)
     for out, first, sign in ((kept, c, 1), (given, 1 - c, -1)):
-        order = [(sign * k, place) for k in range(chips // 2 - 1, 0, -1) for place in (first, 1 - first)]
-        for i, (steps, place) in enumerate([*order, (chips // 2, first), (0, first)]):
-            out[i] = dot32(inner, down_t[:, features(steps, place)]).astype(out.dtype)
+        for i, place in enumerate(ring_order(chips, first, sign)):
+            out[i] = dot32(inner, down_t[:, features(*place)]).astype(out.dtype)
 
 
 def shared_parts(at, own, par, mine, theirs, gain, gate_t, up_t, w_down):
@@ -532,12 +551,13 @@
     seq_count, model_width = tokens.shape
     ep_count, z_count = lax.axis_size("ep"), lax.axis_size("z")
     z, c = lax.axis_index("z"), lax.axis_index("c")
-    core = c.reshape(1)
     slice_width = model_width // (2 * z_count)
     offset = (2 * z + c) * slice_width
+    other_offset = (2 * z + 1 - c) * slice_width
 
     new_real, new_imag, kept, given = front(
-        core,
+        c.reshape(1),
+        z.reshape(1),
         log_step,
         tokens,
         norm_gain.reshape(1, -1),
@@ -554,15 +574,17 @@
         w_out,
     )
     got = swapped(given)
-    both = (kept.astype(F32) + got.astype(F32)).astype(BF16)
+    own_part, parts = ring_sums(kept, got)
 
     gate_par, up_par, down_par = (swapped(w) for w in (expert_gate, expert_up, expert_down))
 
-    mixer_own = lax.all_to_all(both, "z", split_axis=0, concat_axis=0, tiled=True)
-    mixer_own = mixer_own.astype(F32).sum(axis=0)
+    own_sum = own_part.astype(F32) + sum(part[0].astype(F32) for part in parts)
+    other_sum = sum(part[1].astype(F32) for part in parts if part.shape[0] > 1)
+    got = swapped(jnp.stack([own_sum, other_sum]).astype(BF16)).astype(F32)
     own_tokens = lax.dynamic_slice_in_dim(tokens, offset, slice_width, 1)
-    resid_own = (own_tokens.astype(F32) + mixer_own).astype(BF16)
-    resid_par = swapped(resid_own)
+    other_tokens = lax.dynamic_slice_in_dim(tokens, other_offset, slice_width, 1)
+    resid_own = (own_tokens.astype(F32) + (own_sum + got[1])).astype(BF16)
+    resid_par = (other_tokens.astype(F32) + (other_sum + got[0])).astype(BF16)
 
     expert_dev = expert_gate.shape[0]
     half = expert_dev // 2
@@ -622,17 +644,12 @@
         shared_down,
     )
     got = swapped(given)
-    leaving = (kept.astype(F32) + got.astype(F32)).astype(BF16)
-    shared_chip = []
-    for steps in range(1, middle + 1):
-        first = 2 * (middle - 1 - steps) if steps < middle else 2 * (middle - 1)
-        part = leaving[first : first + (2 if steps < middle else 1)]
-        shared_chip.append(both_ways(part, steps))
+    own_part, shared_chip = ring_sums(kept, got)
 
     weights = route_weight / jnp.sum(route_weight, axis=1, keepdims=True) * ROUTED_SCALE
     chosen = target.reshape(seq_count, top_count)[:, :, None] == slot_ids[None, None, :]
     combine = jnp.sum(jnp.where(chosen, weights[:, :, None], 0.0), axis=1)
-    own, given = combined(combine, returned, leaving[-1], shared_chip)
+    own, given = combined(combine, returned, own_part, shared_chip)
     got = swapped(given)
     mixed = (resid_own.astype(F32) + own + got.astype(F32)).astype(BF16)
     return (mixed, new_real, new_imag)

time: 137 us -> 132 us (0.964)
  waiting for transfers between devices: 39.8 us -> 33.6 us
  starting transfers between devices: 70.1 us -> 71.9 us
    ppermute x8 -> x12, starting transfers between devices: 18 us -> 28.3 us  [both_ways(): return lax.ppermute(x, TP, ups + downs)]
    all_to_all x1 -> x0, waiting for transfers between devices: 9.9 us -> none  [local(): lax.all_to_all(both, 'z', split_axis=0, concat_axis=0, tiled=True)]
    all_to_all x1 -> x0, starting transfers between devices: 6.48 us -> none  [local(): lax.all_to_all(both, 'z', split_axis=0, concat_axis=0, tiled=True)]
    ppermute x8 -> x12, waiting for transfers between devices: 6.98 us -> 12.2 us  [both_ways(): return lax.ppermute(x, TP, ups + downs)]
    ppermute x11, waiting for transfers between devices: 5.97 us -> 4.18 us  [swapped(): return lax.ppermute(x, 'c', [(0, 1), (1, 0)])]
    convert_element_type x3 -> x4, other arithmetic: 3.51 us -> 2.88 us  [the longest x2 2.04 us: ring_sums(): sums = (kept.astype(F32) + got.astype(F32)).astype(BF16)]
  transfers between devices with their start and end apart: 29 -> 32, of which waited for: 14 -> 11; matrix products, arithmetic and copies ran while one was open for 4% -> 4% of each run, Pallas kernels for 14% -> 11%
where the time goes in v5:
time: 132 us
  starting transfers between devices  71.9 us (54%)
  waiting for transfers between devices  33.6 us (25%)
  Pallas kernels  18.9 us (14%)
  other arithmetic  4.72 us (4%)
  local copies, waits for them, and re-layouts  1.59 us (1%)
    ppermute x12, starting transfers between devices, both_ways(): return lax.ppermute(x, TP, ups + downs)  28.3 us
    ppermute x11, starting transfers between devices, swapped(): return lax.ppermute(x, 'c', [(0, 1), (1, 0)])  16.2 us
    ppermute x12, waiting for transfers between devices, both_ways(): return lax.ppermute(x, TP, ups + downs)  12.2 us
    ppermute x6, starting transfers between devices, moved(): lax.ppermute(x, axis, [(i, (i + steps) % count) for i in range(count)])  11 us
    all_to_all x1, waiting for transfers between devices, local(): lax.all_to_all(outgoing, 'ep', split_axis=0, concat_axis=0, tiled=True)  8.08 us
    ppermute x6, waiting for transfers between devices, moved(): lax.ppermute(x, axis, [(i, (i + steps) % count) for i in range(count)])  7.51 us
    all_to_all x1, starting transfers between devices, local(): lax.all_to_all(outgoing, 'ep', split_axis=0, concat_axis=0, tiled=True)  6.75 us
    all_to_all x1, starting transfers between devices, local(): lax.all_to_all(copies, 'z', split_axis=0, concat_axis=0, tiled=True)  6.14 us
  transfers between devices with their start and end apart: 32, of which 11 were waited for; matrix products, arithmetic and copies ran while one was open for 4% of the time, Pallas kernels for 11%

profile of v5, /device:TPU:1, one launch (start us, length us, event | category | flops | bytes accessed | tf_op | source)
XLA Modules:
  0.0 131.6 jit_solution(8592261016825553579)
XLA Ops:
  0.7 4.1 %front.1 = (f32[64,512]{1,0:T(8,128)}, f32[64,512]{1,0:T(8,128)}, bf16[8,64,256]{2,1,0:T(8,128)(2,1)}, bf16[8,64,256]{2,1,0:T(8,128)(2,1)}) custom-call(s32[1]{0:T(128)} %bitcast.core, s32[1]{0:T(128)} %bitcast.1.chip, f32[8]{0:T(128)} %log_step.1, bf16[64,4096]{1,0:T(8,128)(2,1)} %tokens.1, f32[1,4096]{1,0:T(1,128)} %bitcast.50, bf16[4096,128]{1,0:T(8,128)(2,1)} %w_in.1, ...), custom_call_target="tpu_custom_call" | custom-call | flops 134217728 | bytes 2097152 | tf_op jit(solution)/shard_map/front/pallas_call | solution.py:176
  4.8 3.3 %collective-permute-start = (bf16[8,64,256]{2,1,0:T(8,128)(2,1)}, bf16[8,64,256]{2,1,0:T(8,128)(2,1)S(1)}, u32[]{:S(2)}, u32[]{:S(2)}) collective-permute-start(bf16[8,64,256]{2,1,0:T(8,128)(2,1)} %get-tuple-element.19), channel_id=1, source_target_pairs={{0,1},{1,0},{2,3},{3,2},{4,5},{5,4},{6,7},{7,6},{8,9},{9,8},{10,11... | collective-permute-start | bytes 786440 | tf_op jit(solution)/shard_map/ppermute | solution.py:21
  11.1 5.3 %collective-permute-start.4 = (bf16[1,64,256]{2,1,0:T(8,128)(2,1)S(1)}, bf16[1,64,256]{2,1,0:T(8,128)(2,1)S(1)}, u32[]{:S(2)}, u32[]{:S(2)}) collective-permute-start(bf16[1,64,256]{2,1,0:T(8,128)(2,1)S(1)} %slice.99), channel_id=1, source_target_pairs={{0,8},{2,10},{4,12},{6,14},{8,0},{10,2},{12,4},{14,6},{1,9},{3,11}... | collective-permute-start | bytes 98312 | tf_op jit(solution)/shard_map/ppermute | solution.py:33
  16.5 4.0 %collective-permute-start.2 = (bf16[2,64,256]{2,1,0:T(8,128)(2,1)S(1)}, bf16[2,64,256]{2,1,0:T(8,128)(2,1)S(1)}, u32[]{:S(2)}, u32[]{:S(2)}) collective-permute-start(bf16[2,64,256]{2,1,0:T(8,128)(2,1)S(1)} %get-tuple-element.42), channel_id=1, source_target_pairs={{0,4},{2,6},{4,8},{6,10},{8,12},{10,14},{12,0},{14,2},{1,13},{3,15... | collective-permute-start | bytes 196616 | tf_op jit(solution)/shard_map/ppermute | solution.py:33
  24.3 2.6 %collective-permute-start.5 = (bf16[2,64,256]{2,1,0:T(8,128)(2,1)S(1)}, bf16[2,64,256]{2,1,0:T(8,128)(2,1)S(1)}, u32[]{:S(2)}, u32[]{:S(2)}) collective-permute-start(bf16[2,64,256]{2,1,0:T(8,128)(2,1)S(1)} %pad_maximum_fusion), channel_id=1, source_target_pairs={{0,1},{1,0},{2,3},{3,2},{4,5},{5,4},{6,7},{7,6},{8,9},{9,8},{10,11... | collective-permute-start | bytes 196616 | tf_op jit(solution)/shard_map/ppermute | solution.py:21
  30.0 6.8 %all-to-all-start = ((bf16[16,2,16,256]{3,2,1,0:T(8,128)(2,1)}), bf16[16,2,16,256]{3,2,1,0:T(8,128)(2,1)S(1)}, u32[]{:S(2)}, u32[]{:S(2)}) async-start(bf16[16,2,16,256]{3,2,1,0:T(8,128)(2,1)} %dispatch.1), calls=%async_computation | async-start | bytes 524288 | tf_op jit(solution)/shard_map/all_to_all | solution.py:607
  36.9 8.1 %all-to-all-done.arrived = bf16[16,2,16,256]{3,2,1,0:T(8,128)(2,1)S(1)} async-done(((bf16[16,2,16,256]{3,2,1,0:T(8,128)(2,1)}), bf16[16,2,16,256]{3,2,1,0:T(8,128)(2,1)S(1)}, u32[]{:S(2)}, u32[]{:S(2)}) %all-to-all-start) | async-done | bytes 262176 | tf_op jit(solution)/shard_map/all_to_all | solution.py:607
  44.9 4.6 %gate_up.1 = (bf16[528,128]{1,0:T(8,128)(2,1)S(1)}, bf16[792,128]{1,0:T(8,128)(2,1)S(1)}, bf16[528,128]{1,0:T(8,128)(2,1)S(1)}, bf16[528,128]{1,0:T(8,128)(2,1)S...) custom-call(s32[4]{0:T(128)S(1)} %add_add_fusion.at, ...), custom_call_target="tpu_custom_call" | custom-call | flops 536870912 | bytes 4194304 | tf_op jit(solution)/shard_map/gate_up/pallas_call | solution.py:270
  58.0 2.6 %collective-permute-start.13 = (bf16[528,128]{1,0:T(8,128)(2,1)S(1)}, bf16[528,128]{1,0:T(8,128)(2,1)S(1)}, u32[]{:S(2)}, u32[]{:S(2)}) collective-permute-start(bf16[528,128]{1,0:T(8,128)(2,1)S(1)} %add_convert_fusion.2), channel_id=1, source_target_pairs={{0,10},{2,12},{4,14},{6,0},{8,2},{10,4},{12,6},{14,8},{1,11},{3,13... | collective-permute-start | bytes 405512 | tf_op jit(solution)/shard_map/ppermute | solution.py:26
  60.6 4.5 %collective-permute-done.11.refs_4_ = bf16[528,128]{1,0:T(8,128)(2,1)S(1)} collective-permute-done((bf16[528,128]{1,0:T(8,128)(2,1)S(1)}, bf16[528,128]{1,0:T(8,128)(2,1)S(1)}, u32[]{:S(2)}, u32[]{:S(2)}) %collective-permute-start.11) | collective-permute-done | bytes 135200 | tf_op jit(solution)/shard_map/ppermute | solution.py:26
  65.1 3.0 %collective-permute-done.12.refs_5_ = bf16[528,128]{1,0:T(8,128)(2,1)S(1)} collective-permute-done((bf16[528,128]{1,0:T(8,128)(2,1)S(1)}, bf16[528,128]{1,0:T(8,128)(2,1)S(1)}, u32[]{:S(2)}, u32[]{:S(2)}) %collective-permute-start.12) | collective-permute-done | bytes 135200 | tf_op jit(solution)/shard_map/ppermute | solution.py:26
  68.1 2.3 %inner.1 = bf16[8,256,128]{2,1,0:T(8,128)(2,1)} custom-call(bf16[528,128]{1,0:T(8,128)(2,1)S(1)} %get-tuple-element.20.refs_0_, bf16[792,128]{1,0:T(8,128)(2,1)S(1)} %collective-permute-done.8.refs_1_, bf16[792,128]{1,0:T(8,128)(2,1)S(1)} %collective-permute-done.9.refs_2_, bf16[528,128]{1,0:T(8,128)(2,1)S(1)} %collective-permute-done.10.refs_3_, ...), custom_call_target="tpu_custom_call" | custom-call | flops 2162688 | bytes 2162688 | tf_op jit(solution)/shard_map/inner/pallas_call | solution.py:455
  70.4 6.1 %all-to-all-start.1 = ((bf16[8,256,128]{2,1,0:T(8,128)(2,1)}), bf16[8,256,128]{2,1,0:T(8,128)(2,1)S(1)}, u32[]{:S(2)}, u32[]{:S(2)}) async-start(bf16[8,256,128]{2,1,0:T(8,128)(2,1)} %inner.1), calls=%async_computation.1 | async-start | bytes 1048576 | tf_op jit(solution)/shard_map/all_to_all | solution.py:623
  76.6 4.5 %collective-permute-start.17 = (bf16[2,64,256]{2,1,0:T(8,128)(2,1)S(1)}, bf16[2,64,256]{2,1,0:T(8,128)(2,1)S(1)}, u32[]{:S(2)}, u32[]{:S(2)}) collective-permute-start(bf16[2,64,256]{2,1,0:T(8,128)(2,1)S(1)} %pad_maximum_fusion.1), channel_id=1, source_target_pairs={{0,6},{2,8},{4,10},{6,12},{8,14},{10,0},{12,2},{14,4},{1,11},{3,13... | collective-permute-start | bytes 196616 | tf_op jit(solution)/shard_map/ppermute | solution.py:33
  82.6 2.7 %collective-permute-done.17.refs_2_ = bf16[2,64,256]{2,1,0:T(8,128)(2,1)S(1)} collective-permute-done((bf16[2,64,256]{2,1,0:T(8,128)(2,1)S(1)}, bf16[2,64,256]{2,1,0:T(8,128)(2,1)S(1)}, u32[]{:S(2)}, u32[]{:S(2)}) %collective-permute-start.17) | collective-permute-done | bytes 65568 | tf_op jit(solution)/shard_map/ppermute | solution.py:33
  85.3 2.9 %collective-permute-start.18 = (bf16[1,64,256]{2,1,0:T(8,128)(2,1)S(1)}, bf16[1,64,256]{2,1,0:T(8,128)(2,1)S(1)}, u32[]{:S(2)}, u32[]{:S(2)}) collective-permute-start(bf16[1,64,256]{2,1,0:T(8,128)(2,1)S(1)} %slice.108), channel_id=1, source_target_pairs={{0,2},{2,4},{4,6},{6,8},{8,10},{10,12},{12,14},{14,0},{1,15},{3,1}... | collective-permute-start | bytes 98312 | tf_op jit(solution)/shard_map/ppermute | solution.py:33
  88.2 5.4 %collective-permute-done.15.refs_0_ = bf16[2,64,256]{2,1,0:T(8,128)(2,1)S(1)} collective-permute-done((bf16[2,64,256]{2,1,0:T(8,128)(2,1)S(1)}, bf16[2,64,256]{2,1,0:T(8,128)(2,1)S(1)}, u32[]{:S(2)}, u32[]{:S(2)}) %collective-permute-start.15) | collective-permute-done | bytes 65568 | tf_op jit(solution)/shard_map/ppermute | solution.py:33
  93.5 3.8 %collective-permute-start.19 = (bf16[2,64,256]{2,1,0:T(8,128)(2,1)S(1)}, bf16[2,64,256]{2,1,0:T(8,128)(2,1)S(1)}, u32[]{:S(2)}, u32[]{:S(2)}) collective-permute-start(bf16[2,64,256]{2,1,0:T(8,128)(2,1)S(1)} %collective-permute-done.15.refs_0_), channel_id=1, source_target_pairs={{0,1},{1,0},{2,3},{3,2},{4,5},{5,4},{6,7},{7,6},{8,9},{9,8},{10,11... | collective-permute-start | bytes 196616 | tf_op jit(solution)/shard_map/ppermute | solution.py:21
  100.4 3.4 %shared.1 = (bf16[8,64,256]{2,1,0:T(8,128)(2,1)S(1)}, bf16[8,64,256]{2,1,0:T(8,128)(2,1)}) custom-call(s32[4]{0:T(128)S(1)} %add_add_fusion.at, bf16[64,256]{1,0:T(8,128)(2,1)S(1)} %get-tuple-element.34.own_in.own, bf16[64,256]{1,0:T(8,128)(2,1)S(1)} %get-tuple-element.33.par_in.par, bf16[2,64,256]{2,1,0:T(8,128)(2,1)S(1)} %collective-permute-done.15.refs_0_, ...), custom_call_target="tpu_custom_call" | custom-call | flops 100663296 | bytes 1572864 | tf_op jit(solution)/shard_map/shared/pallas_call | solution.py:401
  110.3 3.1 %collective-permute-start.26 = (bf16[2,64,256]{2,1,0:T(8,128)(2,1)S(1)}, bf16[2,64,256]{2,1,0:T(8,128)(2,1)S(1)}, u32[]{:S(2)}, u32[]{:S(2)}) collective-permute-start(bf16[2,64,256]{2,1,0:T(8,128)(2,1)S(1)} %get-tuple-element.37), channel_id=1, source_target_pairs={{0,6},{2,8},{4,10},{6,12},{8,14},{10,0},{12,2},{14,4},{1,11},{3,13... | collective-permute-start | bytes 196616 | tf_op jit(solution)/shard_map/ppermute | solution.py:33
  113.4 3.3 %down.1 = bf16[16,2,16,256]{3,2,1,0:T(8,128)(2,1)} custom-call(s32[4]{0:T(128)S(1)} %add_add_fusion.at, bf16[8,256,128]{2,1,0:T(8,128)(2,1)S(1)} %all-to-all-done.1.arrived, bf16[4,1024,256]{2,1,0:T(8,128)(2,1)S(1)} %copy-done, bf16[4,1024,256]{2,1,0:T(8,128)(2,1)} %collective-permute-done.14.par), custom_call_target="tpu_custom_call" | custom-call | flops 268435456 | bytes 2097152 | tf_op jit(solution)/shard_map/down/pallas_call | solution.py:508
  116.6 3.5 %all-to-all-start.2 = ((bf16[16,2,16,256]{3,2,1,0:T(8,128)(2,1)}), bf16[16,2,16,256]{3,2,1,0:T(8,128)(2,1)S(1)}, u32[]{:S(2)}, u32[]{:S(2)}) async-start(bf16[16,2,16,256]{3,2,1,0:T(8,128)(2,1)} %down.1), calls=%async_computation.2 | async-start | bytes 524288 | tf_op jit(solution)/shard_map/all_to_all | solution.py:625
  120.2 2.6 %collective-permute-start.27 = (bf16[1,64,256]{2,1,0:T(8,128)(2,1)S(1)}, bf16[1,64,256]{2,1,0:T(8,128)(2,1)S(1)}, u32[]{:S(2)}, u32[]{:S(2)}) collective-permute-start(bf16[1,64,256]{2,1,0:T(8,128)(2,1)S(1)} %get-tuple-element.35), channel_id=1, source_target_pairs={{0,8},{2,10},{4,12},{6,14},{8,0},{10,2},{12,4},{14,6},{1,9},{3,11}... | collective-permute-start | bytes 98312 | tf_op jit(solution)/shard_map/ppermute | solution.py:33
  122.9 4.1 %collective-permute-done.27.refs_3_ = bf16[1,64,256]{2,1,0:T(8,128)(2,1)S(1)} collective-permute-done((bf16[1,64,256]{2,1,0:T(8,128)(2,1)S(1)}, bf16[1,64,256]{2,1,0:T(8,128)(2,1)S(1)}, u32[]{:S(2)}, u32[]{:S(2)}) %collective-permute-start.27) | collective-permute-done | bytes 32800 | tf_op jit(solution)/shard_map/ppermute | solution.py:33
  (98 shorter events, 34.3 us)
Async XLA Ops:
  8.1 36.8 %collective-permute-start.6 = (bf16[4,256,1024]{2,1,0:T(8,128)(2,1)}, bf16[4,256,1024]{2,1,0:T(8,128)(2,1)}, u32[]{:S(2)}, u32[]{:S(2)}) collective-permute-start(bf16[4,256,1024]{2,1,0:T(8,128)(2,1)} %gate.1), channel_id=1, source_target_pairs={{0,1},{1,0},{2,3},{3,2},{4,5},{5,4},{6,7},{7,6},{8,9},{9,8},{10,11... | collective-permute-start | bytes 6291464 | tf_op jit(solution)/shard_map/ppermute | solution.py:21
  8.2 36.7 %collective-permute-start.7 = (bf16[4,256,1024]{2,1,0:T(8,128)(2,1)}, bf16[4,256,1024]{2,1,0:T(8,128)(2,1)}, u32[]{:S(2)}, u32[]{:S(2)}) collective-permute-start(bf16[4,256,1024]{2,1,0:T(8,128)(2,1)} %up.1), channel_id=1, source_target_pairs={{0,1},{1,0},{2,3},{3,2},{4,5},{5,4},{6,7},{7,6},{8,9},{9,8},{10,11... | collective-permute-start | bytes 6291464 | tf_op jit(solution)/shard_map/ppermute | solution.py:21
  11.1 9.4 %collective-permute-start.4 = (bf16[1,64,256]{2,1,0:T(8,128)(2,1)S(1)}, bf16[1,64,256]{2,1,0:T(8,128)(2,1)S(1)}, u32[]{:S(2)}, u32[]{:S(2)}) collective-permute-start(bf16[1,64,256]{2,1,0:T(8,128)(2,1)S(1)} %slice.99), channel_id=1, source_target_pairs={{0,8},{2,10},{4,12},{6,14},{8,0},{10,2},{12,4},{14,6},{1,9},{3,11}... | collective-permute-start | bytes 98312 | tf_op jit(solution)/shard_map/ppermute | solution.py:33
  16.4 5.7 %collective-permute-start.3 = (bf16[2,64,256]{2,1,0:T(8,128)(2,1)S(1)}, bf16[2,64,256]{2,1,0:T(8,128)(2,1)S(1)}, u32[]{:S(2)}, u32[]{:S(2)}) collective-permute-start(bf16[2,64,256]{2,1,0:T(8,128)(2,1)S(1)} %get-tuple-element.41), channel_id=1, source_target_pairs={{0,6},{2,8},{4,10},{6,12},{8,14},{10,0},{12,2},{14,4},{1,11},{3,13... | collective-permute-start | bytes 196616 | tf_op jit(solution)/shard_map/ppermute | solution.py:33
  16.5 7.8 %collective-permute-start.2 = (bf16[2,64,256]{2,1,0:T(8,128)(2,1)S(1)}, bf16[2,64,256]{2,1,0:T(8,128)(2,1)S(1)}, u32[]{:S(2)}, u32[]{:S(2)}) collective-permute-start(bf16[2,64,256]{2,1,0:T(8,128)(2,1)S(1)} %get-tuple-element.42), channel_id=1, source_target_pairs={{0,4},{2,6},{4,8},{6,10},{8,12},{10,14},{12,0},{14,2},{1,13},{3,15... | collective-permute-start | bytes 196616 | tf_op jit(solution)/shard_map/ppermute | solution.py:33
  22.1 91.3 %collective-permute-start.14 = (bf16[4,1024,256]{2,1,0:T(8,128)(2,1)S(1)}, bf16[4,1024,256]{2,1,0:T(8,128)(2,1)}, u32[]{:S(2)}, u32[]{:S(2)}) collective-permute-start(bf16[4,1024,256]{2,1,0:T(8,128)(2,1)S(1)} %copy-done), channel_id=1, source_target_pairs={{0,1},{1,0},{2,3},{3,2},{4,5},{5,4},{6,7},{7,6},{8,9},{9,8},{10,11... | collective-permute-start | bytes 6291464 | tf_op jit(solution)/shard_map/ppermute | solution.py:21
  30.0 14.9 %all-to-all-start = ((bf16[16,2,16,256]{3,2,1,0:T(8,128)(2,1)}), bf16[16,2,16,256]{3,2,1,0:T(8,128)(2,1)S(1)}, u32[]{:S(2)}, u32[]{:S(2)}) async-start(bf16[16,2,16,256]{3,2,1,0:T(8,128)(2,1)} %dispatch.1), calls=%async_computation | async-start | bytes 524288 | tf_op jit(solution)/shard_map/all_to_all | solution.py:607
  49.6 6.4 %collective-permute-start.8 = (bf16[792,128]{1,0:T(8,128)(2,1)S(1)}, bf16[792,128]{1,0:T(8,128)(2,1)S(1)}, u32[]{:S(2)}, u32[]{:S(2)}) collective-permute-start(bf16[792,128]{1,0:T(8,128)(2,1)S(1)} %get-tuple-element.21), channel_id=1, source_target_pairs={{0,2},{2,4},{4,6},{6,8},{8,10},{10,12},{12,14},{14,0},{1,3},{3,5},... | collective-permute-start | bytes 608264 | tf_op jit(solution)/shard_map/ppermute | solution.py:26
  51.1 6.9 %collective-permute-start.9 = (bf16[792,128]{1,0:T(8,128)(2,1)S(1)}, bf16[792,128]{1,0:T(8,128)(2,1)S(1)}, u32[]{:S(2)}, u32[]{:S(2)}) collective-permute-start(bf16[792,128]{1,0:T(8,128)(2,1)S(1)} %get-tuple-element.22), channel_id=1, source_target_pairs={{0,14},{2,0},{4,2},{6,4},{8,6},{10,8},{12,10},{14,12},{1,15},{3,1}... | collective-permute-start | bytes 608264 | tf_op jit(solution)/shard_map/ppermute | solution.py:26
  52.3 8.3 %collective-permute-start.10 = (bf16[528,128]{1,0:T(8,128)(2,1)S(1)}, bf16[528,128]{1,0:T(8,128)(2,1)S(1)}, u32[]{:S(2)}, u32[]{:S(2)}) collective-permute-start(bf16[528,128]{1,0:T(8,128)(2,1)S(1)} %get-tuple-element.23), channel_id=1, source_target_pairs={{0,4},{2,6},{4,8},{6,10},{8,12},{10,14},{12,0},{14,2},{1,5},{3,7},... | collective-permute-start | bytes 405512 | tf_op jit(solution)/shard_map/ppermute | solution.py:26
  54.3 10.9 %collective-permute-start.11 = (bf16[528,128]{1,0:T(8,128)(2,1)S(1)}, bf16[528,128]{1,0:T(8,128)(2,1)S(1)}, u32[]{:S(2)}, u32[]{:S(2)}) collective-permute-start(bf16[528,128]{1,0:T(8,128)(2,1)S(1)} %get-tuple-element.24), channel_id=1, source_target_pairs={{0,12},{2,14},{4,0},{6,2},{8,4},{10,6},{12,8},{14,10},{1,13},{3,15... | collective-permute-start | bytes 405512 | tf_op jit(solution)/shard_map/ppermute | solution.py:26
  56.0 12.2 %collective-permute-start.12 = (bf16[528,128]{1,0:T(8,128)(2,1)S(1)}, bf16[528,128]{1,0:T(8,128)(2,1)S(1)}, u32[]{:S(2)}, u32[]{:S(2)}) collective-permute-start(bf16[528,128]{1,0:T(8,128)(2,1)S(1)} %add_convert_fusion.3), channel_id=1, source_target_pairs={{0,6},{2,8},{4,10},{6,12},{8,14},{10,0},{12,2},{14,4},{1,7},{3,9},... | collective-permute-start | bytes 405512 | tf_op jit(solution)/shard_map/ppermute | solution.py:26
  58.0 10.1 %collective-permute-start.13 = (bf16[528,128]{1,0:T(8,128)(2,1)S(1)}, bf16[528,128]{1,0:T(8,128)(2,1)S(1)}, u32[]{:S(2)}, u32[]{:S(2)}) collective-permute-start(bf16[528,128]{1,0:T(8,128)(2,1)S(1)} %add_convert_fusion.2), channel_id=1, source_target_pairs={{0,10},{2,12},{4,14},{6,0},{8,2},{10,4},{12,6},{14,8},{1,11},{3,13... | collective-permute-start | bytes 405512 | tf_op jit(solution)/shard_map/ppermute | solution.py:26
  70.4 43.0 %all-to-all-start.1 = ((bf16[8,256,128]{2,1,0:T(8,128)(2,1)}), bf16[8,256,128]{2,1,0:T(8,128)(2,1)S(1)}, u32[]{:S(2)}, u32[]{:S(2)}) async-start(bf16[8,256,128]{2,1,0:T(8,128)(2,1)} %inner.1), calls=%async_computation.1 | async-start | bytes 1048576 | tf_op jit(solution)/shard_map/all_to_all | solution.py:623
  76.6 8.7 %collective-permute-start.17 = (bf16[2,64,256]{2,1,0:T(8,128)(2,1)S(1)}, bf16[2,64,256]{2,1,0:T(8,128)(2,1)S(1)}, u32[]{:S(2)}, u32[]{:S(2)}) collective-permute-start(bf16[2,64,256]{2,1,0:T(8,128)(2,1)S(1)} %pad_maximum_fusion.1), channel_id=1, source_target_pairs={{0,6},{2,8},{4,10},{6,12},{8,14},{10,0},{12,2},{14,4},{1,11},{3,13... | collective-permute-start | bytes 196616 | tf_op jit(solution)/shard_map/ppermute | solution.py:33
  81.1 12.4 %collective-permute-start.15 = (bf16[2,64,256]{2,1,0:T(8,128)(2,1)S(1)}, bf16[2,64,256]{2,1,0:T(8,128)(2,1)S(1)}, u32[]{:S(2)}, u32[]{:S(2)}) collective-permute-start(bf16[2,64,256]{2,1,0:T(8,128)(2,1)S(1)} %pad_maximum_fusion.1), channel_id=1, source_target_pairs={{0,2},{2,4},{4,6},{6,8},{8,10},{10,12},{12,14},{14,0},{1,15},{3,1}... | collective-permute-start | bytes 196616 | tf_op jit(solution)/shard_map/ppermute | solution.py:33
  82.3 15.0 %collective-permute-start.16 = (bf16[2,64,256]{2,1,0:T(8,128)(2,1)S(1)}, bf16[2,64,256]{2,1,0:T(8,128)(2,1)S(1)}, u32[]{:S(2)}, u32[]{:S(2)}) collective-permute-start(bf16[2,64,256]{2,1,0:T(8,128)(2,1)S(1)} %pad_maximum_fusion.1), channel_id=1, source_target_pairs={{0,4},{2,6},{4,8},{6,10},{8,12},{10,14},{12,0},{14,2},{1,13},{3,15... | collective-permute-start | bytes 196616 | tf_op jit(solution)/shard_map/ppermute | solution.py:33
  85.3 12.8 %collective-permute-start.18 = (bf16[1,64,256]{2,1,0:T(8,128)(2,1)S(1)}, bf16[1,64,256]{2,1,0:T(8,128)(2,1)S(1)}, u32[]{:S(2)}, u32[]{:S(2)}) collective-permute-start(bf16[1,64,256]{2,1,0:T(8,128)(2,1)S(1)} %slice.108), channel_id=1, source_target_pairs={{0,2},{2,4},{4,6},{6,8},{8,10},{10,12},{12,14},{14,0},{1,15},{3,1}... | collective-permute-start | bytes 98312 | tf_op jit(solution)/shard_map/ppermute | solution.py:33
  93.5 6.0 %collective-permute-start.19 = (bf16[2,64,256]{2,1,0:T(8,128)(2,1)S(1)}, bf16[2,64,256]{2,1,0:T(8,128)(2,1)S(1)}, u32[]{:S(2)}, u32[]{:S(2)}) collective-permute-start(bf16[2,64,256]{2,1,0:T(8,128)(2,1)S(1)} %collective-permute-done.15.refs_0_), channel_id=1, source_target_pairs={{0,1},{1,0},{2,3},{3,2},{4,5},{5,4},{6,7},{7,6},{8,9},{9,8},{10,11... | collective-permute-start | bytes 196616 | tf_op jit(solution)/shard_map/ppermute | solution.py:21
  107.4 19.6 %collective-permute-start.24 = (bf16[2,64,256]{2,1,0:T(8,128)(2,1)S(1)}, bf16[2,64,256]{2,1,0:T(8,128)(2,1)S(1)}, u32[]{:S(2)}, u32[]{:S(2)}) collective-permute-start(bf16[2,64,256]{2,1,0:T(8,128)(2,1)S(1)} %get-tuple-element.39), channel_id=1, source_target_pairs={{0,2},{2,4},{4,6},{6,8},{8,10},{10,12},{12,14},{14,0},{1,15},{3,1}... | collective-permute-start | bytes 196616 | tf_op jit(solution)/shard_map/ppermute | solution.py:33
  108.9 18.0 %collective-permute-start.25 = (bf16[2,64,256]{2,1,0:T(8,128)(2,1)S(1)}, bf16[2,64,256]{2,1,0:T(8,128)(2,1)S(1)}, u32[]{:S(2)}, u32[]{:S(2)}) collective-permute-start(bf16[2,64,256]{2,1,0:T(8,128)(2,1)S(1)} %get-tuple-element.38), channel_id=1, source_target_pairs={{0,4},{2,6},{4,8},{6,10},{8,12},{10,14},{12,0},{14,2},{1,13},{3,15... | collective-permute-start | bytes 196616 | tf_op jit(solution)/shard_map/ppermute | solution.py:33
  110.3 16.7 %collective-permute-start.26 = (bf16[2,64,256]{2,1,0:T(8,128)(2,1)S(1)}, bf16[2,64,256]{2,1,0:T(8,128)(2,1)S(1)}, u32[]{:S(2)}, u32[]{:S(2)}) collective-permute-start(bf16[2,64,256]{2,1,0:T(8,128)(2,1)S(1)} %get-tuple-element.37), channel_id=1, source_target_pairs={{0,6},{2,8},{4,10},{6,12},{8,14},{10,0},{12,2},{14,4},{1,11},{3,13... | collective-permute-start | bytes 196616 | tf_op jit(solution)/shard_map/ppermute | solution.py:33
  116.6 11.9 %all-to-all-start.2 = ((bf16[16,2,16,256]{3,2,1,0:T(8,128)(2,1)}), bf16[16,2,16,256]{3,2,1,0:T(8,128)(2,1)S(1)}, u32[]{:S(2)}, u32[]{:S(2)}) async-start(bf16[16,2,16,256]{3,2,1,0:T(8,128)(2,1)} %down.1), calls=%async_computation.2 | async-start | bytes 524288 | tf_op jit(solution)/shard_map/all_to_all | solution.py:625
  120.2 6.8 %collective-permute-start.27 = (bf16[1,64,256]{2,1,0:T(8,128)(2,1)S(1)}, bf16[1,64,256]{2,1,0:T(8,128)(2,1)S(1)}, u32[]{:S(2)}, u32[]{:S(2)}) collective-permute-start(bf16[1,64,256]{2,1,0:T(8,128)(2,1)S(1)} %get-tuple-element.35), channel_id=1, source_target_pairs={{0,8},{2,10},{4,12},{6,14},{8,0},{10,2},{12,4},{14,6},{1,9},{3,11}... | collective-permute-start | bytes 98312 | tf_op jit(solution)/shard_map/ppermute | solution.py:33
  (16 other events, 225.0 us)

commit v6 on v5

--- a/solution.py
+++ b/solution.py
@@ -434,7 +434,7 @@
     for i in range(1, len(copies)):
         totals = totals + parcels[i].astype(F32)
     lanes = totals.shape[1]
-    z_count, pair_rows, _ = inner.shape
+    pair_rows = inner.shape[0]
     rows = pair_rows // half
     for e in range(half):
         line = 2 * pair_rows + 8 * e
@@ -443,18 +443,16 @@
         factor = jnp.broadcast_to(factor, (lanes, rows)).T
         gate = totals[e * rows : (e + 1) * rows] * factor
         up = totals[pair_rows + e * rows : pair_rows + (e + 1) * rows] * factor
-        done = (gate / (1.0 + jnp.exp(-gate)) * up).astype(BF16)
-        for z in range(z_count):
-            inner[z, e * rows : (e + 1) * rows, :] = done
-
-
-def inner_copies(parcels, z_count, model_width, half):
+        inner[e * rows : (e + 1) * rows, :] = (gate / (1.0 + jnp.exp(-gate)) * up).astype(BF16)
+
+
+def inner_rows(parcels, model_width, half):
     depth, lanes = parcels[0].shape
     pair_rows = (depth - half * 8) // 2
     count = len(parcels)
     return pl.pallas_call(
         functools.partial(inner_kernel, model_width, half),
-        out_shape=jax.ShapeDtypeStruct((z_count, pair_rows, lanes), BF16),
+        out_shape=jax.ShapeDtypeStruct((pair_rows, lanes), BF16),
         in_specs=[pl.BlockSpec(memory_space=pl.ANY)] * count,
         out_specs=pl.BlockSpec(memory_space=pltpu.VMEM),
         scratch_shapes=[
@@ -467,25 +465,37 @@
     )(*parcels)
 
 
-def down_kernel(at, arrived, own, par, sent, inner, weights, results, ins, outs):
-    half = weights.shape[0]
-    first = pltpu.make_async_copy(arrived, inner, ins.at[0])
-    first.start()
+def down_kernel(at, mine, gathered, crossed, opposite, own, par, sent, *scratch):
+    inner, weights, results, ins, outs = scratch
+    half, lanes, chips = weights.shape[0], mine.shape[1], inner.shape[1] // mine.shape[1]
+    way = 1 - 2 * at[0]
+    pieces = [(mine, 0), (opposite, chips // 2)]
+    for k, (piece, crossing) in enumerate(zip(gathered, crossed, strict=True)):
+        pieces += [(piece.at[0], -(k + 1)), (crossing, k + 1)]
+    arriving = []
+    for i, (source, steps) in enumerate(pieces):
+        chip = lax.rem(at[3] + way * steps + 2 * chips, chips)
+        place = pl.ds(pl.multiple_of(chip * lanes, lanes), lanes)
+        copy = pltpu.make_async_copy(source, inner.at[:, place], ins.at[i])
+        copy.start()
+        arriving.append(copy)
     loads = []
     for e in range(half):
-        for part, source in enumerate((own.at[half * at[0] + e], par.at[half * at[0] + e])):
-            arrival = ins.at[1 + 2 * e + part]
-            copy = pltpu.make_async_copy(source, weights.at[e, part], arrival)
+        for part, source in enumerate((own, par)):
+            arrival = ins.at[chips + 2 * e + part]
+            copy = pltpu.make_async_copy(
+                source.at[half * at[0] + e], weights.at[e, part], arrival
+            )
             copy.start()
             loads.append(copy)
-    first.wait()
-    rows = inner.shape[1] // half
+    for copy in arriving:
+        copy.wait()
+    rows = inner.shape[0] // half
     seq_devs, _, pair_slots, width = results.shape
     capacity = pair_slots // half
     stores = []
     for e in range(half):
-        row = [inner[z, e * rows : (e + 1) * rows, :] for z in range(inner.shape[0])]
-        row = jnp.concatenate(row, axis=1)
+        row = inner[e * rows : (e + 1) * rows, :]
         place = slice(e * capacity, (e + 1) * capacity)
         for part in range(2):
             loads[2 * e + part].wait()
@@ -501,26 +511,32 @@
         copy.wait()
 
 
-def down(at, inner, w_down, w_par, seq_devs, capacity):
+def down(at, mine, gathered, crossed, opposite, w_down, w_par, seq_devs, capacity):
     half, units, width = w_par.shape[0] // 2, *w_par.shape[1:]
     results = (seq_devs, 2, half * capacity, width)
     smem, any_place = pl.BlockSpec(memory_space=pltpu.SMEM), pl.BlockSpec(memory_space=pl.ANY)
+    count = len(gathered)
+
+    def kernel(at, mine, *refs):
+        first, second, rest = refs[:count], refs[count : 2 * count], refs[2 * count :]
+        down_kernel(at, mine, first, second, *rest)
+
     return pl.pallas_call(
-        down_kernel,
-        in_specs=[smem, any_place, any_place, any_place],
+        kernel,
+        in_specs=[smem] + [any_place] * (2 * count + 4),
         out_specs=pl.BlockSpec(memory_space=pltpu.HBM),
         out_shape=pltpu.HBM(results, BF16),
         scratch_shapes=[
-            pltpu.VMEM(inner.shape, BF16),
+            pltpu.VMEM((mine.shape[0], units), BF16),
             pltpu.VMEM((half, 2, units, width), BF16),
             pltpu.VMEM(results, BF16),
-            pltpu.SemaphoreType.DMA((1 + 2 * half,)),
+            pltpu.SemaphoreType.DMA((2 * count + 2 + 2 * half,)),
             pltpu.SemaphoreType.DMA((half,)),
         ],
         compiler_params=ROOM,
-        cost_estimate=cost(4 * inner.shape[1] * units * width, 4 * half * units * width),
+        cost_estimate=cost(4 * mine.shape[0] * units * width, 4 * half * units * width),
         name="down",
-    )(at, inner, w_down, w_par)
+    )(at, mine, *gathered, *crossed, opposite, w_down, w_par)
 
 
 def local(
@@ -619,9 +635,24 @@
             chunks[z_count - steps] = added(chunks[z_count - steps], parcels[2][depth:], depth // 2)
         parcels.append(moved(chunks[steps], "z", steps))
         parcels.append(moved(chunks[z_count - steps], "z", -steps))
-    copies = inner_copies(parcels, z_count, model_width, half)
-    inner_all = lax.all_to_all(copies, "z", split_axis=0, concat_axis=0, tiled=True)
-    results = down(at, inner_all, expert_down, down_par, ep_count, capacity)
+    inner_mine = inner_rows(parcels, model_width, half)
+    inner_held = jnp.stack([inner_mine, swapped(inner_mine)])
+    gathered, crossed = [], []
+    for steps in range(1, middle):
+        gathered.append(both_ways(inner_held, steps))
+        crossed.append(swapped(gathered[-1][1]))
+    opposite = both_ways(gathered[-1][0], 1)
+    results = down(
+        at,
+        inner_mine,
+        gathered,
+        crossed,
+        opposite,
+        expert_down,
+        down_par,
+        ep_count,
+        capacity,
+    )
     returned = lax.all_to_all(results, "ep", split_axis=0, concat_axis=0, tiled=True)
 
     held = jnp.stack([resid_own, resid_par])

time: 132 us -> 133 us (level)
  waiting for transfers between devices: 33.6 us -> 25.7 us
  starting transfers between devices: 71.9 us -> 76.3 us
  local copies, waits for them, and re-layouts: 1.59 us -> 5.94 us
    ppermute x12 -> x16, starting transfers between devices: 28.3 us -> 35.1 us  [both_ways(): return lax.ppermute(x, TP, ups + downs)]
    ppermute x6, waiting for transfers between devices: 7.51 us -> 0.95 us  [moved(): lax.ppermute(x, axis, [(i, (i + steps) % count) for i in range(count)])]
    all_to_all x1 -> x0, starting transfers between devices: 6.14 us -> none  [local(): lax.all_to_all(copies, 'z', split_axis=0, concat_axis=0, tiled=True)]
    unnamed x17 -> x33, local copies, waits for them, and re-layouts: 0.85 us -> 5.18 us
    ppermute x11 -> x15, starting transfers between devices: 16.2 us -> 20 us  [swapped(): return lax.ppermute(x, 'c', [(0, 1), (1, 0)])]
    ppermute x11 -> x15, waiting for transfers between devices: 4.18 us -> 2.47 us  [swapped(): return lax.ppermute(x, 'c', [(0, 1), (1, 0)])]
    ppermute x12 -> x16, waiting for transfers between devices: 12.2 us -> 13 us  [both_ways(): return lax.ppermute(x, TP, ups + downs)]
  transfers between devices with their start and end apart: 32 -> 39, of which waited for: 11 -> 11; matrix products, arithmetic and copies ran while one was open for 4% -> 4% of each run, Pallas kernels for 11% -> 7%
where the time goes in v6:
time: 133 us; the launch traced here: 132 us
  starting transfers between devices  76.3 us (57%)
  waiting for transfers between devices  25.7 us (19%)
  Pallas kernels  18.3 us (14%)
  local copies, waits for them, and re-layouts  5.94 us (4%)
  other arithmetic  5.08 us (4%)
    ppermute x16, starting transfers between devices, both_ways(): return lax.ppermute(x, TP, ups + downs)  35.1 us
    ppermute x15, starting transfers between devices, swapped(): return lax.ppermute(x, 'c', [(0, 1), (1, 0)])  20 us
    ppermute x16, waiting for transfers between devices, both_ways(): return lax.ppermute(x, TP, ups + downs)  13 us
    ppermute x6, starting transfers between devices, moved(): lax.ppermute(x, axis, [(i, (i + steps) % count) for i in range(count)])  10.8 us
    all_to_all x1, waiting for transfers between devices, local(): lax.all_to_all(outgoing, 'ep', split_axis=0, concat_axis=0, tiled=True)  8.09 us
    all_to_all x1, starting transfers between devices, local(): lax.all_to_all(outgoing, 'ep', split_axis=0, concat_axis=0, tiled=True)  6.77 us
    unnamed x33, local copies, waits for them, and re-layouts  5.18 us
    pallas_call x1, Pallas kernels, gate_up(): pl.pallas_call(gate_up_kernel, in_specs=[smem, any_place, vmem, far, any_...  4.71 us
  transfers between devices with their start and end apart: 39, of which 11 were waited for; matrix products, arithmetic and copies ran while one was open for 4% of the time, Pallas kernels for 7%

profile of v6, /device:TPU:1, one launch (start us, length us, event | category | flops | bytes accessed | tf_op | source)
XLA Modules:
  0.0 132.2 jit_solution(16145724112124813973)
XLA Ops:
  0.7 4.0 %front.1 = (f32[64,512]{1,0:T(8,128)}, f32[64,512]{1,0:T(8,128)}, bf16[8,64,256]{2,1,0:T(8,128)(2,1)}, bf16[8,64,256]{2,1,0:T(8,128)(2,1)}) custom-call(s32[1]{0:T(128)} %bitcast.core, s32[1]{0:T(128)} %bitcast.1.chip, f32[8]{0:T(128)} %log_step.1, bf16[64,4096]{1,0:T(8,128)(2,1)} %tokens.1, f32[1,4096]{1,0:T(1,128)} %bitcast.62, bf16[4096,128]{1,0:T(8,128)(2,1)} %w_in.1, ...), custom_call_target="tpu_custom_call" | custom-call | flops 134217728 | bytes 2097152 | tf_op jit(solution)/shard_map/front/pallas_call | solution.py:176
  4.7 3.3 %collective-permute-start = (bf16[8,64,256]{2,1,0:T(8,128)(2,1)}, bf16[8,64,256]{2,1,0:T(8,128)(2,1)S(1)}, u32[]{:S(2)}, u32[]{:S(2)}) collective-permute-start(bf16[8,64,256]{2,1,0:T(8,128)(2,1)} %get-tuple-element.19), channel_id=1, source_target_pairs={{0,1},{1,0},{2,3},{3,2},{4,5},{5,4},{6,7},{7,6},{8,9},{9,8},{10,11... | collective-permute-start | bytes 786440 | tf_op jit(solution)/shard_map/ppermute | solution.py:21
  10.9 5.3 %collective-permute-start.4 = (bf16[1,64,256]{2,1,0:T(8,128)(2,1)S(1)}, bf16[1,64,256]{2,1,0:T(8,128)(2,1)S(1)}, u32[]{:S(2)}, u32[]{:S(2)}) collective-permute-start(bf16[1,64,256]{2,1,0:T(8,128)(2,1)S(1)} %slice.115), channel_id=1, source_target_pairs={{0,8},{2,10},{4,12},{6,14},{8,0},{10,2},{12,4},{14,6},{1,9},{3,11}... | collective-permute-start | bytes 98312 | tf_op jit(solution)/shard_map/ppermute | solution.py:33
  16.3 4.0 %collective-permute-start.2 = (bf16[2,64,256]{2,1,0:T(8,128)(2,1)S(1)}, bf16[2,64,256]{2,1,0:T(8,128)(2,1)S(1)}, u32[]{:S(2)}, u32[]{:S(2)}) collective-permute-start(bf16[2,64,256]{2,1,0:T(8,128)(2,1)S(1)} %get-tuple-element.42), channel_id=1, source_target_pairs={{0,4},{2,6},{4,8},{6,10},{8,12},{10,14},{12,0},{14,2},{1,13},{3,15... | collective-permute-start | bytes 196616 | tf_op jit(solution)/shard_map/ppermute | solution.py:33
  23.9 2.8 %collective-permute-start.5 = (bf16[2,64,256]{2,1,0:T(8,128)(2,1)S(1)}, bf16[2,64,256]{2,1,0:T(8,128)(2,1)S(1)}, u32[]{:S(2)}, u32[]{:S(2)}) collective-permute-start(bf16[2,64,256]{2,1,0:T(8,128)(2,1)S(1)} %pad_maximum_fusion.1), channel_id=1, source_target_pairs={{0,1},{1,0},{2,3},{3,2},{4,5},{5,4},{6,7},{7,6},{8,9},{9,8},{10,11... | collective-permute-start | bytes 196616 | tf_op jit(solution)/shard_map/ppermute | solution.py:21
  29.5 6.8 %all-to-all-start = ((bf16[16,2,16,256]{3,2,1,0:T(8,128)(2,1)}), bf16[16,2,16,256]{3,2,1,0:T(8,128)(2,1)S(1)}, u32[]{:S(2)}, u32[]{:S(2)}) async-start(bf16[16,2,16,256]{3,2,1,0:T(8,128)(2,1)} %dispatch.1), calls=%async_computation | async-start | bytes 524288 | tf_op jit(solution)/shard_map/all_to_all | solution.py:623
  36.3 8.1 %all-to-all-done.arrived = bf16[16,2,16,256]{3,2,1,0:T(8,128)(2,1)S(1)} async-done(((bf16[16,2,16,256]{3,2,1,0:T(8,128)(2,1)}), bf16[16,2,16,256]{3,2,1,0:T(8,128)(2,1)S(1)}, u32[]{:S(2)}, u32[]{:S(2)}) %all-to-all-start) | async-done | bytes 262176 | tf_op jit(solution)/shard_map/all_to_all | solution.py:623
  44.5 4.7 %gate_up.1 = (bf16[528,128]{1,0:T(8,128)(2,1)S(1)}, bf16[792,128]{1,0:T(8,128)(2,1)S(1)}, bf16[528,128]{1,0:T(8,128)(2,1)}, bf16[528,128]{1,0:T(8,128)(2,1)S(1)}...) custom-call(s32[4]{0:T(128)S(1)} %add_add_fusion.at, ...), custom_call_target="tpu_custom_call" | custom-call | flops 536870912 | bytes 4194304 | tf_op jit(solution)/shard_map/gate_up/pallas_call | solution.py:270
  52.0 3.1 %collective-permute-start.25 = (bf16[2,64,256]{2,1,0:T(8,128)(2,1)S(1)}, bf16[2,64,256]{2,1,0:T(8,128)(2,1)S(1)}, u32[]{:S(2)}, u32[]{:S(2)}) collective-permute-start(bf16[2,64,256]{2,1,0:T(8,128)(2,1)S(1)} %pad_maximum_fusion.2), channel_id=1, source_target_pairs={{0,6},{2,8},{4,10},{6,12},{8,14},{10,0},{12,2},{14,4},{1,11},{3,13... | collective-permute-start | bytes 196616 | tf_op jit(solution)/shard_map/ppermute | solution.py:33
  57.7 2.4 %collective-permute-start.26 = (bf16[1,64,256]{2,1,0:T(8,128)(2,1)S(1)}, bf16[1,64,256]{2,1,0:T(8,128)(2,1)S(1)}, u32[]{:S(2)}, u32[]{:S(2)}) collective-permute-start(bf16[1,64,256]{2,1,0:T(8,128)(2,1)S(1)} %slice.128), channel_id=1, source_target_pairs={{0,2},{2,4},{4,6},{6,8},{8,10},{10,12},{12,14},{14,0},{1,15},{3,1}... | collective-permute-start | bytes 98312 | tf_op jit(solution)/shard_map/ppermute | solution.py:33
  62.3 2.5 %collective-permute-start.27 = (bf16[2,64,256]{2,1,0:T(8,128)(2,1)S(1)}, bf16[2,64,256]{2,1,0:T(8,128)(2,1)S(1)}, u32[]{:S(2)}, u32[]{:S(2)}) collective-permute-start(bf16[2,64,256]{2,1,0:T(8,128)(2,1)S(1)} %collective-permute-done.23.refs_0_), channel_id=1, source_target_pairs={{0,1},{1,0},{2,3},{3,2},{4,5},{5,4},{6,7},{7,6},{8,9},{9,8},{10,11... | collective-permute-start | bytes 196616 | tf_op jit(solution)/shard_map/ppermute | solution.py:21
  64.8 2.4 %collective-permute-start.28 = (bf16[2,64,256]{2,1,0:T(8,128)(2,1)S(1)}, bf16[2,64,256]{2,1,0:T(8,128)(2,1)S(1)}, u32[]{:S(2)}, u32[]{:S(2)}) collective-permute-start(bf16[2,64,256]{2,1,0:T(8,128)(2,1)S(1)} %collective-permute-done.24.refs_1_), channel_id=1, source_target_pairs={{0,1},{1,0},{2,3},{3,2},{4,5},{5,4},{6,7},{7,6},{8,9},{9,8},{10,11... | collective-permute-start | bytes 196616 | tf_op jit(solution)/shard_map/ppermute | solution.py:21
  69.8 3.6 %collective-permute-start.11 = (bf16[528,128]{1,0:T(8,128)(2,1)}, bf16[528,128]{1,0:T(8,128)(2,1)S(1)}, u32[]{:S(2)}, u32[]{:S(2)}) collective-permute-start(bf16[528,128]{1,0:T(8,128)(2,1)} %get-tuple-element.24), channel_id=1, source_target_pairs={{0,12},{2,14},{4,0},{6,2},{8,4},{10,6},{12,8},{14,10},{1,13},{3,15... | collective-permute-start | bytes 405512 | tf_op jit(solution)/shard_map/ppermute | solution.py:26
  74.0 4.5 %collective-permute-start.13 = (bf16[528,128]{1,0:T(8,128)(2,1)}, bf16[528,128]{1,0:T(8,128)(2,1)S(1)}, u32[]{:S(2)}, u32[]{:S(2)}) collective-permute-start(bf16[528,128]{1,0:T(8,128)(2,1)} %add_convert_fusion.2), channel_id=1, source_target_pairs={{0,10},{2,12},{4,14},{6,0},{8,2},{10,4},{12,6},{14,8},{1,11},{3,13... | collective-permute-start | bytes 405512 | tf_op jit(solution)/shard_map/ppermute | solution.py:26
  81.7 3.4 %shared.1 = (bf16[8,64,256]{2,1,0:T(8,128)(2,1)S(1)}, bf16[8,64,256]{2,1,0:T(8,128)(2,1)}) custom-call(s32[4]{0:T(128)S(1)} %copy-done.9, bf16[64,256]{1,0:T(8,128)(2,1)S(1)} %get-tuple-element.34.own_in.own, bf16[64,256]{1,0:T(8,128)(2,1)S(1)} %get-tuple-element.33.par_in.par, bf16[2,64,256]{2,1,0:T(8,128)(2,1)S(1)} %collective-permute-done.23.refs_0_, ...), custom_call_target="tpu_custom_call" | custom-call | flops 100663296 | bytes 1572864 | tf_op jit(solution)/shard_map/shared/pallas_call | solution.py:401
  90.9 2.9 %collective-permute-start.15 = (bf16[2,256,128]{2,1,0:T(8,128)(2,1)S(1)}, bf16[2,256,128]{2,1,0:T(8,128)(2,1)S(1)}, u32[]{:S(2)}, u32[]{:S(2)}) collective-permute-start(bf16[2,256,128]{2,1,0:T(8,128)(2,1)S(1)} %pad_maximum_fusion), channel_id=1, source_target_pairs={{0,2},{2,4},{4,6},{6,8},{8,10},{10,12},{12,14},{14,0},{1,15},{3,1}... | collective-permute-start | bytes 393224 | tf_op jit(solution)/shard_map/ppermute | solution.py:33
  93.9 2.8 %collective-permute-start.16 = (bf16[2,256,128]{2,1,0:T(8,128)(2,1)S(1)}, bf16[2,256,128]{2,1,0:T(8,128)(2,1)S(1)}, u32[]{:S(2)}, u32[]{:S(2)}) collective-permute-start(bf16[2,256,128]{2,1,0:T(8,128)(2,1)S(1)} %pad_maximum_fusion), channel_id=1, source_target_pairs={{0,4},{2,6},{4,8},{6,10},{8,12},{10,14},{12,0},{14,2},{1,13},{3,15... | collective-permute-start | bytes 393224 | tf_op jit(solution)/shard_map/ppermute | solution.py:33
  99.1 4.5 %collective-permute-done.16.refs_1_ = bf16[2,256,128]{2,1,0:T(8,128)(2,1)S(1)} collective-permute-done((bf16[2,256,128]{2,1,0:T(8,128)(2,1)S(1)}, bf16[2,256,128]{2,1,0:T(8,128)(2,1)S(1)}, u32[]{:S(2)}, u32[]{:S(2)}) %collective-permute-start.16) | collective-permute-done | bytes 131104 | tf_op jit(solution)/shard_map/ppermute | solution.py:33
  103.6 2.9 %collective-permute-start.19 = (bf16[256,128]{1,0:T(8,128)(2,1)S(1)}, bf16[256,128]{1,0:T(8,128)(2,1)S(1)}, u32[]{:S(2)}, u32[]{:S(2)}) collective-permute-start(bf16[256,128]{1,0:T(8,128)(2,1)S(1)} %slice_bitcast_fusion.2), channel_id=1, source_target_pairs={{0,1},{1,0},{2,3},{3,2},{4,5},{5,4},{6,7},{7,6},{8,9},{9,8},{10,11... | collective-permute-start | bytes 196616 | tf_op jit(solution)/shard_map/ppermute | solution.py:21
  111.4 2.8 %collective-permute-start.34 = (bf16[2,64,256]{2,1,0:T(8,128)(2,1)S(1)}, bf16[2,64,256]{2,1,0:T(8,128)(2,1)S(1)}, u32[]{:S(2)}, u32[]{:S(2)}) collective-permute-start(bf16[2,64,256]{2,1,0:T(8,128)(2,1)S(1)} %get-tuple-element.37), channel_id=1, source_target_pairs={{0,6},{2,8},{4,10},{6,12},{8,14},{10,0},{12,2},{14,4},{1,11},{3,13... | collective-permute-start | bytes 196616 | tf_op jit(solution)/shard_map/ppermute | solution.py:33
  114.2 3.5 %down.1 = bf16[16,2,16,256]{3,2,1,0:T(8,128)(2,1)} custom-call(s32[4]{0:T(128)S(1)} %copy-done.10, bf16[256,128]{1,0:T(8,128)(2,1)S(1)} %inner.1.mine, bf16[2,256,128]{2,1,0:T(8,128)(2,1)S(1)} %collective-permute-done.15.refs_0_, bf16[2,256,128]{2,1,0:T(8,128)(2,1)S(1)} %collective-permute-done.16.refs_1_, ...), custom_call_target="tpu_custom_call" | custom-call | flops 268435456 | bytes 2097152 | tf_op jit(solution)/shard_map/down/pallas_call | solution.py:524
  117.7 3.5 %all-to-all-start.1 = ((bf16[16,2,16,256]{3,2,1,0:T(8,128)(2,1)}), bf16[16,2,16,256]{3,2,1,0:T(8,128)(2,1)S(1)}, u32[]{:S(2)}, u32[]{:S(2)}) async-start(bf16[16,2,16,256]{3,2,1,0:T(8,128)(2,1)} %down.1), calls=%async_computation.1 | async-start | bytes 524288 | tf_op jit(solution)/shard_map/all_to_all | solution.py:656
  121.3 2.9 %collective-permute-start.35 = (bf16[1,64,256]{2,1,0:T(8,128)(2,1)S(1)}, bf16[1,64,256]{2,1,0:T(8,128)(2,1)S(1)}, u32[]{:S(2)}, u32[]{:S(2)}) collective-permute-start(bf16[1,64,256]{2,1,0:T(8,128)(2,1)S(1)} %get-tuple-element.35), channel_id=1, source_target_pairs={{0,8},{2,10},{4,12},{6,14},{8,0},{10,2},{12,4},{14,6},{1,9},{3,11}... | collective-permute-start | bytes 98312 | tf_op jit(solution)/shard_map/ppermute | solution.py:33
  124.2 4.5 %collective-permute-done.35.refs_3_ = bf16[1,64,256]{2,1,0:T(8,128)(2,1)S(1)} collective-permute-done((bf16[1,64,256]{2,1,0:T(8,128)(2,1)S(1)}, bf16[1,64,256]{2,1,0:T(8,128)(2,1)S(1)}, u32[]{:S(2)}, u32[]{:S(2)}) %collective-permute-start.35) | collective-permute-done | bytes 32800 | tf_op jit(solution)/shard_map/ppermute | solution.py:33
  (132 shorter events, 40.2 us)
Async XLA Ops:
  8.0 36.5 %collective-permute-start.6 = (bf16[4,256,1024]{2,1,0:T(8,128)(2,1)}, bf16[4,256,1024]{2,1,0:T(8,128)(2,1)}, u32[]{:S(2)}, u32[]{:S(2)}) collective-permute-start(bf16[4,256,1024]{2,1,0:T(8,128)(2,1)} %gate.1), channel_id=1, source_target_pairs={{0,1},{1,0},{2,3},{3,2},{4,5},{5,4},{6,7},{7,6},{8,9},{9,8},{10,11... | collective-permute-start | bytes 6291464 | tf_op jit(solution)/shard_map/ppermute | solution.py:21
  8.1 36.4 %collective-permute-start.7 = (bf16[4,256,1024]{2,1,0:T(8,128)(2,1)}, bf16[4,256,1024]{2,1,0:T(8,128)(2,1)}, u32[]{:S(2)}, u32[]{:S(2)}) collective-permute-start(bf16[4,256,1024]{2,1,0:T(8,128)(2,1)} %up.1), channel_id=1, source_target_pairs={{0,1},{1,0},{2,3},{3,2},{4,5},{5,4},{6,7},{7,6},{8,9},{9,8},{10,11... | collective-permute-start | bytes 6291464 | tf_op jit(solution)/shard_map/ppermute | solution.py:21
  10.9 9.4 %collective-permute-start.4 = (bf16[1,64,256]{2,1,0:T(8,128)(2,1)S(1)}, bf16[1,64,256]{2,1,0:T(8,128)(2,1)S(1)}, u32[]{:S(2)}, u32[]{:S(2)}) collective-permute-start(bf16[1,64,256]{2,1,0:T(8,128)(2,1)S(1)} %slice.115), channel_id=1, source_target_pairs={{0,8},{2,10},{4,12},{6,14},{8,0},{10,2},{12,4},{14,6},{1,9},{3,11}... | collective-permute-start | bytes 98312 | tf_op jit(solution)/shard_map/ppermute | solution.py:33
  29.5 14.9 %all-to-all-start = ((bf16[16,2,16,256]{3,2,1,0:T(8,128)(2,1)}), bf16[16,2,16,256]{3,2,1,0:T(8,128)(2,1)S(1)}, u32[]{:S(2)}, u32[]{:S(2)}) async-start(bf16[16,2,16,256]{3,2,1,0:T(8,128)(2,1)} %dispatch.1), calls=%async_computation | async-start | bytes 524288 | tf_op jit(solution)/shard_map/all_to_all | solution.py:623
  49.2 10.9 %collective-permute-start.8 = (bf16[792,128]{1,0:T(8,128)(2,1)S(1)}, bf16[792,128]{1,0:T(8,128)(2,1)S(1)}, u32[]{:S(2)}, u32[]{:S(2)}) collective-permute-start(bf16[792,128]{1,0:T(8,128)(2,1)S(1)} %get-tuple-element.21), channel_id=1, source_target_pairs={{0,2},{2,4},{4,6},{6,8},{8,10},{10,12},{12,14},{14,0},{1,3},{3,5},... | collective-permute-start | bytes 608264 | tf_op jit(solution)/shard_map/ppermute | solution.py:26
  49.7 17.4 %collective-permute-start.9 = (bf16[792,128]{1,0:T(8,128)(2,1)S(1)}, bf16[792,128]{1,0:T(8,128)(2,1)S(1)}, u32[]{:S(2)}, u32[]{:S(2)}) collective-permute-start(bf16[792,128]{1,0:T(8,128)(2,1)S(1)} %get-tuple-element.22), channel_id=1, source_target_pairs={{0,14},{2,0},{4,2},{6,4},{8,6},{10,8},{12,10},{14,12},{1,15},{3,1}... | collective-permute-start | bytes 608264 | tf_op jit(solution)/shard_map/ppermute | solution.py:26
  60.1 47.7 %collective-permute-start.22 = (bf16[4,1024,256]{2,1,0:T(8,128)(2,1)S(1)}, bf16[4,1024,256]{2,1,0:T(8,128)(2,1)}, u32[]{:S(2)}, u32[]{:S(2)}) collective-permute-start(bf16[4,1024,256]{2,1,0:T(8,128)(2,1)S(1)} %copy-done), channel_id=1, source_target_pairs={{0,1},{1,0},{2,3},{3,2},{4,5},{5,4},{6,7},{7,6},{8,9},{9,8},{10,11... | collective-permute-start | bytes 6291464 | tf_op jit(solution)/shard_map/ppermute | solution.py:21
  62.2 11.2 %collective-permute-start.29 = (bf16[2,64,256]{2,1,0:T(8,128)(2,1)S(1)}, bf16[2,64,256]{2,1,0:T(8,128)(2,1)S(1)}, u32[]{:S(2)}, u32[]{:S(2)}) collective-permute-start(bf16[2,64,256]{2,1,0:T(8,128)(2,1)S(1)} %collective-permute-done.25.refs_2_), channel_id=1, source_target_pairs={{0,1},{1,0},{2,3},{3,2},{4,5},{5,4},{6,7},{7,6},{8,9},{9,8},{10,11... | collective-permute-start | bytes 196616 | tf_op jit(solution)/shard_map/ppermute | solution.py:21
  69.2 15.9 %collective-permute-start.10 = (bf16[528,128]{1,0:T(8,128)(2,1)}, bf16[528,128]{1,0:T(8,128)(2,1)S(1)}, u32[]{:S(2)}, u32[]{:S(2)}) collective-permute-start(bf16[528,128]{1,0:T(8,128)(2,1)} %get-tuple-element.23), channel_id=1, source_target_pairs={{0,4},{2,6},{4,8},{6,10},{8,12},{10,14},{12,0},{14,2},{1,5},{3,7},... | collective-permute-start | bytes 405512 | tf_op jit(solution)/shard_map/ppermute | solution.py:26
  69.8 17.0 %collective-permute-start.11 = (bf16[528,128]{1,0:T(8,128)(2,1)}, bf16[528,128]{1,0:T(8,128)(2,1)S(1)}, u32[]{:S(2)}, u32[]{:S(2)}) collective-permute-start(bf16[528,128]{1,0:T(8,128)(2,1)} %get-tuple-element.24), channel_id=1, source_target_pairs={{0,12},{2,14},{4,0},{6,2},{8,4},{10,6},{12,8},{14,10},{1,13},{3,15... | collective-permute-start | bytes 405512 | tf_op jit(solution)/shard_map/ppermute | solution.py:26
  74.0 13.7 %collective-permute-start.12 = (bf16[528,128]{1,0:T(8,128)(2,1)}, bf16[528,128]{1,0:T(8,128)(2,1)S(1)}, u32[]{:S(2)}, u32[]{:S(2)}) collective-permute-start(bf16[528,128]{1,0:T(8,128)(2,1)} %add_convert_fusion.3), channel_id=1, source_target_pairs={{0,6},{2,8},{4,10},{6,12},{8,14},{10,0},{12,2},{14,4},{1,7},{3,9},... | collective-permute-start | bytes 405512 | tf_op jit(solution)/shard_map/ppermute | solution.py:26
  74.0 13.7 %collective-permute-start.13 = (bf16[528,128]{1,0:T(8,128)(2,1)}, bf16[528,128]{1,0:T(8,128)(2,1)S(1)}, u32[]{:S(2)}, u32[]{:S(2)}) collective-permute-start(bf16[528,128]{1,0:T(8,128)(2,1)} %add_convert_fusion.2), channel_id=1, source_target_pairs={{0,10},{2,12},{4,14},{6,0},{8,2},{10,4},{12,6},{14,8},{1,11},{3,13... | collective-permute-start | bytes 405512 | tf_op jit(solution)/shard_map/ppermute | solution.py:26
  85.1 8.8 %collective-permute-start.31 = (bf16[8,64,256]{2,1,0:T(8,128)(2,1)}, bf16[8,64,256]{2,1,0:T(8,128)(2,1)S(1)}, u32[]{:S(2)}, u32[]{:S(2)}) collective-permute-start(bf16[8,64,256]{2,1,0:T(8,128)(2,1)} %get-tuple-element.28), channel_id=1, source_target_pairs={{0,1},{1,0},{2,3},{3,2},{4,5},{5,4},{6,7},{7,6},{8,9},{9,8},{10,11... | collective-permute-start | bytes 786440 | tf_op jit(solution)/shard_map/ppermute | solution.py:21
  90.9 8.1 %collective-permute-start.15 = (bf16[2,256,128]{2,1,0:T(8,128)(2,1)S(1)}, bf16[2,256,128]{2,1,0:T(8,128)(2,1)S(1)}, u32[]{:S(2)}, u32[]{:S(2)}) collective-permute-start(bf16[2,256,128]{2,1,0:T(8,128)(2,1)S(1)} %pad_maximum_fusion), channel_id=1, source_target_pairs={{0,2},{2,4},{4,6},{6,8},{8,10},{10,12},{12,14},{14,0},{1,15},{3,1}... | collective-permute-start | bytes 393224 | tf_op jit(solution)/shard_map/ppermute | solution.py:33
  93.9 9.6 %collective-permute-start.16 = (bf16[2,256,128]{2,1,0:T(8,128)(2,1)S(1)}, bf16[2,256,128]{2,1,0:T(8,128)(2,1)S(1)}, u32[]{:S(2)}, u32[]{:S(2)}) collective-permute-start(bf16[2,256,128]{2,1,0:T(8,128)(2,1)S(1)} %pad_maximum_fusion), channel_id=1, source_target_pairs={{0,4},{2,6},{4,8},{6,10},{8,12},{10,14},{12,0},{14,2},{1,13},{3,15... | collective-permute-start | bytes 393224 | tf_op jit(solution)/shard_map/ppermute | solution.py:33
  96.7 9.7 %collective-permute-start.17 = (bf16[2,256,128]{2,1,0:T(8,128)(2,1)S(1)}, bf16[2,256,128]{2,1,0:T(8,128)(2,1)S(1)}, u32[]{:S(2)}, u32[]{:S(2)}) collective-permute-start(bf16[2,256,128]{2,1,0:T(8,128)(2,1)S(1)} %pad_maximum_fusion), channel_id=1, source_target_pairs={{0,6},{2,8},{4,10},{6,12},{8,14},{10,0},{12,2},{14,4},{1,11},{3,13... | collective-permute-start | bytes 393224 | tf_op jit(solution)/shard_map/ppermute | solution.py:33
  99.0 10.7 %collective-permute-start.18 = (bf16[256,128]{1,0:T(8,128)(2,1)S(1)}, bf16[256,128]{1,0:T(8,128)(2,1)S(1)}, u32[]{:S(2)}, u32[]{:S(2)}) collective-permute-start(bf16[256,128]{1,0:T(8,128)(2,1)S(1)} %slice_bitcast_fusion.3), channel_id=1, source_target_pairs={{0,1},{1,0},{2,3},{3,2},{4,5},{5,4},{6,7},{7,6},{8,9},{9,8},{10,11... | collective-permute-start | bytes 196616 | tf_op jit(solution)/shard_map/ppermute | solution.py:21
  103.6 7.9 %collective-permute-start.19 = (bf16[256,128]{1,0:T(8,128)(2,1)S(1)}, bf16[256,128]{1,0:T(8,128)(2,1)S(1)}, u32[]{:S(2)}, u32[]{:S(2)}) collective-permute-start(bf16[256,128]{1,0:T(8,128)(2,1)S(1)} %slice_bitcast_fusion.2), channel_id=1, source_target_pairs={{0,1},{1,0},{2,3},{3,2},{4,5},{5,4},{6,7},{7,6},{8,9},{9,8},{10,11... | collective-permute-start | bytes 196616 | tf_op jit(solution)/shard_map/ppermute | solution.py:21
  106.5 7.8 %collective-permute-start.20 = (bf16[256,128]{1,0:T(8,128)(2,1)S(1)}, bf16[256,128]{1,0:T(8,128)(2,1)S(1)}, u32[]{:S(2)}, u32[]{:S(2)}) collective-permute-start(bf16[256,128]{1,0:T(8,128)(2,1)S(1)} %get-tuple-element.46), channel_id=1, source_target_pairs={{0,1},{1,0},{2,3},{3,2},{4,5},{5,4},{6,7},{7,6},{8,9},{9,8},{10,11... | collective-permute-start | bytes 196616 | tf_op jit(solution)/shard_map/ppermute | solution.py:21
  107.7 21.0 %collective-permute-start.32 = (bf16[2,64,256]{2,1,0:T(8,128)(2,1)S(1)}, bf16[2,64,256]{2,1,0:T(8,128)(2,1)S(1)}, u32[]{:S(2)}, u32[]{:S(2)}) collective-permute-start(bf16[2,64,256]{2,1,0:T(8,128)(2,1)S(1)} %get-tuple-element.39), channel_id=1, source_target_pairs={{0,2},{2,4},{4,6},{6,8},{8,10},{10,12},{12,14},{14,0},{1,15},{3,1}... | collective-permute-start | bytes 196616 | tf_op jit(solution)/shard_map/ppermute | solution.py:33
  109.7 19.1 %collective-permute-start.33 = (bf16[2,64,256]{2,1,0:T(8,128)(2,1)S(1)}, bf16[2,64,256]{2,1,0:T(8,128)(2,1)S(1)}, u32[]{:S(2)}, u32[]{:S(2)}) collective-permute-start(bf16[2,64,256]{2,1,0:T(8,128)(2,1)S(1)} %get-tuple-element.38), channel_id=1, source_target_pairs={{0,4},{2,6},{4,8},{6,10},{8,12},{10,14},{12,0},{14,2},{1,13},{3,15... | collective-permute-start | bytes 196616 | tf_op jit(solution)/shard_map/ppermute | solution.py:33
  111.4 17.4 %collective-permute-start.34 = (bf16[2,64,256]{2,1,0:T(8,128)(2,1)S(1)}, bf16[2,64,256]{2,1,0:T(8,128)(2,1)S(1)}, u32[]{:S(2)}, u32[]{:S(2)}) collective-permute-start(bf16[2,64,256]{2,1,0:T(8,128)(2,1)S(1)} %get-tuple-element.37), channel_id=1, source_target_pairs={{0,6},{2,8},{4,10},{6,12},{8,14},{10,0},{12,2},{14,4},{1,11},{3,13... | collective-permute-start | bytes 196616 | tf_op jit(solution)/shard_map/ppermute | solution.py:33
  117.7 12.3 %all-to-all-start.1 = ((bf16[16,2,16,256]{3,2,1,0:T(8,128)(2,1)}), bf16[16,2,16,256]{3,2,1,0:T(8,128)(2,1)S(1)}, u32[]{:S(2)}, u32[]{:S(2)}) async-start(bf16[16,2,16,256]{3,2,1,0:T(8,128)(2,1)} %down.1), calls=%async_computation.1 | async-start | bytes 524288 | tf_op jit(solution)/shard_map/all_to_all | solution.py:656
  121.3 7.5 %collective-permute-start.35 = (bf16[1,64,256]{2,1,0:T(8,128)(2,1)S(1)}, bf16[1,64,256]{2,1,0:T(8,128)(2,1)S(1)}, u32[]{:S(2)}, u32[]{:S(2)}) collective-permute-start(bf16[1,64,256]{2,1,0:T(8,128)(2,1)S(1)} %get-tuple-element.35), channel_id=1, source_target_pairs={{0,8},{2,10},{4,12},{6,14},{8,0},{10,2},{12,4},{14,6},{1,9},{3,11}... | collective-permute-start | bytes 98312 | tf_op jit(solution)/shard_map/ppermute | solution.py:33
  (31 other events, 322.2 us)
